TPU v7x, 32 devices: a whole 2x2x4 slice. The times are simulated.
32 devices in a mesh: grp: 2 (over x), sp: 8 (over z, y), tp: 2 (over core).
Axes of the slice: x: 2, y: 2, z: 4, core: 2. Of those that a mesh axis runs over, the one named last changes fastest.
Arguments:
- tokens: bfloat16 [8192, 2048], P(('grp', 'sp', 'tp')), parts along dimension 0, may hold values from -64 to 64
- w_query: bfloat16 [2048, 1024], P(None, 'tp'), may hold values from -0.125 to 0.125
- w_key: bfloat16 [2048, 1024], P(None, 'tp'), may hold values from -0.125 to 0.125
- w_value: bfloat16 [2048, 1024], P(None, 'tp'), may hold values from -0.25 to 0.25
- w_out: bfloat16 [1024, 2048], P('tp'), may hold values from -0.1875 to 0.1875
Outputs:
- mixed: bfloat16 [8192, 2048], P(('grp', 'sp', 'tp')), parts along dimension 0
- log_sums: float32 [16, 8192], P('tp', ('grp', 'sp')), parts along dimension 1
There are 2 independent parts, one for each index of `grp`. A program takes and returns all parts, laid end to end along the dimension named above; an argument that names none is the same for every part. Nothing has to cross between parts.
All inputs are finite; a program needn't handle non-finite values.
Results may differ from a plain program's by a relative error of at most 0.013.
The roundings to bfloat16 on the way count: a program that leaves them out, or rounds other values in their place, can miss the bound.
Values may be sent and summed in bfloat16 or wider, within the bound.
No kernel may reach another device: no remote copies, remote signals or barrier semaphores. Data moves between devices by JAX's collectives and lax.ppermute only.
A program may use at most 128 MiB of HBM per device.

v0:
```python
import math

import jax
import jax.numpy as jnp
from jax import lax
from jax.sharding import PartitionSpec as P

HEADS = 16
HEAD_DIM = 64
WINDOW_KEY_STEPS = 128
MIDDLE_DILATION = 4
FAR_DILATION = 16
REACH = 2048


ALIBI_EXP = 16.0


def shifted(value, axis, steps):
    count = lax.axis_size(axis)
    leading, last = (max(0, -steps), min(count, count - steps))
    return lax.ppermute(value, axis, [(source, source + steps) for source in range(leading, last)])


def dilated_attention(queries, key_values, dilation, window_steps, head_slopes, first_position):
    heads, length, depth = queries.shape
    total_rows = key_values.shape[2]
    strided = length // dilation
    block_rows = math.gcd(strided, 128)
    num_blocks = strided // block_rows
    behind = (total_rows - length) // dilation
    grouped = queries.reshape(heads, num_blocks, block_rows, dilation, depth)
    columns = key_values.reshape(2, heads, total_rows // dilation, dilation, depth)
    spans = jnp.stack(
        [
            columns[
                :, :, behind + index * block_rows - window_steps : behind + (index + 1) * block_rows
            ]
            for index in range(num_blocks)
        ],
        axis=2,
    )
    scores = jnp.einsum(
        "hbqre,hbkre->hrbqk", grouped, spans[0], preferred_element_type=jnp.float32
    ) * depth ** (-0.5)
    row_pos = jnp.arange(block_rows, dtype=jnp.int32)[:, None]
    key_pos = jnp.arange(window_steps + block_rows, dtype=jnp.int32)[None, :]
    distance = window_steps + row_pos - key_pos
    inside = (distance >= 0) & (distance <= window_steps)
    block_pos = jnp.arange(num_blocks, dtype=jnp.int32)[None, :, None, None]
    residue = jnp.arange(dilation, dtype=jnp.int32)[:, None, None, None]
    source = (
        first_position
        + (block_pos * block_rows - window_steps + key_pos[None, None]) * dilation
        + residue
    )
    allowed = inside[None, None] & (source >= 0)
    penalty = -head_slopes[:, None, None] * (distance * dilation).astype(jnp.float32)
    scores = jnp.where(allowed[None], scores + penalty[:, None, None], -jnp.inf)
    maxima = jnp.max(scores, axis=-1, keepdims=True)
    weights = jnp.exp(scores - maxima)
    totals = jnp.sum(weights, axis=-1, keepdims=True)
    summed = jnp.einsum(
        "hrbqk,hbkre->hbqre",
        weights.astype(jnp.bfloat16),
        spans[1],
        preferred_element_type=jnp.float32,
    )
    outputs = summed / totals.transpose(0, 2, 3, 1, 4)
    log_part = (maxima + jnp.log(totals))[..., 0]
    outputs = outputs.reshape(heads, length, depth)
    log_part = log_part.transpose(0, 2, 3, 1).reshape(heads, length)
    return (outputs, log_part)


def combine(queries, key_values, head_slopes, first_position):
    heads, length, depth = queries.shape
    window_results = [
        dilated_attention(
            queries, key_values, window_stride, WINDOW_KEY_STEPS, head_slopes, first_position
        )
        for window_stride in (1, MIDDLE_DILATION, FAR_DILATION)
    ]
    stacked = jnp.stack([item[1] for item in window_results])
    log_total = jax.nn.logsumexp(stacked, axis=0)
    hidden = jnp.zeros((heads, length, depth), jnp.float32)
    for item in window_results:
        hidden = hidden + jnp.exp(item[1] - log_total)[..., None] * item[0]
    hidden = hidden.astype(jnp.bfloat16).transpose(1, 0, 2).reshape(length, heads * depth)
    return (hidden, log_total)


def body(tokens, w_query, w_key, w_value, w_out):
    width = w_query.shape[1]
    local_heads = width // HEAD_DIM
    query_heads = w_query.reshape(w_query.shape[0], local_heads, HEAD_DIM)
    key_heads = w_key.reshape(w_key.shape[0], local_heads, HEAD_DIM)
    value_heads = w_value.reshape(w_value.shape[0], local_heads, HEAD_DIM)
    piece = lax.all_gather(tokens, "tp", axis=0, tiled=True)
    projected = jnp.stack(
        [
            jnp.einsum(
                "td,dhe->hte", piece, query_heads, preferred_element_type=jnp.float32
            ).astype(jnp.bfloat16),
            jnp.einsum("td,dhe->hte", piece, key_heads, preferred_element_type=jnp.float32).astype(
                jnp.bfloat16
            ),
            jnp.einsum(
                "td,dhe->hte", piece, value_heads, preferred_element_type=jnp.float32
            ).astype(jnp.bfloat16),
        ]
    )
    length = projected.shape[2]
    queries = projected[0]
    key_values = projected[1:]
    hop_count = -(-REACH // length)
    pieces = [key_values]
    carried = key_values
    for distance_dev in range(hop_count):
        carried = shifted(carried, "sp", 1)
        pieces = [carried] + pieces
    window_rows = jnp.concatenate(pieces, axis=2)
    first_position = lax.axis_index("sp") * length
    head_ids = lax.axis_index("tp") * local_heads + jnp.arange(1, local_heads + 1, dtype=jnp.int32)
    head_slopes = jnp.exp2(-ALIBI_EXP * head_ids.astype(jnp.float32) / HEADS)
    hidden, log_total = combine(queries, window_rows, head_slopes, first_position)
    mixed = lax.psum_scatter(
        jnp.dot(hidden, w_out, preferred_element_type=jnp.float32).astype(jnp.bfloat16),
        "tp",
        scatter_dimension=0,
        tiled=True,
    )
    return (mixed, log_total)


def solution(mesh):
    in_specs = (
        P(("grp", "sp", "tp"), None),
        P(None, "tp"),
        P(None, "tp"),
        P(None, "tp"),
        P("tp", None),
    )
    out_specs = (P(("grp", "sp", "tp"), None), P("tp", ("grp", "sp")))
    return jax.shard_map(body, mesh=mesh, in_specs=in_specs, out_specs=out_specs, check_vma=False)
```

profile of v0, /device:TPU:0, one launch (start us, length us, event | category | flops | bytes accessed | tf_op | source)
XLA Modules:
  0.0 257.2 jit_solution(8725447888651697060)
XLA Ops:
  8.0 4.0 %copy.93 = bf16[2048,512]{0,1:T(8,128)(2,1)} copy(bf16[2048,512]{1,0:T(8,128)(2,1)} %param.8) | data formatting | bytes 4194304 | tf_op args[3]
  11.9 4.0 %copy.92 = bf16[2048,512]{0,1:T(8,128)(2,1)} copy(bf16[2048,512]{1,0:T(8,128)(2,1)} %param.7) | data formatting | bytes 4194304 | tf_op args[2]
  15.9 7.0 %all-gather.2.cloned.1.call-done = bf16[512,2048]{1,0:T(8,128)(2,1)} async-done(((bf16[256,2048]{1,0:T(8,128)(2,1)}), bf16[512,2048]{1,0:T(8,128)(2,1)}) %all-gather.2.cloned.1.call-update) | async-done | bytes 2097168 | tf_op jit(solution)/shard_map/all_gather | solution.py:99
  22.9 3.7 %fusion.46 = bf16[1,8,512,64]{2,3,1,0:T(8,128)(2,1)S(1)} fusion(bf16[2048,8,64]{0,2,1:T(8,128)(2,1)} %bitcast.148, bf16[512,2048]{1,0:T(8,128)(2,1)} %all-gather.2.cloned.1.call-done), kind=kOutput, calls=%fused_computation.42 | convolution fusion | flops 1074003968 | bytes 4718592 | tf_op jit(solution)/shard_map/td,dhe->hte/dot_general | solution.py:108
  26.6 1.3 fusion.49
  29.0 3.7 %collective-permute-start = (bf16[2,8,512,64]{2,3,1,0:T(8,128)(2,1)}, bf16[2,8,512,64]{2,3,1,0:T(8,128)(2,1)S(1)}, u32[]{:S(2)}, u32[]{:S(2)}) collective-permute-start(bf16[2,8,512,64]{2,3,1,0:T(8,128)(2,1)} %pad_maximum_fusion.1), channel_id=1, source_target_pairs={{0,2},{2,4},{4,6},{6,8},{8,10},{10,12},{12,14},{1,3},{3,5},{5,7},{... | collective-permute-start | bytes 3145736 | tf_op jit(solution)/shard_map/ppermute | solution.py:22
  32.7 23.1 %collective-permute-done = bf16[2,8,512,64]{2,3,1,0:T(8,128)(2,1)S(1)} collective-permute-done((bf16[2,8,512,64]{2,3,1,0:T(8,128)(2,1)}, bf16[2,8,512,64]{2,3,1,0:T(8,128)(2,1)S(1)}, u32[]{:S(2)}, u32[]{:S(2)}) %collective-permute-start) | collective-permute-done | bytes 1048608 | tf_op jit(solution)/shard_map/ppermute | solution.py:22
  55.8 5.3 %collective-permute-start.1 = (bf16[2,8,512,64]{2,3,1,0:T(8,128)(2,1)S(1)}, bf16[2,8,512,64]{2,3,1,0:T(8,128)(2,1)}, u32[]{:S(2)}, u32[]{:S(2)}) collective-permute-start(bf16[2,8,512,64]{2,3,1,0:T(8,128)(2,1)S(1)} %collective-permute-done), channel_id=1, source_target_pairs={{0,2},{2,4},{4,6},{6,8},{8,10},{10,12},{12,14},{1,3},{3,5},{5,7},{... | collective-permute-start | bytes 3145736 | tf_op jit(solution)/shard_map/ppermute | solution.py:22
  61.3 20.8 %collective-permute-done.1 = bf16[2,8,512,64]{2,3,1,0:T(8,128)(2,1)} collective-permute-done((bf16[2,8,512,64]{2,3,1,0:T(8,128)(2,1)S(1)}, bf16[2,8,512,64]{2,3,1,0:T(8,128)(2,1)}, u32[]{:S(2)}, u32[]{:S(2)}) %collective-permute-start.1) | collective-permute-done | bytes 1048608 | tf_op jit(solution)/shard_map/ppermute | solution.py:22
  82.1 5.5 %collective-permute-start.2 = (bf16[2,8,512,64]{2,3,1,0:T(8,128)(2,1)}, bf16[2,8,512,64]{2,3,1,0:T(8,128)(2,1)}, u32[]{:S(2)}, u32[]{:S(2)}) collective-permute-start(bf16[2,8,512,64]{2,3,1,0:T(8,128)(2,1)} %collective-permute-done.1), channel_id=1, source_target_pairs={{0,2},{2,4},{4,6},{6,8},{8,10},{10,12},{12,14},{1,3},{3,5},{5,7},{... | collective-permute-start | bytes 3145736 | tf_op jit(solution)/shard_map/ppermute | solution.py:22
  87.6 4.0 %copy.91 = bf16[2048,512]{0,1:T(8,128)(2,1)} copy(bf16[2048,512]{1,0:T(8,128)(2,1)} %param.6) | data formatting | bytes 4194304 | tf_op args[1]
  92.7 15.4 %collective-permute-done.2 = bf16[2,8,512,64]{2,3,1,0:T(8,128)(2,1)} collective-permute-done((bf16[2,8,512,64]{2,3,1,0:T(8,128)(2,1)}, bf16[2,8,512,64]{2,3,1,0:T(8,128)(2,1)}, u32[]{:S(2)}, u32[]{:S(2)}) %collective-permute-start.2) | collective-permute-done | bytes 1048608 | tf_op jit(solution)/shard_map/ppermute | solution.py:22
  108.0 6.1 %collective-permute-start.3 = (bf16[2,8,512,64]{2,3,1,0:T(8,128)(2,1)}, bf16[2,8,512,64]{2,3,1,0:T(8,128)(2,1)}, u32[]{:S(2)}, u32[]{:S(2)}) collective-permute-start(bf16[2,8,512,64]{2,3,1,0:T(8,128)(2,1)} %collective-permute-done.2), channel_id=1, source_target_pairs={{0,2},{2,4},{4,6},{6,8},{8,10},{10,12},{12,14},{1,3},{3,5},{5,7},{... | collective-permute-start | bytes 3145736 | tf_op jit(solution)/shard_map/ppermute | solution.py:22
  114.3 1.2 broadcast_multiply_fusion.1
  115.6 4.3 %fusion.37 = bf16[8,64,512]{2,1,0:T(8,128)(2,1)} fusion(bf16[2048,8,64]{0,2,1:T(8,128)(2,1)} %bitcast.146, bf16[512,2048]{1,0:T(8,128)(2,1)} %all-gather.2.cloned.1.call-done), kind=kOutput, calls=%fused_computation.39 | convolution fusion | flops 1074003968 | bytes 4718592 | tf_op jit(solution)/shard_map/td,dhe->hte/dot_general | solution.py:102
  119.9 2.4 copy.101
  122.2 2.8 %copy.96 = bf16[8,512,64]{2,0,1:T(8,128)(2,1)} copy(bf16[8,512,64]{1,2,0:T(8,128)(2,1)} %bitcast.142) | data formatting | bytes 1048576 | tf_op jit(solution)/shard_map/convert_element_type | solution.py:104
  125.1 8.7 %collective-permute-done.3 = bf16[2,8,512,64]{2,3,1,0:T(8,128)(2,1)} collective-permute-done((bf16[2,8,512,64]{2,3,1,0:T(8,128)(2,1)}, bf16[2,8,512,64]{2,3,1,0:T(8,128)(2,1)}, u32[]{:S(2)}, u32[]{:S(2)}) %collective-permute-start.3) | collective-permute-done | bytes 1048608 | tf_op jit(solution)/shard_map/ppermute | solution.py:22
  133.8 1.3 constant_dynamic-update-slice_fusion.4
  135.1 1.3 constant_dynamic-update-slice_fusion.3
  136.4 1.3 constant_dynamic-update-slice_fusion.2
  137.9 2.3 copy-done.1
  140.2 2.8 %fusion.93 = (bf16[1,8,2560,64]{2,3,1,0:T(8,128)(2,1)}, bf16[1,8,2560,64]{2,3,1,0:T(8,128)(2,1)}) fusion(bf16[2,8,2560,64]{2,3,1,0:T(8,128)(2,1)S(1)} %constant_dynamic-update-slice_fusion), kind=kLoop, calls=%fused_computation.116 | loop fusion | bytes 10485760 | tf_op jit(solution)/shard_map/slice | solution.py:66
  143.0 12.2 %copy.97 = bf16[2,8,2560,64]{3,1,2,0:T(8,128)(2,1)} copy(bf16[2,8,2560,64]{2,3,1,0:T(8,128)(2,1)} %copy-done.1) | data formatting | bytes 10485760 | tf_op jit(solution)/shard_map/concatenate | solution.py:122
  155.2 6.0 %copy.102 = bf16[1,8,2560,64]{3,2,1,0:T(8,128)(2,1)} copy(bf16[1,8,2560,64]{2,3,1,0:T(8,128)(2,1)} %get-tuple-element.15) | data formatting | bytes 5242880 | tf_op jit(solution)/shard_map/slice | solution.py:44
  161.1 6.3 %fusion.12 = (f32[8,16,32]{2,1,0:T(8,128)S(1)}, f32[8,16,32,160]{3,2,1,0:T(8,128)S(1)}) fusion(f32[8,32,160]{2,1,0:T(8,128)} %broadcast_multiply_fusion.2, pred[16,32,160]{2,1,0:T(8,128)(4,1)S(1)} %broadcast_and_fusion, bf16[8,160,16,64]{3,2,1,0:T(8,128)(2,1)} %bitcast.140, bf16[8,32,16,64]{3,2,1,0:T(8,128)(2,1)} %bitcast.149), kind=kOutput, calls=%fused_computation.19 | convolution fusion | flops 86503424 | bytes 6029312 | tf_op jit(solution)/shard_map/hbqre,hbkre->hrbqk/dot_general | solution.py:43
  167.4 2.0 copy-done.9
  169.4 1.7 fusion.9
  174.2 6.0 %copy.116 = bf16[1,8,2560,64]{3,2,1,0:T(8,128)(2,1)} copy(bf16[1,8,2560,64]{2,3,1,0:T(8,128)(2,1)} %get-tuple-element.14) | data formatting | bytes 5242880 | tf_op jit(solution)/shard_map/slice | solution.py:66
  180.2 5.4 %bitcast_divide_fusion = f32[8,1,32,16,64]{4,2,3,0,1:T(8,128)S(1)} fusion(f32[8,32,16]{1,2,0:T(8,128)} %bitcast.151, bf16[8,160,16,64]{3,2,1,0:T(8,128)(2,1)} %bitcast.139, f32[8,16,32,160]{3,2,1,0:T(8,128)} %copy-done.9, f32[8,16,32]{2,1,0:T(8,128)} %copy-done.21, f32[8,32,160]{2,1,0:T(8,128)} %broadcast_multiply_fusion.2, ...), kind=kOutput, calls=%fused_computation.21 | convolution fusion | flops 87425024 | bytes 6569984 | tf_op jit(solution)/shard_map/hrbqk,hbkre->hbqre/dot_general | solution.py:63
  185.6 2.5 copy.118
  188.1 3.1 %copy.119 = f32[8,512,64]{1,2,0:T(8,128)} copy(f32[8,512,64]{2,1,0:T(8,128)} %bitcast.138) | data formatting | bytes 2097152 | tf_op jit(solution)/shard_map/reshape | solution.py:71
  191.2 4.9 %fusion.92 = (bf16[1,8,256,4,64]{4,1,3,2,0:T(8,128)(2,1)}, bf16[1,8,256,4,64]{4,1,3,2,0:T(8,128)(2,1)}) fusion(bf16[2,8,640,4,64]{4,1,3,2,0:T(8,128)(2,1)} %bitcast.136), kind=kLoop, calls=%fused_computation.115 | loop fusion | bytes 4194304 | tf_op jit(solution)/shard_map/slice | solution.py:66
  196.1 3.6 %copy.120 = bf16[1,8,256,4,64]{2,4,3,1,0:T(8,128)(2,1)} copy(bf16[1,8,256,4,64]{4,1,3,2,0:T(8,128)(2,1)} %get-tuple-element.9) | data formatting | bytes 2097152
  199.7 3.6 %copy.121 = bf16[1,8,256,4,64]{2,4,3,1,0:T(8,128)(2,1)} copy(bf16[1,8,256,4,64]{4,1,3,2,0:T(8,128)(2,1)} %get-tuple-element.8) | data formatting | bytes 2097152
  203.3 1.7 slice_bitcast_fusion.5
  206.4 1.4 fusion.10
  208.0 1.6 fusion.11
  209.5 3.6 %fusion.5 = (f32[8,4,128]{2,1,0:T(4,128)S(1)}, f32[8,4,128]{2,1,0:T(4,128)S(1)}) fusion(f32[8,4,128,256]{3,2,1,0:T(8,128)S(1)} %get-tuple-element.31, f32[8,4,128]{2,1,0:T(4,128)S(1)} %get-tuple-element.30, f32[8,128,256]{2,1,0:T(8,128)S(1)} %copy-done.3, pred[4,128,256]{2,1,0:T(8,128)(4,1)S(1)} %get-tuple-element.18, ...), kind=kLoop, calls=%fused_computation.11 | loop fusion | flops 10477568 | bytes 10813440 | tf_op jit(solution)/shard_map/reduce_sum | solution.py:62
  213.2 2.6 %fusion.60 = f32[8,1,128,4,64]{2,4,3,0,1:T(8,128)} fusion(f32[8,4,128,256]{3,2,1,0:T(8,128)S(1)} %get-tuple-element.29, f32[8,4,128]{2,1,0:T(4,128)S(1)} %get-tuple-element.28, f32[8,128,256]{2,1,0:T(8,128)S(1)} %get-tuple-element.23, pred[4,128,256]{2,1,0:T(8,128)(4,1)S(1)} %get-tuple-element.19, bf16[1,8,256,4,64]{2,4,3,1,0:T(8,128)(2,1)S(1)} %copy-done.15, ...), kind=kOutput, calls=%fused_computation.57 | convolution fusion | flops 139722752 | bytes 7503872 | tf_op jit(solution)/shard_map/hrbqk,hbkre->hbqre/dot_general | solution.py:63
  215.8 4.2 %copy.114 = f32[8,1,128,4,64]{4,0,3,2,1:T(8,128)} copy(f32[8,1,128,4,64]{2,4,3,0,1:T(8,128)} %fusion.60) | data formatting | bytes 2097152 | tf_op jit(solution)/shard_map/div | solution.py:69
  220.0 3.2 %copy.115 = f32[8,512,64]{1,2,0:T(8,128)} copy(f32[8,512,64]{2,0,1:T(8,128)} %bitcast.137) | data formatting | bytes 2097152 | tf_op jit(solution)/shard_map/reshape | solution.py:71
  223.2 3.9 %divide_bitcast_fusion = f32[8,4,128,1,64]{2,4,1,0,3:T(8,128)S(1)} fusion(f32[8,4,128,256]{3,2,1,0:T(8,128)} %copy-done.2, f32[8,4,128]{2,1,0:T(4,128)S(1)} %get-tuple-element.30, f32[8,128,256]{2,1,0:T(8,128)S(1)} %copy-done.4, pred[4,128,256]{2,1,0:T(8,128)(4,1)S(1)} %get-tuple-element.18, bf16[8,4,256,64]{2,3,0,1:T(8,128)(2,1)} %get-tuple-element.16, ...), kind=kOutput, calls=%fused_computation.56 | convolution fusion | flops 139722752 | bytes 7503872 | tf_op jit(solution)/shard_map/hrbqk,hbkre->hbqre/dot_general | solution.py:63
  227.2 1.6 copy.111
  228.8 2.6 %reshape.591 = f32[8,512,64]{1,2,0:T(8,128)} reshape(f32[8,4,128,1,64]{2,1,4,0,3:T(4,128)} %copy.111) | data formatting | bytes 2097152 | tf_op jit(solution)/shard_map/reshape | solution.py:71
  232.0 2.0 add_convert_fusion
  233.9 2.6 %convolution_convert_fusion = bf16[512,2048]{1,0:T(8,128)(2,1)} fusion(bf16[512,512]{0,1:T(8,128)(2,1)S(1)} %bitcast.150, bf16[512,2048]{1,0:T(8,128)(2,1)S(1)} %copy-done), kind=kOutput, calls=%fused_computation.16 | convolution fusion | flops 1074790400 | bytes 4718592 | tf_op jit(solution)/shard_map/dot_general | solution.py:128
  236.6 13.8 %reduce-scatter.2.cloned.1.call-done = bf16[256,2048]{1,0:T(8,128)(2,1)} async-done(((bf16[512,2048]{1,0:T(8,128)(2,1)}), bf16[256,2048]{1,0:T(8,128)(2,1)}) %reduce-scatter.2.cloned.1.call-update) | async-done | bytes 1048592 | tf_op jit(solution)/shard_map/reduce_scatter | solution.py:127
  (89 shorter events, 8.6 us)
Async XLA Ops:
  7.2 226.8 %copy-start = (bf16[512,2048]{1,0:T(8,128)(2,1)S(1)}, bf16[512,2048]{1,0:T(8,128)(2,1)}, u32[]{:S(2)}) copy-start(bf16[512,2048]{1,0:T(8,128)(2,1)} %param.9) | copy-start | bytes 6291460
  7.2 15.7 %all-gather.2.cloned.1.call-start = ((), (), s32[]{:S(2)}) async-start(), calls=%async_computation.1 | async-start | bytes 3145728 | tf_op jit(solution)/shard_map/all_gather | solution.py:99
  7.9 242.4 %reduce-scatter.2.cloned.1.call-start = ((), (), s32[]{:S(2)}) async-start(), calls=%async_computation.2 | async-start | bytes 3145728 | tf_op jit(solution)/shard_map/reduce_scatter | solution.py:127
  22.9 3.7 %copy-start.10 = (bf16[2048,512]{0,1:T(8,128)(2,1)S(1)}, bf16[2048,512]{0,1:T(8,128)(2,1)}, u32[]{:S(2)}) copy-start(bf16[2048,512]{0,1:T(8,128)(2,1)} %copy.92) | copy-start | bytes 6291460
  22.9 3.7 %copy-start.25 = (bf16[512,2048]{1,0:T(8,128)(2,1)S(1)}, bf16[512,2048]{1,0:T(8,128)(2,1)}, u32[]{:S(2)}) copy-start(bf16[512,2048]{1,0:T(8,128)(2,1)} %all-gather.2.cloned.1.call-done) | copy-start | bytes 6291460
  26.5 2.5 copy-start.11
  27.8 4.9 %copy-start.13 = (bf16[1,8,512,64]{2,3,1,0:T(8,128)(2,1)}, bf16[1,8,512,64]{2,3,1,0:T(8,128)(2,1)S(1)}, u32[]{:S(2)}) copy-start(bf16[1,8,512,64]{2,3,1,0:T(8,128)(2,1)S(1)} %fusion.49) | copy-start | bytes 1572868
  29.0 26.8 %collective-permute-start = (bf16[2,8,512,64]{2,3,1,0:T(8,128)(2,1)}, bf16[2,8,512,64]{2,3,1,0:T(8,128)(2,1)S(1)}, u32[]{:S(2)}, u32[]{:S(2)}) collective-permute-start(bf16[2,8,512,64]{2,3,1,0:T(8,128)(2,1)} %pad_maximum_fusion.1), channel_id=1, source_target_pairs={{0,2},{2,4},{4,6},{6,8},{8,10},{10,12},{12,14},{1,3},{3,5},{5,7},{... | collective-permute-start | bytes 3145736 | tf_op jit(solution)/shard_map/ppermute | solution.py:22
  55.8 58.5 %copy-start.17 = (bf16[2,8,512,64]{2,3,1,0:T(8,128)(2,1)}, bf16[2,8,512,64]{2,3,1,0:T(8,128)(2,1)S(1)}, u32[]{:S(2)}) copy-start(bf16[2,8,512,64]{2,3,1,0:T(8,128)(2,1)S(1)} %collective-permute-done) | copy-start | bytes 3145732
  55.8 26.3 %collective-permute-start.1 = (bf16[2,8,512,64]{2,3,1,0:T(8,128)(2,1)S(1)}, bf16[2,8,512,64]{2,3,1,0:T(8,128)(2,1)}, u32[]{:S(2)}, u32[]{:S(2)}) collective-permute-start(bf16[2,8,512,64]{2,3,1,0:T(8,128)(2,1)S(1)} %collective-permute-done), channel_id=1, source_target_pairs={{0,2},{2,4},{4,6},{6,8},{8,10},{10,12},{12,14},{1,3},{3,5},{5,7},{... | collective-permute-start | bytes 3145736 | tf_op jit(solution)/shard_map/ppermute | solution.py:22
  82.1 26.0 %collective-permute-start.2 = (bf16[2,8,512,64]{2,3,1,0:T(8,128)(2,1)}, bf16[2,8,512,64]{2,3,1,0:T(8,128)(2,1)}, u32[]{:S(2)}, u32[]{:S(2)}) collective-permute-start(bf16[2,8,512,64]{2,3,1,0:T(8,128)(2,1)} %collective-permute-done.1), channel_id=1, source_target_pairs={{0,2},{2,4},{4,6},{6,8},{8,10},{10,12},{12,14},{1,3},{3,5},{5,7},{... | collective-permute-start | bytes 3145736 | tf_op jit(solution)/shard_map/ppermute | solution.py:22
  91.8 75.6 %copy-start.19 = (pred[16,32,160]{2,1,0:T(8,128)(4,1)}, pred[16,32,160]{2,1,0:T(8,128)(4,1)S(1)}, u32[]{:S(2)}) copy-start(pred[16,32,160]{2,1,0:T(8,128)(4,1)S(1)} %broadcast_and_fusion) | copy-start | bytes 245764
  108.0 25.7 %collective-permute-start.3 = (bf16[2,8,512,64]{2,3,1,0:T(8,128)(2,1)}, bf16[2,8,512,64]{2,3,1,0:T(8,128)(2,1)}, u32[]{:S(2)}, u32[]{:S(2)}) collective-permute-start(bf16[2,8,512,64]{2,3,1,0:T(8,128)(2,1)} %collective-permute-done.2), channel_id=1, source_target_pairs={{0,2},{2,4},{4,6},{6,8},{8,10},{10,12},{12,14},{1,3},{3,5},{5,7},{... | collective-permute-start | bytes 3145736 | tf_op jit(solution)/shard_map/ppermute | solution.py:22
  125.0 12.6 %copy-start.18 = (bf16[2,8,512,64]{2,3,1,0:T(8,128)(2,1)S(1)}, bf16[2,8,512,64]{2,3,1,0:T(8,128)(2,1)}, u32[]{:S(2)}) copy-start(bf16[2,8,512,64]{2,3,1,0:T(8,128)(2,1)} %copy-done.17) | copy-start | bytes 3145732
  125.0 12.7 %copy-start.12 = (bf16[1,8,512,64]{2,3,1,0:T(8,128)(2,1)S(1)}, bf16[1,8,512,64]{2,3,1,0:T(8,128)(2,1)}, u32[]{:S(2)}) copy-start(bf16[1,8,512,64]{2,3,1,0:T(8,128)(2,1)} %copy-done.11) | copy-start | bytes 1572868
  125.1 12.7 %copy-start.14 = (bf16[1,8,512,64]{2,3,1,0:T(8,128)(2,1)S(1)}, bf16[1,8,512,64]{2,3,1,0:T(8,128)(2,1)}, u32[]{:S(2)}) copy-start(bf16[1,8,512,64]{2,3,1,0:T(8,128)(2,1)} %copy-done.13) | copy-start | bytes 1572868
  137.8 2.3 copy-start.1
  161.1 8.3 %copy-start.16 = (f32[8,32,160]{2,1,0:T(8,128)S(1)}, f32[8,32,160]{2,1,0:T(8,128)}, u32[]{:S(2)}) copy-start(f32[8,32,160]{2,1,0:T(8,128)} %broadcast_multiply_fusion.2) | copy-start | bytes 491524
  167.4 2.0 copy-start.9
  167.4 3.7 %copy-start.21 = (f32[8,16,32]{2,1,0:T(8,128)}, f32[8,16,32]{2,1,0:T(8,128)S(1)}, u32[]{:S(2)}) copy-start(f32[8,16,32]{2,1,0:T(8,128)S(1)} %get-tuple-element.26) | copy-start | bytes 49156
  171.1 0.6 copy-start.22
  174.2 6.0 %copy-start.20 = (pred[16,32,160]{2,1,0:T(8,128)(4,1)S(1)}, pred[16,32,160]{2,1,0:T(8,128)(4,1)}, u32[]{:S(2)}) copy-start(pred[16,32,160]{2,1,0:T(8,128)(4,1)} %copy-done.19) | copy-start | bytes 245764
  205.0 1.4 copy-start.3
  205.0 1.4 copy-start.5
  206.4 1.4 copy-start.7
  206.4 1.5 copy-start.8
  207.8 5.3 %copy-start.2 = (f32[8,4,128,256]{3,2,1,0:T(8,128)}, f32[8,4,128,256]{3,2,1,0:T(8,128)S(1)}, u32[]{:S(2)}) copy-start(f32[8,4,128,256]{3,2,1,0:T(8,128)S(1)} %get-tuple-element.31) | copy-start | bytes 12582916
  209.5 3.7 %copy-start.15 = (bf16[1,8,256,4,64]{2,4,3,1,0:T(8,128)(2,1)S(1)}, bf16[1,8,256,4,64]{2,4,3,1,0:T(8,128)(2,1)}, u32[]{:S(2)}) copy-start(bf16[1,8,256,4,64]{2,4,3,1,0:T(8,128)(2,1)} %copy.121) | copy-start | bytes 3145732
  215.8 7.4 %copy-start.4 = (f32[8,128,256]{2,1,0:T(8,128)S(1)}, f32[8,128,256]{2,1,0:T(8,128)}, u32[]{:S(2)}) copy-start(f32[8,128,256]{2,1,0:T(8,128)} %get-tuple-element.22) | copy-start | bytes 3145732
  227.1 4.7 %copy-start.23 = (f32[1,8,512]{2,1,0:T(8,128)S(1)}, f32[1,8,512]{2,1,0:T(8,128)}, u32[]{:S(2)}) copy-start(f32[1,8,512]{2,1,0:T(8,128)} %stack_reshape.12) | copy-start | bytes 49156
  227.2 4.8 %copy-start.6 = (f32[8,512,64]{1,2,0:T(8,128)S(1)}, f32[8,512,64]{1,2,0:T(8,128)}, u32[]{:S(2)}) copy-start(f32[8,512,64]{1,2,0:T(8,128)} %copy.119) | copy-start | bytes 3145732
  231.9 4.6 %copy-start.24 = (f32[8,512]{1,0:T(8,128)}, f32[8,512]{1,0:T(8,128)S(1)}, u32[]{:S(2)}) copy-start(f32[8,512]{1,0:T(8,128)S(1)} %get-tuple-element.7) | copy-start | bytes 49156
Sparse Core Ops, SparseCore 0:
  9.5 13.2 all-gather.1
  236.7 13.5 reduce-scatter.1
where the time goes:
time: 259 us; the launch traced here: 257 us
  waiting for transfers between devices  89.4 us (35%)
  local copies, waits for them, and re-layouts  87.4 us (34%)
  matrix products  32.9 us (13%)
  starting transfers between devices  20.7 us (8%)
  between operations  14.5 us (6%)
  other arithmetic  12.2 us (5%)
    ppermute x4, waiting for transfers between devices, shifted(): lax.ppermute(value, axis, [(source, source + steps) for source in range(l...  68 us
    unnamed x61, local copies, waits for them, and re-layouts  28.1 us
    ppermute x4, starting transfers between devices, shifted(): lax.ppermute(value, axis, [(source, source + steps) for source in range(l...  20.6 us
    reduce_scatter x1, waiting for transfers between devices, body(): lax.psum_scatter(jnp.dot(hidden, w_out, preferred_element_type=jnp.float3...  13.8 us
    slice x3, local copies, waits for them, and re-layouts, dilated_attention(): spans[1]  13.7 us
    concatenate x1, local copies, waits for them, and re-layouts, body(): window_rows = jnp.concatenate(pieces, axis=2)  12.2 us
    dot_general x3, matrix products, dilated_attention(): jnp.einsum('hrbqk,hbkre->hbqre', weights.astype(jnp.bfloat16), spans[1],...  11.9 us
    dot_general x3, matrix products, dilated_attention(): jnp.einsum('hbqre,hbkre->hrbqk', grouped, spans[0], preferred_element_typ...  9.22 us
  transfers between devices with their start and end apart: 6, of which 6 were waited for; matrix products, arithmetic and copies ran while one was open for 9% of the time, Pallas kernels for 0%

commit v1 on v0

v1 whole, which is shorter than its diff:
```python
import functools
import math

import jax
import jax.numpy as jnp
from jax import lax
from jax.experimental import pallas as pl
from jax.experimental.pallas import tpu as pltpu
from jax.sharding import PartitionSpec as P

HEADS = 16
HEAD_DIM = 64
WINDOW_KEY_STEPS = 128
MIDDLE_DILATION = 4
FAR_DILATION = 16
REACH = 2048
ALIBI_EXP = 16.0

LOG2E = math.log2(math.e)
LN2 = math.log(2.0)
MASKED = -1e30
FLOOR = -1e25
F32 = jnp.float32
BF16 = jnp.bfloat16
ANY = pl.BlockSpec(memory_space=pl.ANY)
SMEM = pl.BlockSpec(memory_space=pltpu.SMEM)
VMEM = pl.BlockSpec(memory_space=pltpu.VMEM)
PARAMS = pltpu.CompilerParams(vmem_limit_bytes=56 * 1024 * 1024)

SUB = 16


def aligned(value, multiple):
    return value if isinstance(value, int) else pl.multiple_of(value, multiple)


def copy_all(pairs, sems):
    copies = [pltpu.make_async_copy(s, d, sems.at[n]) for n, (s, d) in enumerate(pairs)]
    for item in copies:
        item.start()
    return copies


def project_kernel(lanes, meta, x_own, x_other, w_q, w_k, w_v, kv_out, q_out, xs, ws, acc, sems):
    side, tp = meta[0], meta[1]
    rows = xs.shape[1]
    columns = pl.ds(aligned(side * lanes, lanes), lanes)
    copies = copy_all(
        [
            (x_own, xs.at[0]),
            (w_k.at[:, columns], ws.at[0]),
            (w_v.at[:, columns], ws.at[1]),
            (x_other, xs.at[1]),
            (w_q.at[:, columns], ws.at[2]),
        ],
        sems,
    )
    copies[0].wait()
    for which in range(3):
        copies[(1, 2, 4)[which]].wait()
        for half in range(2):
            if which == 0 and half == 1:
                copies[3].wait()
            result = jnp.dot(xs[half], ws[which], preferred_element_type=F32)
            for part in range(lanes // 128):
                acc[part] = result[:, part * 128 : (part + 1) * 128]
            place = (tp if half == 0 else 1 - tp) * rows
            for residue in range(FAR_DILATION):
                for part in range(lanes // 128):
                    chunk = acc[part, pl.ds(residue, SUB, stride=FAR_DILATION), :].astype(BF16)
                    target = pl.ds(aligned(place + residue * SUB, SUB), SUB)
                    if which < 2:
                        start = which * lanes + part * 128
                        kv_out[target, start : start + 128] = chunk
                    else:
                        q_out[target, part * 128 : (part + 1) * 128] = chunk


def project(meta, x_own, x_other, w_q, w_k, w_v, lanes):
    rows, width = x_own.shape
    return pl.pallas_call(
        functools.partial(project_kernel, lanes),
        out_shape=[
            jax.ShapeDtypeStruct((2 * rows, 2 * lanes), BF16),
            jax.ShapeDtypeStruct((2 * rows, lanes), BF16),
        ],
        in_specs=[SMEM] + [ANY] * 5,
        out_specs=[VMEM, VMEM],
        scratch_shapes=[
            pltpu.VMEM((2, rows, width), BF16),
            pltpu.VMEM((3, width, lanes), BF16),
            pltpu.VMEM((lanes // 128, rows, 128), F32),
            pltpu.SemaphoreType.DMA((5,)),
        ],
        compiler_params=PARAMS,
        cost_estimate=pl.CostEstimate(
            flops=2 * 2 * rows * width * 3 * lanes,
            bytes_accessed=2 * width * (2 * rows + 3 * lanes),
            transcendentals=0,
        ),
        name="project",
    )(meta, x_own, x_other, w_q, w_k, w_v)


def attend(queries, keys, values, bias):
    rows = queries.shape[0]
    low = lax.broadcasted_iota(jnp.int32, (rows, 128), 1) < HEAD_DIM
    zero = jnp.zeros_like(queries)
    stacked = jnp.concatenate([jnp.where(low, queries, zero), jnp.where(low, zero, queries)], axis=0)
    scores = lax.dot_general(
        stacked, keys, (((1,), (1,)), ((), ())), preferred_element_type=F32
    )
    scores = scores * (HEAD_DIM**-0.5 * LOG2E) + bias
    maxima = jnp.maximum(jnp.max(scores, axis=1, keepdims=True), FLOOR)
    weights = jnp.exp2(scores - maxima)
    totals = jnp.sum(weights, axis=1, keepdims=True)
    summed = jnp.dot(weights.astype(BF16), values, preferred_element_type=F32)
    pick = lambda item: jnp.where(low, item[:rows], item[rows:])
    return pick(summed), pick(maxima), pick(totals)


def merge(first, second):
    o1, m1, l1 = first
    o2, m2, l2 = second
    top = jnp.maximum(m1, m2)
    a, b = jnp.exp2(m1 - top), jnp.exp2(m2 - top)
    return o1 * a + o2 * b, top, l1 * a + l2 * b


def near_distance(keys_before, keys_own):
    tile = FAR_DILATION * SUB
    token = lambda n: FAR_DILATION * (n % SUB) + n // SUB
    shape = (tile, (tile if keys_before else 0) + (tile if keys_own else 0))
    row = token(lax.broadcasted_iota(jnp.int32, shape, 0))
    col = lax.broadcasted_iota(jnp.int32, shape, 1)
    if keys_before:
        key = jnp.where(col < tile, token(col) - tile, token(col - tile))
    else:
        key = token(col)
    return row - key


def middle_distance(keys_before, keys_own, chunks):
    group = FAR_DILATION // MIDDLE_DILATION
    size = chunks * group * SUB
    step = lambda n: (n // (group * SUB)) * (group * SUB) + group * (n % SUB) + (n // SUB) % group
    shape = (size, (size if keys_before else 0) + (size if keys_own else 0))
    row = step(lax.broadcasted_iota(jnp.int32, shape, 0))
    col = lax.broadcasted_iota(jnp.int32, shape, 1)
    if keys_before:
        key = jnp.where(col < size, step(col) - size, step(col - size))
    else:
        key = step(col)
    return row - key


def bias_of(distance, slope, stride):
    allowed = (distance >= 0) & (distance <= WINDOW_KEY_STEPS)
    return jnp.where(allowed, distance.astype(F32) * (slope * (-float(stride))), MASKED)


def rows_of(ref, starts, lanes):
    return jnp.concatenate([ref[pl.ds(aligned(s, SUB), SUB), lanes] for s in starts], axis=0)


def middle_starts(block, residue, chunks):
    tile = FAR_DILATION * SUB
    group = FAR_DILATION // MIDDLE_DILATION
    return [
        (block * chunks + s) * tile + (residue + MIDDLE_DILATION * b) * SUB
        for s in range(chunks)
        for b in range(group)
    ]


def far_starts(residue, chunks):
    return [g * FAR_DILATION * SUB + residue * SUB for g in range(chunks)]


def fold_in(refs, starts, lanes, new):
    size = SUB
    for n, start in enumerate(starts):
        where = (pl.ds(aligned(start, SUB), size), lanes)
        old = tuple(ref[where] for ref in refs)
        piece = tuple(item[n * size : (n + 1) * size] for item in new)
        for ref, value in zip(refs, merge(old, piece)):
            ref[where] = value


def pair_lanes(pair, offset=0):
    return slice(offset + pair * 128, offset + (pair + 1) * 128)


def local_kernel(meta, slopes, q_mine, q_part, kv_mine, kv_part, o_ref, m_ref, l_ref, q, kv, near, mid, sems):
    y = meta[2]
    block, lanes = q_mine.shape
    pairs = lanes // 128
    tile = FAR_DILATION * SUB
    chunks = block // tile
    mine = pl.ds(aligned(y * block, block), block)
    part = pl.ds(aligned((1 - y) * block, block), block)
    copies = copy_all(
        [(q_mine, q.at[mine]), (q_part, q.at[part]), (kv_mine, kv.at[mine]), (kv_part, kv.at[part])],
        sems,
    )
    distance = near_distance(True, True)
    for head in range(2 * pairs):
        near[head] = bias_of(distance, slopes[head], 1)
    distance = middle_distance(True, True, chunks)
    for head in range(2 * pairs):
        mid[head] = bias_of(distance, slopes[head], MIDDLE_DILATION)
    for item in copies:
        item.wait()
    refs = (o_ref, m_ref, l_ref)
    step = 64
    per_tile = tile // step

    def near_step(tile_index, inner, before):
        start = aligned(tile_index * tile + inner * step, step)
        first = aligned((tile_index - 1) * tile if before else tile_index * tile, tile)
        count = 2 * tile if before else tile
        for pair in range(pairs):
            select = pl.ds(aligned(inner * step, step), step)
            columns = slice(0, 2 * tile) if before else slice(tile, 2 * tile)
            bias = jnp.concatenate(
                [near[2 * pair, select, columns], near[2 * pair + 1, select, columns]], axis=0
            )
            result = attend(
                q[pl.ds(start, step), pair_lanes(pair)],
                kv[pl.ds(first, count), pair_lanes(pair)],
                kv[pl.ds(first, count), pair_lanes(pair, lanes)],
                bias,
            )
            for ref, value in zip(refs, result):
                ref[pl.ds(start, step), pair_lanes(pair)] = value

    @pl.loop(0, per_tile)
    def _(n):
        near_step(0, n, False)

    @pl.loop(0, (2 * chunks - 1) * per_tile)
    def _(n):
        near_step(1 + n // per_tile, n % per_tile, True)

    size = mid.shape[1]

    @pl.loop(0, MIDDLE_DILATION)
    def _(residue):
        for index in range(2):
            starts = middle_starts(index, residue, chunks)
            key_starts = (middle_starts(0, residue, chunks) if index else []) + starts
            columns = slice(0, 2 * size) if index else slice(size, 2 * size)
            for pair in range(pairs):
                bias = jnp.concatenate([mid[2 * pair, :, columns], mid[2 * pair + 1, :, columns]], axis=0)
                result = attend(
                    rows_of(q, starts, pair_lanes(pair)),
                    rows_of(kv, key_starts, pair_lanes(pair)),
                    rows_of(kv, key_starts, pair_lanes(pair, lanes)),
                    bias,
                )
                fold_in(refs, starts, pair_lanes(pair), result)


def local_attention(meta, slopes, q_mine, q_part, kv_mine, kv_part):
    block, lanes = q_mine.shape
    tile = FAR_DILATION * SUB
    state = jax.ShapeDtypeStruct((2 * block, lanes), F32)
    heads = lanes // HEAD_DIM
    size = block // MIDDLE_DILATION
    return pl.pallas_call(
        local_kernel,
        out_shape=[state] * 3,
        in_specs=[SMEM, SMEM] + [ANY] * 4,
        out_specs=[VMEM] * 3,
        scratch_shapes=[
            pltpu.VMEM((2 * block, lanes), BF16),
            pltpu.VMEM((2 * block, 2 * lanes), BF16),
            pltpu.VMEM((heads, tile, 2 * tile), F32),
            pltpu.VMEM((heads, size, 2 * size), F32),
            pltpu.SemaphoreType.DMA((4,)),
        ],
        compiler_params=PARAMS,
        cost_estimate=pl.CostEstimate(flops=4 * 10**9, bytes_accessed=4 * 10**6, transcendentals=0),
        name="local",
    )(meta, slopes, q_mine, q_part, kv_mine, kv_part)


def before_kernel(
    meta, slopes, gate, q_mine, q_part, kv_mine, kv_part, kv_a, kv_b, o_in, m_in, l_in,
    o_ref, m_ref, l_ref, q, kv, past, near, mid, far, sems,
):
    y = meta[2]
    block, lanes = q_mine.shape
    pairs = lanes // 128
    tile = FAR_DILATION * SUB
    chunks = block // tile
    mine = pl.ds(aligned(y * block, block), block)
    part = pl.ds(aligned((1 - y) * block, block), block)
    copies = copy_all(
        [
            (q_mine, q.at[mine]), (q_part, q.at[part]), (kv_mine, kv.at[mine]), (kv_part, kv.at[part]),
            (kv_a, past.at[mine]), (kv_b, past.at[part]),
            (o_in, o_ref), (m_in, m_ref), (l_in, l_ref),
        ],
        sems,
    )
    closed = gate[0]
    size = mid.shape[1]
    row = lax.broadcasted_iota(jnp.int32, far.shape[1:], 0)
    col = lax.broadcasted_iota(jnp.int32, far.shape[1:], 1)
    half = far.shape[2] // 2
    steps = row - col + half
    for head in range(2 * pairs):
        far[head] = bias_of(steps, slopes[head], FAR_DILATION) + jnp.where(col < half, closed, 0.0)
        near[head] = bias_of(near_distance(True, False), slopes[head], 1) + closed
        mid[head] = bias_of(middle_distance(True, False, chunks), slopes[head], MIDDLE_DILATION) + closed
    for item in copies:
        item.wait()
    refs = (o_ref, m_ref, l_ref)

    @pl.loop(0, FAR_DILATION)
    def _(residue):
        starts = far_starts(residue, 2 * chunks)
        for pair in range(pairs):
            keys = [rows_of(ref, starts, pair_lanes(pair)) for ref in (past, kv)]
            values = [rows_of(ref, starts, pair_lanes(pair, lanes)) for ref in (past, kv)]
            result = attend(
                rows_of(q, starts, pair_lanes(pair)),
                jnp.concatenate(keys, axis=0),
                jnp.concatenate(values, axis=0),
                jnp.concatenate([far[2 * pair], far[2 * pair + 1]], axis=0),
            )
            fold_in(refs, starts, pair_lanes(pair), result)

    step = 64
    last = (2 * chunks - 1) * tile

    @pl.loop(0, tile // step)
    def _(n):
        select = pl.ds(aligned(n * step, step), step)
        for pair in range(pairs):
            result = attend(
                q[select, pair_lanes(pair)],
                past[last : last + tile, pair_lanes(pair)],
                past[last : last + tile, pair_lanes(pair, lanes)],
                jnp.concatenate([near[2 * pair, select], near[2 * pair + 1, select]], axis=0),
            )
            old = tuple(ref[select, pair_lanes(pair)] for ref in refs)
            for ref, value in zip(refs, merge(old, result)):
                ref[select, pair_lanes(pair)] = value

    @pl.loop(0, MIDDLE_DILATION)
    def _(residue):
        starts = middle_starts(0, residue, chunks)
        key_starts = middle_starts(1, residue, chunks)
        for pair in range(pairs):
            result = attend(
                rows_of(q, starts, pair_lanes(pair)),
                rows_of(past, key_starts, pair_lanes(pair)),
                rows_of(past, key_starts, pair_lanes(pair, lanes)),
                jnp.concatenate([mid[2 * pair], mid[2 * pair + 1]], axis=0),
            )
            fold_in(refs, starts, pair_lanes(pair), result)


def before_attention(meta, slopes, gate, q_mine, q_part, kv_mine, kv_part, kv_a, kv_b, state):
    block, lanes = q_mine.shape
    tile = FAR_DILATION * SUB
    shape = jax.ShapeDtypeStruct((2 * block, lanes), F32)
    heads = lanes // HEAD_DIM
    size = block // MIDDLE_DILATION
    reach = 2 * block // FAR_DILATION
    return pl.pallas_call(
        before_kernel,
        out_shape=[shape] * 3,
        in_specs=[SMEM, SMEM, SMEM] + [ANY] * 9,
        out_specs=[VMEM] * 3,
        scratch_shapes=[
            pltpu.VMEM((2 * block, lanes), BF16),
            pltpu.VMEM((2 * block, 2 * lanes), BF16),
            pltpu.VMEM((2 * block, 2 * lanes), BF16),
            pltpu.VMEM((heads, tile, tile), F32),
            pltpu.VMEM((heads, size, size), F32),
            pltpu.VMEM((heads, reach, 2 * reach), F32),
            pltpu.SemaphoreType.DMA((9,)),
        ],
        compiler_params=PARAMS,
        cost_estimate=pl.CostEstimate(flops=2 * 10**9, bytes_accessed=4 * 10**6, transcendentals=0),
        name="before",
    )(meta, slopes, gate, q_mine, q_part, kv_mine, kv_part, kv_a, kv_b, *state)


def selector(lanes, part):
    shape = (16, lanes)
    row = lax.broadcasted_iota(jnp.int32, shape, 0)
    lane = lax.broadcasted_iota(jnp.int32, shape, 1)
    heads = lanes // HEAD_DIM
    return jnp.where((row // heads == part) & (lane == (row % heads) * HEAD_DIM), 1.0, 0.0).astype(BF16)


def spreader(lanes):
    shape = (16, lanes)
    row = lax.broadcasted_iota(jnp.int32, shape, 0)
    lane = lax.broadcasted_iota(jnp.int32, shape, 1)
    heads = lanes // HEAD_DIM
    return jnp.where((row < 3 * heads) & (lane // HEAD_DIM == row % heads), 1.0, 0.0).astype(BF16)


def pack_sums(sums):
    lanes = sums.shape[1]
    total = jnp.zeros((16, sums.shape[0]), F32)
    for part in range(3):
        piece = sums.astype(BF16)
        sums = sums - piece.astype(F32)
        total = total + lax.dot_general(
            selector(lanes, part), piece, (((1,), (1,)), ((), ())), preferred_element_type=F32
        )
    return total.astype(BF16)


def unpack_sums(packed, lanes):
    return lax.dot_general(packed, spreader(lanes), (((0,), (0,)), ((), ())), preferred_element_type=F32)


def remote_kernel(meta, slopes, gate, q_a, q_b, kv_a, kv_b, own_ref, other_ref, q, kv, far, out, sums, sems):
    y = meta[2]
    block, lanes = q_a.shape
    pairs = lanes // 128
    tile = FAR_DILATION * SUB
    chunks = block // tile
    mine = pl.ds(aligned(y * block, block), block)
    part = pl.ds(aligned((1 - y) * block, block), block)
    copies = copy_all(
        [(q_a, q.at[mine]), (q_b, q.at[part]), (kv_a, kv.at[mine]), (kv_b, kv.at[part])], sems
    )
    closed = gate[0]
    row = lax.broadcasted_iota(jnp.int32, far.shape[1:], 0)
    col = lax.broadcasted_iota(jnp.int32, far.shape[1:], 1)
    steps = row - col + 2 * far.shape[2]
    for head in range(2 * pairs):
        far[head] = bias_of(steps, slopes[head], FAR_DILATION) + closed
    for item in copies:
        item.wait()

    @pl.loop(0, FAR_DILATION)
    def _(residue):
        starts = far_starts(residue, 2 * chunks)
        for pair in range(pairs):
            o, m, l = attend(
                rows_of(q, starts, pair_lanes(pair)),
                rows_of(kv, starts, pair_lanes(pair)),
                rows_of(kv, starts, pair_lanes(pair, lanes)),
                jnp.concatenate([far[2 * pair], far[2 * pair + 1]], axis=0),
            )
            some = l > 0.0
            safe = jnp.where(some, l, 1.0)
            o = o / safe
            s = jnp.where(some, m + jnp.log2(safe), FLOOR)
            for n, start in enumerate(starts):
                where = (pl.ds(aligned(start, SUB), SUB), pair_lanes(pair))
                out[where] = o[n * SUB : (n + 1) * SUB].astype(BF16)
                sums[where] = s[n * SUB : (n + 1) * SUB]

    for select, ref in ((mine, own_ref), (part, other_ref)):
        ref[:block] = out[select]
        packed = pack_sums(sums[select])
        for n in range(block // lanes):
            ref[block + 16 * n : block + 16 * (n + 1)] = packed[:, n * lanes : (n + 1) * lanes]


def remote_attention(meta, slopes, gate, q_a, q_b, kv_a, kv_b):
    block, lanes = q_a.shape
    heads = lanes // HEAD_DIM
    reach = 2 * block // FAR_DILATION
    shape = jax.ShapeDtypeStruct((block + 16 * (block // lanes), lanes), BF16)
    return pl.pallas_call(
        remote_kernel,
        out_shape=[shape] * 2,
        in_specs=[SMEM, SMEM, SMEM] + [ANY] * 4,
        out_specs=[VMEM] * 2,
        scratch_shapes=[
            pltpu.VMEM((2 * block, lanes), BF16),
            pltpu.VMEM((2 * block, 2 * lanes), BF16),
            pltpu.VMEM((heads, reach, reach), F32),
            pltpu.VMEM((2 * block, lanes), BF16),
            pltpu.VMEM((2 * block, lanes), F32),
            pltpu.SemaphoreType.DMA((4,)),
        ],
        compiler_params=PARAMS,
        cost_estimate=pl.CostEstimate(flops=10**9, bytes_accessed=2 * 10**6, transcendentals=0),
        name="remote",
    )(meta, slopes, gate, q_a, q_b, kv_a, kv_b)


def finish_kernel(meta, gate, o_in, m_in, l_in, far_in, stay_ref, go_ref, o_s, m_s, l_s, turned, sems):
    which, tp = meta[0], meta[1]
    block, lanes = o_s.shape
    tile = FAR_DILATION * SUB
    chunks = block // tile
    select = pl.ds(aligned(which * block, block), block)
    copies = copy_all(
        [(o_in.at[select], o_s), (m_in.at[select], m_s), (l_in.at[select], l_s)], sems
    )
    for item in copies:
        item.wait()
    per = lanes // tile
    for s in range(chunks):
        rows = slice(s * tile, (s + 1) * tile)
        packed = far_in[block + 16 * (s // per) : block + 16 * (s // per) + 16, (s % per) * tile : (s % per + 1) * tile]
        far_sums = unpack_sums(packed, lanes) + gate[0]
        o, m, l = merge(
            (o_s[rows], m_s[rows], l_s[rows]),
            (far_in[rows].astype(F32), far_sums, jnp.ones_like(far_sums)),
        )
        o_s[rows] = o / l
        m_s[rows] = (m + jnp.log2(l)) * LN2
    for item, ref in enumerate((o_s, m_s)):
        for s in range(chunks):
            for residue in range(FAR_DILATION):
                for part in range(lanes // 128):
                    turned[item, part, pl.ds(s * tile + residue, SUB, stride=FAR_DILATION), :] = ref[
                        s * tile + residue * SUB : s * tile + (residue + 1) * SUB, part * 128 : (part + 1) * 128
                    ]
    half = block // 2
    for part in range(lanes // 128):
        for ref, place in ((stay_ref, tp * half), (go_ref, (1 - tp) * half)):
            ref[:half, part * 128 : (part + 1) * 128] = turned[0, part, pl.ds(aligned(place, half), half), :].astype(BF16)
    sums = jnp.concatenate([turned[1, part] for part in range(lanes // 128)], axis=1)
    packed = pack_sums(sums)
    for n in range(block // lanes):
        stay_ref[half + 16 * n : half + 16 * (n + 1)] = packed[:, n * lanes : (n + 1) * lanes]


def finish(meta, gate, state, far):
    lanes = far.shape[1]
    block = state[0].shape[0] // 2
    half = block // 2
    return pl.pallas_call(
        finish_kernel,
        out_shape=[
            jax.ShapeDtypeStruct((half + 16 * (block // lanes), lanes), BF16),
            jax.ShapeDtypeStruct((half, lanes), BF16),
        ],
        in_specs=[SMEM, SMEM] + [ANY] * 3 + [VMEM],
        out_specs=[VMEM] * 2,
        scratch_shapes=[
            pltpu.VMEM((block, lanes), F32),
            pltpu.VMEM((block, lanes), F32),
            pltpu.VMEM((block, lanes), F32),
            pltpu.VMEM((2, lanes // 128, block, 128), F32),
            pltpu.SemaphoreType.DMA((3,)),
        ],
        compiler_params=PARAMS,
        cost_estimate=pl.CostEstimate(flops=5 * 10**8, bytes_accessed=2 * 10**6, transcendentals=0),
        name="finish",
    )(meta, gate, *state, far)


def output_kernel(meta, stay, same, tp_piece, cross, w_mine, w_other, out_ref, sums_ref):
    y = meta[2]
    half, width = out_ref.shape
    lanes = stay.shape[1]
    heads = lanes // HEAD_DIM
    block = 2 * half
    near_rows = pl.ds(aligned(y * lanes, lanes), lanes)
    far_rows = pl.ds(aligned((1 - y) * lanes, lanes), lanes)
    step = 512
    for start in range(0, width, step):
        columns = slice(start, start + step)
        first = jnp.dot(stay[:half], w_mine[near_rows, columns], preferred_element_type=F32)
        first += jnp.dot(same[:half], w_mine[far_rows, columns], preferred_element_type=F32)
        second = jnp.dot(tp_piece[...], w_other[near_rows, columns], preferred_element_type=F32)
        second += jnp.dot(cross[...], w_other[far_rows, columns], preferred_element_type=F32)
        out_ref[:, columns] = (first.astype(BF16).astype(F32) + second.astype(BF16).astype(F32)).astype(BF16)
    for ref, place in ((stay, y), (same, 1 - y)):
        for n in range(block // lanes):
            packed = ref[half + 16 * n : half + 16 * (n + 1)].astype(F32)
            total = packed[:heads] + packed[heads : 2 * heads] + packed[2 * heads : 3 * heads]
            sums_ref[place, :, n * lanes : (n + 1) * lanes] = total


def output(meta, stay, same, tp_piece, cross, w_mine, w_other):
    half, lanes = tp_piece.shape
    width = w_mine.shape[1]
    heads = lanes // HEAD_DIM
    return pl.pallas_call(
        output_kernel,
        out_shape=[
            jax.ShapeDtypeStruct((half, width), BF16),
            jax.ShapeDtypeStruct((2, heads, 2 * half), F32),
        ],
        in_specs=[SMEM] + [VMEM] * 6,
        out_specs=[VMEM] * 2,
        compiler_params=PARAMS,
        cost_estimate=pl.CostEstimate(
            flops=2 * half * width * 4 * lanes, bytes_accessed=6 * 10**6, transcendentals=0
        ),
        name="output",
    )(meta, stay, same, tp_piece, cross, w_mine, w_other)


def body(tokens, w_query, w_key, w_value, w_out):
    half, _ = tokens.shape
    block = 2 * half
    width = w_query.shape[1]
    lanes = width // 2
    count = lax.axis_size("sp")
    pair = 2
    assert lax.axis_size("tp") == 2 and count % pair == 0
    assert REACH == 2 * pair * block and half == FAR_DILATION * SUB and lanes % 128 == 0
    ahead = [(n, n + pair) for n in range(count - pair)]
    back = [(n + pair, n) for n in range(count - pair)]
    beside = [(n, n ^ 1) for n in range(count)]
    swap = [(0, 1), (1, 0)]
    crossed = [(2 * n + c, 2 * (n ^ 1) + 1 - c) for n in range(count) for c in range(2)]

    place = lax.axis_index("sp")
    y = place % 2
    z = place // 2
    tp = lax.axis_index("tp")
    meta_mine = jnp.stack([y, tp, y]).astype(jnp.int32)
    meta_other = jnp.stack([1 - y, tp, y]).astype(jnp.int32)
    heads = lanes // HEAD_DIM
    head_ids = tp * (2 * heads) + y * heads + jnp.arange(1, heads + 1, dtype=jnp.int32)
    slopes = jnp.exp2(-ALIBI_EXP * head_ids.astype(F32) / HEADS) * LOG2E
    gate = jnp.where(z > 0, 0.0, MASKED).astype(F32).reshape(1)

    x_other = lax.ppermute(tokens, "tp", swap)
    kv_t, q_t = project(meta_other, tokens, x_other, w_query, w_key, w_value, lanes)
    kv_m, q_m = project(meta_mine, tokens, x_other, w_query, w_key, w_value, lanes)
    kv_p = lax.ppermute(kv_t, "sp", beside)
    kv_a = lax.ppermute(kv_m, "sp", ahead)
    q_p = lax.ppermute(q_t, "sp", beside)
    q_a = lax.ppermute(q_m, "sp", back)
    kv_b = lax.ppermute(kv_p, "sp", ahead)
    q_b = lax.ppermute(q_p, "sp", back)
    w_other = lax.ppermute(w_out, "tp", swap)
    state = local_attention(meta_mine, slopes, q_m, q_p, kv_m, kv_p)
    far_own, far_other = remote_attention(meta_mine, slopes, gate, q_a, q_b, kv_a, kv_b)
    far_p = lax.ppermute(far_other, "sp", ahead)
    far_m = lax.ppermute(far_own, "sp", ahead)
    state = before_attention(meta_mine, slopes, gate, q_m, q_p, kv_m, kv_p, kv_a, kv_b, state)
    same_go, cross_go = finish(meta_other, gate, state, far_p)
    same = lax.ppermute(same_go, "sp", beside)
    cross = lax.ppermute(cross_go, ("sp", "tp"), crossed)
    stay, tp_go = finish(meta_mine, gate, state, far_m)
    tp_piece = lax.ppermute(tp_go, "tp", swap)
    mixed, sums = output(meta_mine, stay, same, tp_piece, cross, w_out, w_other)
    return mixed, sums.reshape(2 * heads, block)


def solution(mesh):
    in_specs = (
        P(("grp", "sp", "tp"), None),
        P(None, "tp"),
        P(None, "tp"),
        P(None, "tp"),
        P("tp", None),
    )
    out_specs = (P(("grp", "sp", "tp"), None), P("tp", ("grp", "sp")))
    return jax.shard_map(body, mesh=mesh, in_specs=in_specs, out_specs=out_specs, check_vma=False)
```

time: 259 us -> 126 us (0.49)
  local copies, waits for them, and re-layouts: 87.4 us -> 4.42 us
  Pallas kernels: 0 us -> 75.5 us
  waiting for transfers between devices: 89.4 us -> 17.3 us
  matrix products: 32.9 us -> 0 us
  between operations: 14.5 us -> 0.82 us
  other arithmetic: 12.2 us -> 1.78 us
  starting transfers between devices: 20.7 us -> 25.2 us
    pallas_call x0 -> x8, Pallas kernels: none -> 75.5 us  [the longest x1 20 us: before_attention(): pl.pallas_call(before_kernel, out_shape=[shape] * 3, in_specs=[SMEM, SMEM...]
    ppermute x4 -> x13, waiting for transfers between devices: 68 us -> 17.3 us  [the longest x1 8.19 us: body(): q_a = lax.ppermute(q_m, 'sp', back)]
    dot_general x10 -> x0, matrix products: 32.9 us -> none  [the longest x3 11.9 us: dilated_attention(): jnp.einsum('hrbqk,hbkre->hbqre', weights.astype(jnp.bfloat16), spans[1],...]
    unnamed x61 -> x20, local copies, waits for them, and re-layouts: 28.1 us -> 3.09 us
    slice x4 -> x0, local copies, waits for them, and re-layouts: 19.6 us -> none  [the longest x3 13.7 us: dilated_attention(): spans[1]]
    reduce_scatter x1 -> x0, waiting for transfers between devices: 13.8 us -> none  [body(): lax.psum_scatter(jnp.dot(hidden, w_out, preferred_element_type=jnp.float3...]
    concatenate x1 -> x0, local copies, waits for them, and re-layouts: 12.2 us -> none  [body(): window_rows = jnp.concatenate(pieces, axis=2)]
    div x3 -> x0, local copies, waits for them, and re-layouts: 8.32 us -> none  [dilated_attention(): outputs = summed / totals.transpose(0, 2, 3, 1, 4)]
  transfers between devices with their start and end apart: 6 -> 13, of which waited for: 6 -> 7; matrix products, arithmetic and copies ran while one was open for 9% -> 1% of each run, Pallas kernels for 0% -> 57%
where the time goes in v1:
time: 126 us; the launch traced here: 125 us
  Pallas kernels  75.5 us (60%)
  starting transfers between devices  25.2 us (20%)
  waiting for transfers between devices  17.3 us (14%)
  local copies, waits for them, and re-layouts  4.42 us (4%)
  other arithmetic  1.78 us (1%)
    pallas_call x1, Pallas kernels, before_attention(): pl.pallas_call(before_kernel, out_shape=[shape] * 3, in_specs=[SMEM, SMEM...  20 us
    pallas_call x1, Pallas kernels, local_attention(): pl.pallas_call(local_kernel, out_shape=[state] * 3, in_specs=[SMEM, SMEM]...  17.6 us
    pallas_call x2, Pallas kernels, project(): pl.pallas_call(functools.partial(project_kernel, lanes), out_shape=[jax.S...  12.6 us
    pallas_call x1, Pallas kernels, remote_attention(): pl.pallas_call(remote_kernel, out_shape=[shape] * 2, in_specs=[SMEM, SMEM...  12.5 us
    ppermute x1, waiting for transfers between devices, body(): q_a = lax.ppermute(q_m, 'sp', back)  8.19 us
    pallas_call x2, Pallas kernels, finish(): pl.pallas_call(finish_kernel, out_shape=[jax.ShapeDtypeStruct((half + 16...  8.07 us
    pallas_call x1, Pallas kernels, output(): pl.pallas_call(output_kernel, out_shape=[jax.ShapeDtypeStruct((half, widt...  4.81 us
    ppermute x1, starting transfers between devices, body(): kv_b = lax.ppermute(kv_p, 'sp', ahead)  4.8 us
  transfers between devices with their start and end apart: 13, of which 7 were waited for; matrix products, arithmetic and copies ran while one was open for 1% of the time, Pallas kernels for 57%

profile of v1, /device:TPU:0, one launch (start us, length us, event | category | flops | bytes accessed | tf_op | source)
XLA Modules:
  0.0 125.1 jit_solution(15283549632578143220)
XLA Ops:
  0.6 0.6 collective-permute-start
  1.2 0.1 collective-permute-start.12
  1.3 0.6 add_add_fusion.1.meta
  1.9 1.8 %collective-permute-done.x_other = bf16[256,2048]{1,0:T(8,128)(2,1)S(1)} collective-permute-done((bf16[256,2048]{1,0:T(8,128)(2,1)}, bf16[256,2048]{1,0:T(8,128)(2,1)S(1)}, u32[]{:S(2)}, u32[]{:S(2)}) %collective-permute-start) | collective-permute-done | bytes 1048608 | tf_op jit(solution)/shard_map/ppermute | solution.py:628
  3.7 1.0 copy-done
  4.7 6.3 %project.3 = (bf16[512,512]{1,0:T(8,128)(2,1)}, bf16[512,256]{1,0:T(8,128)(2,1)}) custom-call(s32[3]{0:T(128)} %add_add_fusion.1.meta, bf16[256,2048]{1,0:T(8,128)(2,1)} %x_own.3, bf16[256,2048]{1,0:T(8,128)(2,1)} %copy-done, bf16[2048,512]{1,0:T(8,128)(2,1)} %w_q.3, bf16[2048,512]{1,0:T(8,128)(2,1)} %w_k.3, bf16[2048,512]{1,0:T(8,128)(2,1)} %w_v.3), custom_call_target="tpu_custom_call" | custom-call | flops 1610612736 | bytes 5242880 | tf_op jit(solution)/shard_map/project/pallas_call | solution.py:81
  10.9 2.9 %collective-permute-start.2 = (bf16[512,512]{1,0:T(8,128)(2,1)}, bf16[512,512]{1,0:T(8,128)(2,1)S(1)}, u32[]{:S(2)}, u32[]{:S(2)}) collective-permute-start(bf16[512,512]{1,0:T(8,128)(2,1)} %get-tuple-element.23), channel_id=1, source_target_pairs={{0,2},{2,0},{4,6},{6,4},{8,10},{10,8},{12,14},{14,12},{1,3},{3,1},... | collective-permute-start | bytes 1572872 | tf_op jit(solution)/shard_map/ppermute | solution.py:631
  13.9 0.6 add_add_fusion.meta
  14.5 0.0 collective-permute-start.1
  14.5 6.3 %project.2 = (bf16[512,512]{1,0:T(8,128)(2,1)}, bf16[512,256]{1,0:T(8,128)(2,1)}) custom-call(s32[3]{0:T(128)} %add_add_fusion.meta, bf16[256,2048]{1,0:T(8,128)(2,1)} %x_own.3, bf16[256,2048]{1,0:T(8,128)(2,1)} %copy-done, bf16[2048,512]{1,0:T(8,128)(2,1)} %w_q.3, bf16[2048,512]{1,0:T(8,128)(2,1)} %w_k.3, bf16[2048,512]{1,0:T(8,128)(2,1)} %w_v.3), custom_call_target="tpu_custom_call" | custom-call | flops 1610612736 | bytes 5242880 | tf_op jit(solution)/shard_map/project/pallas_call | solution.py:81
  20.8 4.0 %collective-permute-start.3 = (bf16[512,512]{1,0:T(8,128)(2,1)}, bf16[512,512]{1,0:T(8,128)(2,1)S(1)}, u32[]{:S(2)}, u32[]{:S(2)}) collective-permute-start(bf16[512,512]{1,0:T(8,128)(2,1)} %get-tuple-element.22.kv_mine), channel_id=1, source_target_pairs={{0,4},{2,6},{4,8},{6,10},{8,12},{10,14},{1,5},{3,7},{5,9},{7,11},{... | collective-permute-start | bytes 1572872 | tf_op jit(solution)/shard_map/ppermute | solution.py:632
  24.8 2.0 %collective-permute-done.2.kv_part = bf16[512,512]{1,0:T(8,128)(2,1)S(1)} collective-permute-done((bf16[512,512]{1,0:T(8,128)(2,1)}, bf16[512,512]{1,0:T(8,128)(2,1)S(1)}, u32[]{:S(2)}, u32[]{:S(2)}) %collective-permute-start.2) | collective-permute-done | bytes 524320 | tf_op jit(solution)/shard_map/ppermute | solution.py:631
  26.9 4.8 %collective-permute-start.4 = (bf16[512,512]{1,0:T(8,128)(2,1)S(1)}, bf16[512,512]{1,0:T(8,128)(2,1)}, u32[]{:S(2)}, u32[]{:S(2)}) collective-permute-start(bf16[512,512]{1,0:T(8,128)(2,1)S(1)} %collective-permute-done.2.kv_part), channel_id=1, source_target_pairs={{0,4},{2,6},{4,8},{6,10},{8,12},{10,14},{1,5},{3,7},{5,9},{7,11},{... | collective-permute-start | bytes 1572872 | tf_op jit(solution)/shard_map/ppermute | solution.py:635
  31.7 1.3 %collective-permute-start.5 = (bf16[512,256]{1,0:T(8,128)(2,1)}, bf16[512,256]{1,0:T(8,128)(2,1)}, u32[]{:S(2)}, u32[]{:S(2)}) collective-permute-start(bf16[512,256]{1,0:T(8,128)(2,1)} %get-tuple-element.20.q_mine), channel_id=1, source_target_pairs={{4,0},{6,2},{8,4},{10,6},{12,8},{14,10},{5,1},{7,3},{9,5},{11,7},{... | collective-permute-start | bytes 786440 | tf_op jit(solution)/shard_map/ppermute | solution.py:634
  32.9 0.0 collective-permute-done.1.q_part
  33.0 0.0 copy-start.9
  33.0 1.3 %collective-permute-start.6 = (bf16[512,256]{1,0:T(8,128)(2,1)S(1)}, bf16[512,256]{1,0:T(8,128)(2,1)}, u32[]{:S(2)}, u32[]{:S(2)}) collective-permute-start(bf16[512,256]{1,0:T(8,128)(2,1)S(1)} %collective-permute-done.1.q_part), channel_id=1, source_target_pairs={{4,0},{6,2},{8,4},{10,6},{12,8},{14,10},{5,1},{7,3},{9,5},{11,7},{... | collective-permute-start | bytes 786440 | tf_op jit(solution)/shard_map/ppermute | solution.py:636
  34.3 0.6 exponential_multiply_fusion.slopes
  34.8 8.2 %collective-permute-done.5.q_a = bf16[512,256]{1,0:T(8,128)(2,1)} collective-permute-done((bf16[512,256]{1,0:T(8,128)(2,1)}, bf16[512,256]{1,0:T(8,128)(2,1)}, u32[]{:S(2)}, u32[]{:S(2)}) %collective-permute-start.5) | collective-permute-done | bytes 262176 | tf_op jit(solution)/shard_map/ppermute | solution.py:634
  43.0 0.0 collective-permute-done.3.kv_a
  43.0 2.8 %collective-permute-done.6.q_b = bf16[512,256]{1,0:T(8,128)(2,1)} collective-permute-done((bf16[512,256]{1,0:T(8,128)(2,1)S(1)}, bf16[512,256]{1,0:T(8,128)(2,1)}, u32[]{:S(2)}, u32[]{:S(2)}) %collective-permute-start.6) | collective-permute-done | bytes 262176 | tf_op jit(solution)/shard_map/ppermute | solution.py:636
  45.8 1.3 %collective-permute-done.4.kv_b = bf16[512,512]{1,0:T(8,128)(2,1)} collective-permute-done((bf16[512,512]{1,0:T(8,128)(2,1)S(1)}, bf16[512,512]{1,0:T(8,128)(2,1)}, u32[]{:S(2)}, u32[]{:S(2)}) %collective-permute-start.4) | collective-permute-done | bytes 524320 | tf_op jit(solution)/shard_map/ppermute | solution.py:635
  47.2 0.0 copy-done.8
  47.2 12.5 %remote.1 = (bf16[544,256]{1,0:T(8,128)(2,1)}, bf16[544,256]{1,0:T(8,128)(2,1)}) custom-call(s32[3]{0:T(128)} %add_add_fusion.meta, f32[4]{0:T(128)} %exponential_multiply_fusion.slopes, f32[1]{0:T(128)} %bitcast.2.gate, bf16[512,256]{1,0:T(8,128)(2,1)} %collective-permute-done.5.q_a, bf16[512,256]{1,0:T(8,128)(2,1)} %collective-permute-done.6.q_b, ...), custom_call_target="tpu_custom_call" | custom-call | flops 1000000000 | bytes 2000000 | tf_op jit(solution)/shard_map/remote/pallas_call | solution.py:476
  59.7 4.5 %collective-permute-start.8 = (bf16[544,256]{1,0:T(8,128)(2,1)}, bf16[544,256]{1,0:T(8,128)(2,1)S(1)}, u32[]{:S(2)}, u32[]{:S(2)}) collective-permute-start(bf16[544,256]{1,0:T(8,128)(2,1)} %get-tuple-element.32), channel_id=1, source_target_pairs={{0,4},{2,6},{4,8},{6,10},{8,12},{10,14},{1,5},{3,7},{5,9},{7,11},{... | collective-permute-start | bytes 835592 | tf_op jit(solution)/shard_map/ppermute | solution.py:640
  64.2 3.5 %collective-permute-start.7 = (bf16[544,256]{1,0:T(8,128)(2,1)}, bf16[544,256]{1,0:T(8,128)(2,1)S(1)}, u32[]{:S(2)}, u32[]{:S(2)}) collective-permute-start(bf16[544,256]{1,0:T(8,128)(2,1)} %get-tuple-element.30), channel_id=1, source_target_pairs={{0,4},{2,6},{4,8},{6,10},{8,12},{10,14},{1,5},{3,7},{5,9},{7,11},{... | collective-permute-start | bytes 835592 | tf_op jit(solution)/shard_map/ppermute | solution.py:641
  67.7 17.6 %local.1 = (f32[1024,256]{1,0:T(8,128)}, f32[1024,256]{1,0:T(8,128)}, f32[1024,256]{1,0:T(8,128)}) custom-call(s32[3]{0:T(128)} %add_add_fusion.meta, f32[4]{0:T(128)} %exponential_multiply_fusion.slopes, bf16[512,256]{1,0:T(8,128)(2,1)} %get-tuple-element.20.q_mine, bf16[512,256]{1,0:T(8,128)(2,1)} %copy-done.9, ...), custom_call_target="tpu_custom_call" | custom-call | flops 4000000000 | bytes 4000000 | tf_op jit(solution)/shard_map/local/pallas_call | solution.py:270
  85.3 20.0 %before.1 = (f32[1024,256]{1,0:T(8,128)}, f32[1024,256]{1,0:T(8,128)}, f32[1024,256]{1,0:T(8,128)}) custom-call(s32[3]{0:T(128)} %add_add_fusion.meta, f32[4]{0:T(128)} %exponential_multiply_fusion.slopes, f32[1]{0:T(128)} %bitcast.2.gate, bf16[512,256]{1,0:T(8,128)(2,1)} %get-tuple-element.20.q_mine, bf16[512,256]{1,0:T(8,128)(2,1)} %copy-done.9, ...), custom_call_target="tpu_custom_call" | custom-call | flops 2000000000 | bytes 4000000 | tf_op jit(solution)/shard_map/before/pallas_call | solution.py:373
  105.3 0.0 collective-permute-done.8.far_in
  105.3 0.0 copy-start.3
  105.3 0.7 copy-done.3
  106.0 4.0 %finish.3 = (bf16[288,256]{1,0:T(8,128)(2,1)}, bf16[256,256]{1,0:T(8,128)(2,1)}) custom-call(s32[3]{0:T(128)} %add_add_fusion.1.meta, f32[1]{0:T(128)} %bitcast.2.gate, f32[1024,256]{1,0:T(8,128)} %get-tuple-element.27.o_in, f32[1024,256]{1,0:T(8,128)} %get-tuple-element.28.m_in, f32[1024,256]{1,0:T(8,128)} %get-tuple-element.29.l_in, bf16[544,256]{1,0:T(8,128)(2,1)} %copy-done.3), custom_call_target="tpu_custom_call" | custom-call | flops 500000000 | bytes 2000000 | tf_op jit(solution)/shard_map/finish/pallas_call | solution.py:538
  110.0 1.6 %collective-permute-start.9 = (bf16[288,256]{1,0:T(8,128)(2,1)}, bf16[288,256]{1,0:T(8,128)(2,1)S(1)}, u32[]{:S(2)}, u32[]{:S(2)}) collective-permute-start(bf16[288,256]{1,0:T(8,128)(2,1)} %get-tuple-element.33), channel_id=1, source_target_pairs={{0,2},{2,0},{4,6},{6,4},{8,10},{10,8},{12,14},{14,12},{1,3},{3,1},... | collective-permute-start | bytes 442376 | tf_op jit(solution)/shard_map/ppermute | solution.py:644
  111.6 0.0 collective-permute-start.11
  111.6 0.0 collective-permute-done.7.far_in
  111.6 0.7 copy-done.2
  112.3 4.0 %finish.2 = (bf16[288,256]{1,0:T(8,128)(2,1)}, bf16[256,256]{1,0:T(8,128)(2,1)}) custom-call(s32[3]{0:T(128)} %add_add_fusion.meta, f32[1]{0:T(128)} %bitcast.2.gate, f32[1024,256]{1,0:T(8,128)} %get-tuple-element.27.o_in, f32[1024,256]{1,0:T(8,128)} %get-tuple-element.28.m_in, f32[1024,256]{1,0:T(8,128)} %get-tuple-element.29.l_in, bf16[544,256]{1,0:T(8,128)(2,1)} %copy-done.2), custom_call_target="tpu_custom_call" | custom-call | flops 500000000 | bytes 2000000 | tf_op jit(solution)/shard_map/finish/pallas_call | solution.py:538
  116.4 0.7 collective-permute-start.10
  117.1 0.0 collective-permute-done.12.w_other
  117.1 0.6 collective-permute-done.11.cross
  117.6 0.6 collective-permute-done.10.tp_piece
  118.3 0.0 collective-permute-done.9.same
  118.3 0.2 copy-done.1
  118.4 0.0 copy-done.5
  118.4 0.5 copy-done.6
  118.9 0.1 copy-done.4
  119.0 4.8 %output.1 = (bf16[256,2048]{1,0:T(8,128)(2,1)}, f32[2,4,512]{2,1,0:T(4,128)}) custom-call(s32[3]{0:T(128)} %add_add_fusion.meta, bf16[288,256]{1,0:T(8,128)(2,1)} %get-tuple-element.31.stay, bf16[288,256]{1,0:T(8,128)(2,1)} %copy-done.4, bf16[256,256]{1,0:T(8,128)(2,1)} %copy-done.6, bf16[256,256]{1,0:T(8,128)(2,1)} %copy-done.5, bf16[512,2048]{1,0:T(8,128)(2,1)} %w_mine.1, ...), custom_call_target="tpu_custom_call" | custom-call | flops 1073741824 | bytes 6000000 | tf_op jit(solution)/shard_map/output/pallas_call | solution.py:586
  123.8 1.3 %reshape.11 = f32[8,512]{1,0:T(8,128)} reshape(f32[2,4,512]{2,1,0:T(4,128)} %get-tuple-element.37) | data formatting | bytes 32768 | tf_op jit(solution)/shard_map/reshape | solution.py:649
  (10 shorter events, 0.0 us)
Async XLA Ops:
  0.6 3.1 %collective-permute-start = (bf16[256,2048]{1,0:T(8,128)(2,1)}, bf16[256,2048]{1,0:T(8,128)(2,1)S(1)}, u32[]{:S(2)}, u32[]{:S(2)}) collective-permute-start(bf16[256,2048]{1,0:T(8,128)(2,1)} %x_own.3), channel_id=1, source_target_pairs={{0,1},{1,0},{2,3},{3,2},{4,5},{5,4},{6,7},{7,6},{8,9},{9,8},{10,11... | collective-permute-start | bytes 3145736 | tf_op jit(solution)/shard_map/ppermute | solution.py:628
  1.2 115.9 %collective-permute-start.12 = (bf16[512,2048]{1,0:T(8,128)(2,1)}, bf16[512,2048]{1,0:T(8,128)(2,1)S(1)}, u32[]{:S(2)}, u32[]{:S(2)}) collective-permute-start(bf16[512,2048]{1,0:T(8,128)(2,1)} %w_mine.1), channel_id=1, source_target_pairs={{0,1},{1,0},{2,3},{3,2},{4,5},{5,4},{6,7},{7,6},{8,9},{9,8},{10,11... | collective-permute-start | bytes 6291464 | tf_op jit(solution)/shard_map/ppermute | solution.py:637
  3.7 1.0 copy-start
  10.9 15.9 %collective-permute-start.2 = (bf16[512,512]{1,0:T(8,128)(2,1)}, bf16[512,512]{1,0:T(8,128)(2,1)S(1)}, u32[]{:S(2)}, u32[]{:S(2)}) collective-permute-start(bf16[512,512]{1,0:T(8,128)(2,1)} %get-tuple-element.23), channel_id=1, source_target_pairs={{0,2},{2,0},{4,6},{6,4},{8,10},{10,8},{12,14},{14,12},{1,3},{3,1},... | collective-permute-start | bytes 1572872 | tf_op jit(solution)/shard_map/ppermute | solution.py:631
  14.5 18.4 %collective-permute-start.1 = (bf16[512,256]{1,0:T(8,128)(2,1)}, bf16[512,256]{1,0:T(8,128)(2,1)S(1)}, u32[]{:S(2)}, u32[]{:S(2)}) collective-permute-start(bf16[512,256]{1,0:T(8,128)(2,1)} %get-tuple-element.21), channel_id=1, source_target_pairs={{0,2},{2,0},{4,6},{6,4},{8,10},{10,8},{12,14},{14,12},{1,3},{3,1},... | collective-permute-start | bytes 786440 | tf_op jit(solution)/shard_map/ppermute | solution.py:633
  20.8 22.2 %collective-permute-start.3 = (bf16[512,512]{1,0:T(8,128)(2,1)}, bf16[512,512]{1,0:T(8,128)(2,1)S(1)}, u32[]{:S(2)}, u32[]{:S(2)}) collective-permute-start(bf16[512,512]{1,0:T(8,128)(2,1)} %get-tuple-element.22.kv_mine), channel_id=1, source_target_pairs={{0,4},{2,6},{4,8},{6,10},{8,12},{10,14},{1,5},{3,7},{5,9},{7,11},{... | collective-permute-start | bytes 1572872 | tf_op jit(solution)/shard_map/ppermute | solution.py:632
  26.9 40.9 %copy-start.7 = (bf16[512,512]{1,0:T(8,128)(2,1)}, bf16[512,512]{1,0:T(8,128)(2,1)S(1)}, u32[]{:S(2)}) copy-start(bf16[512,512]{1,0:T(8,128)(2,1)S(1)} %collective-permute-done.2.kv_part) | copy-start | bytes 1572868
  26.9 20.3 %collective-permute-start.4 = (bf16[512,512]{1,0:T(8,128)(2,1)S(1)}, bf16[512,512]{1,0:T(8,128)(2,1)}, u32[]{:S(2)}, u32[]{:S(2)}) collective-permute-start(bf16[512,512]{1,0:T(8,128)(2,1)S(1)} %collective-permute-done.2.kv_part), channel_id=1, source_target_pairs={{0,4},{2,6},{4,8},{6,10},{8,12},{10,14},{1,5},{3,7},{5,9},{7,11},{... | collective-permute-start | bytes 1572872 | tf_op jit(solution)/shard_map/ppermute | solution.py:635
  31.7 11.4 %collective-permute-start.5 = (bf16[512,256]{1,0:T(8,128)(2,1)}, bf16[512,256]{1,0:T(8,128)(2,1)}, u32[]{:S(2)}, u32[]{:S(2)}) collective-permute-start(bf16[512,256]{1,0:T(8,128)(2,1)} %get-tuple-element.20.q_mine), channel_id=1, source_target_pairs={{4,0},{6,2},{8,4},{10,6},{12,8},{14,10},{5,1},{7,3},{9,5},{11,7},{... | collective-permute-start | bytes 786440 | tf_op jit(solution)/shard_map/ppermute | solution.py:634
  33.0 34.8 %copy-start.9 = (bf16[512,256]{1,0:T(8,128)(2,1)}, bf16[512,256]{1,0:T(8,128)(2,1)S(1)}, u32[]{:S(2)}) copy-start(bf16[512,256]{1,0:T(8,128)(2,1)S(1)} %collective-permute-done.1.q_part) | copy-start | bytes 786436
  33.0 12.9 %collective-permute-start.6 = (bf16[512,256]{1,0:T(8,128)(2,1)S(1)}, bf16[512,256]{1,0:T(8,128)(2,1)}, u32[]{:S(2)}, u32[]{:S(2)}) collective-permute-start(bf16[512,256]{1,0:T(8,128)(2,1)S(1)} %collective-permute-done.1.q_part), channel_id=1, source_target_pairs={{4,0},{6,2},{8,4},{10,6},{12,8},{14,10},{5,1},{7,3},{9,5},{11,7},{... | collective-permute-start | bytes 786440 | tf_op jit(solution)/shard_map/ppermute | solution.py:636
  43.0 4.1 %copy-start.8 = (bf16[512,512]{1,0:T(8,128)(2,1)}, bf16[512,512]{1,0:T(8,128)(2,1)S(1)}, u32[]{:S(2)}) copy-start(bf16[512,512]{1,0:T(8,128)(2,1)S(1)} %collective-permute-done.3.kv_a) | copy-start | bytes 1572868
  59.7 45.6 %collective-permute-start.8 = (bf16[544,256]{1,0:T(8,128)(2,1)}, bf16[544,256]{1,0:T(8,128)(2,1)S(1)}, u32[]{:S(2)}, u32[]{:S(2)}) collective-permute-start(bf16[544,256]{1,0:T(8,128)(2,1)} %get-tuple-element.32), channel_id=1, source_target_pairs={{0,4},{2,6},{4,8},{6,10},{8,12},{10,14},{1,5},{3,7},{5,9},{7,11},{... | collective-permute-start | bytes 835592 | tf_op jit(solution)/shard_map/ppermute | solution.py:640
  64.2 47.4 %collective-permute-start.7 = (bf16[544,256]{1,0:T(8,128)(2,1)}, bf16[544,256]{1,0:T(8,128)(2,1)S(1)}, u32[]{:S(2)}, u32[]{:S(2)}) collective-permute-start(bf16[544,256]{1,0:T(8,128)(2,1)} %get-tuple-element.30), channel_id=1, source_target_pairs={{0,4},{2,6},{4,8},{6,10},{8,12},{10,14},{1,5},{3,7},{5,9},{7,11},{... | collective-permute-start | bytes 835592 | tf_op jit(solution)/shard_map/ppermute | solution.py:641
  105.3 0.7 copy-start.3
  110.0 8.2 %collective-permute-start.9 = (bf16[288,256]{1,0:T(8,128)(2,1)}, bf16[288,256]{1,0:T(8,128)(2,1)S(1)}, u32[]{:S(2)}, u32[]{:S(2)}) collective-permute-start(bf16[288,256]{1,0:T(8,128)(2,1)} %get-tuple-element.33), channel_id=1, source_target_pairs={{0,2},{2,0},{4,6},{6,4},{8,10},{10,8},{12,14},{14,12},{1,3},{3,1},... | collective-permute-start | bytes 442376 | tf_op jit(solution)/shard_map/ppermute | solution.py:644
  111.6 6.0 %collective-permute-start.11 = (bf16[256,256]{1,0:T(8,128)(2,1)}, bf16[256,256]{1,0:T(8,128)(2,1)S(1)}, u32[]{:S(2)}, u32[]{:S(2)}) collective-permute-start(bf16[256,256]{1,0:T(8,128)(2,1)} %get-tuple-element.35), channel_id=1, source_target_pairs={{0,3},{1,2},{2,1},{3,0},{4,7},{5,6},{6,5},{7,4},{8,11},{9,10},{10,... | collective-permute-start | bytes 393224 | tf_op jit(solution)/shard_map/ppermute | solution.py:645
  111.6 0.7 copy-start.2
  116.4 1.9 %collective-permute-start.10 = (bf16[256,256]{1,0:T(8,128)(2,1)}, bf16[256,256]{1,0:T(8,128)(2,1)S(1)}, u32[]{:S(2)}, u32[]{:S(2)}) collective-permute-start(bf16[256,256]{1,0:T(8,128)(2,1)} %get-tuple-element.34), channel_id=1, source_target_pairs={{0,1},{1,0},{2,3},{3,2},{4,5},{5,4},{6,7},{7,6},{8,9},{9,8},{10,11... | collective-permute-start | bytes 393224 | tf_op jit(solution)/shard_map/ppermute | solution.py:647
  117.1 1.4 %copy-start.1 = (bf16[512,2048]{1,0:T(8,128)(2,1)}, bf16[512,2048]{1,0:T(8,128)(2,1)S(1)}, u32[]{:S(2)}) copy-start(bf16[512,2048]{1,0:T(8,128)(2,1)S(1)} %collective-permute-done.12.w_other) | copy-start | bytes 6291460
  117.6 0.8 copy-start.5
  118.3 0.6 copy-start.6
  118.3 0.7 copy-start.4

commit v2 on v1

--- a/solution.py
+++ b/solution.py
@@ -25,7 +25,12 @@
 ANY = pl.BlockSpec(memory_space=pl.ANY)
 SMEM = pl.BlockSpec(memory_space=pltpu.SMEM)
 VMEM = pl.BlockSpec(memory_space=pltpu.VMEM)
-PARAMS = pltpu.CompilerParams(vmem_limit_bytes=56 * 1024 * 1024)
+MIB = 1024 * 1024
+
+
+def params(limit):
+    return pltpu.CompilerParams(vmem_limit_bytes=limit * MIB)
+
 
 SUB = 16
 
@@ -34,34 +39,13 @@
     return value if isinstance(value, int) else pl.multiple_of(value, multiple)
 
 
-def copy_all(pairs, sems):
-    copies = [pltpu.make_async_copy(s, d, sems.at[n]) for n, (s, d) in enumerate(pairs)]
-    for item in copies:
-        item.start()
-    return copies
-
-
-def project_kernel(lanes, meta, x_own, x_other, w_q, w_k, w_v, kv_out, q_out, xs, ws, acc, sems):
+def project_kernel(lanes, meta, x_own, x_other, w_q, w_k, w_v, kv_out, q_out, acc):
     side, tp = meta[0], meta[1]
-    rows = xs.shape[1]
+    rows = x_own.shape[0]
     columns = pl.ds(aligned(side * lanes, lanes), lanes)
-    copies = copy_all(
-        [
-            (x_own, xs.at[0]),
-            (w_k.at[:, columns], ws.at[0]),
-            (w_v.at[:, columns], ws.at[1]),
-            (x_other, xs.at[1]),
-            (w_q.at[:, columns], ws.at[2]),
-        ],
-        sems,
-    )
-    copies[0].wait()
-    for which in range(3):
-        copies[(1, 2, 4)[which]].wait()
-        for half in range(2):
-            if which == 0 and half == 1:
-                copies[3].wait()
-            result = jnp.dot(xs[half], ws[which], preferred_element_type=F32)
+    for which, w in enumerate((w_k, w_v, w_q)):
+        for half, x in enumerate((x_own, x_other)):
+            result = jnp.dot(x[...], w[:, columns], preferred_element_type=F32)
             for part in range(lanes // 128):
                 acc[part] = result[:, part * 128 : (part + 1) * 128]
             place = (tp if half == 0 else 1 - tp) * rows
@@ -84,15 +68,12 @@
             jax.ShapeDtypeStruct((2 * rows, 2 * lanes), BF16),
             jax.ShapeDtypeStruct((2 * rows, lanes), BF16),
         ],
-        in_specs=[SMEM] + [ANY] * 5,
+        in_specs=[SMEM] + [VMEM] * 5,
         out_specs=[VMEM, VMEM],
         scratch_shapes=[
-            pltpu.VMEM((2, rows, width), BF16),
-            pltpu.VMEM((3, width, lanes), BF16),
             pltpu.VMEM((lanes // 128, rows, 128), F32),
-            pltpu.SemaphoreType.DMA((5,)),
-        ],
-        compiler_params=PARAMS,
+        ],
+        compiler_params=params(14),
         cost_estimate=pl.CostEstimate(
             flops=2 * 2 * rows * width * 3 * lanes,
             bytes_accessed=2 * width * (2 * rows + 3 * lanes),
@@ -191,7 +172,7 @@
     return slice(offset + pair * 128, offset + (pair + 1) * 128)
 
 
-def local_kernel(meta, slopes, q_mine, q_part, kv_mine, kv_part, o_ref, m_ref, l_ref, q, kv, near, mid, sems):
+def local_kernel(meta, slopes, q_mine, q_part, kv_mine, kv_part, o_ref, m_ref, l_ref, q, kv, near, mid):
     y = meta[2]
     block, lanes = q_mine.shape
     pairs = lanes // 128
@@ -199,18 +180,14 @@
     chunks = block // tile
     mine = pl.ds(aligned(y * block, block), block)
     part = pl.ds(aligned((1 - y) * block, block), block)
-    copies = copy_all(
-        [(q_mine, q.at[mine]), (q_part, q.at[part]), (kv_mine, kv.at[mine]), (kv_part, kv.at[part])],
-        sems,
-    )
+    q[mine], q[part] = q_mine[...], q_part[...]
+    kv[mine], kv[part] = kv_mine[...], kv_part[...]
     distance = near_distance(True, True)
     for head in range(2 * pairs):
         near[head] = bias_of(distance, slopes[head], 1)
     distance = middle_distance(True, True, chunks)
     for head in range(2 * pairs):
         mid[head] = bias_of(distance, slopes[head], MIDDLE_DILATION)
-    for item in copies:
-        item.wait()
     refs = (o_ref, m_ref, l_ref)
     step = 64
     per_tile = tile // step
@@ -270,16 +247,15 @@
     return pl.pallas_call(
         local_kernel,
         out_shape=[state] * 3,
-        in_specs=[SMEM, SMEM] + [ANY] * 4,
+        in_specs=[SMEM, SMEM] + [VMEM] * 4,
         out_specs=[VMEM] * 3,
         scratch_shapes=[
             pltpu.VMEM((2 * block, lanes), BF16),
             pltpu.VMEM((2 * block, 2 * lanes), BF16),
             pltpu.VMEM((heads, tile, 2 * tile), F32),
             pltpu.VMEM((heads, size, 2 * size), F32),
-            pltpu.SemaphoreType.DMA((4,)),
-        ],
-        compiler_params=PARAMS,
+        ],
+        compiler_params=params(20),
         cost_estimate=pl.CostEstimate(flops=4 * 10**9, bytes_accessed=4 * 10**6, transcendentals=0),
         name="local",
     )(meta, slopes, q_mine, q_part, kv_mine, kv_part)
@@ -287,7 +263,7 @@
 
 def before_kernel(
     meta, slopes, gate, q_mine, q_part, kv_mine, kv_part, kv_a, kv_b, o_in, m_in, l_in,
-    o_ref, m_ref, l_ref, q, kv, past, near, mid, far, sems,
+    o_ref, m_ref, l_ref, q, kv, past, near, mid, far,
 ):
     y = meta[2]
     block, lanes = q_mine.shape
@@ -296,14 +272,10 @@
     chunks = block // tile
     mine = pl.ds(aligned(y * block, block), block)
     part = pl.ds(aligned((1 - y) * block, block), block)
-    copies = copy_all(
-        [
-            (q_mine, q.at[mine]), (q_part, q.at[part]), (kv_mine, kv.at[mine]), (kv_part, kv.at[part]),
-            (kv_a, past.at[mine]), (kv_b, past.at[part]),
-            (o_in, o_ref), (m_in, m_ref), (l_in, l_ref),
-        ],
-        sems,
-    )
+    q[mine], q[part] = q_mine[...], q_part[...]
+    kv[mine], kv[part] = kv_mine[...], kv_part[...]
+    past[mine], past[part] = kv_a[...], kv_b[...]
+    o_ref[...], m_ref[...], l_ref[...] = o_in[...], m_in[...], l_in[...]
     closed = gate[0]
     size = mid.shape[1]
     row = lax.broadcasted_iota(jnp.int32, far.shape[1:], 0)
@@ -314,12 +286,9 @@
         far[head] = bias_of(steps, slopes[head], FAR_DILATION) + jnp.where(col < half, closed, 0.0)
         near[head] = bias_of(near_distance(True, False), slopes[head], 1) + closed
         mid[head] = bias_of(middle_distance(True, False, chunks), slopes[head], MIDDLE_DILATION) + closed
-    for item in copies:
-        item.wait()
     refs = (o_ref, m_ref, l_ref)
 
-    @pl.loop(0, FAR_DILATION)
-    def _(residue):
+    for residue in range(FAR_DILATION):
         starts = far_starts(residue, 2 * chunks)
         for pair in range(pairs):
             keys = [rows_of(ref, starts, pair_lanes(pair)) for ref in (past, kv)]
@@ -373,7 +342,7 @@
     return pl.pallas_call(
         before_kernel,
         out_shape=[shape] * 3,
-        in_specs=[SMEM, SMEM, SMEM] + [ANY] * 9,
+        in_specs=[SMEM, SMEM, SMEM] + [VMEM] * 9,
         out_specs=[VMEM] * 3,
         scratch_shapes=[
             pltpu.VMEM((2 * block, lanes), BF16),
@@ -382,9 +351,8 @@
             pltpu.VMEM((heads, tile, tile), F32),
             pltpu.VMEM((heads, size, size), F32),
             pltpu.VMEM((heads, reach, 2 * reach), F32),
-            pltpu.SemaphoreType.DMA((9,)),
-        ],
-        compiler_params=PARAMS,
+        ],
+        compiler_params=params(24),
         cost_estimate=pl.CostEstimate(flops=2 * 10**9, bytes_accessed=4 * 10**6, transcendentals=0),
         name="before",
     )(meta, slopes, gate, q_mine, q_part, kv_mine, kv_part, kv_a, kv_b, *state)
@@ -422,7 +390,7 @@
     return lax.dot_general(packed, spreader(lanes), (((0,), (0,)), ((), ())), preferred_element_type=F32)
 
 
-def remote_kernel(meta, slopes, gate, q_a, q_b, kv_a, kv_b, own_ref, other_ref, q, kv, far, out, sums, sems):
+def remote_kernel(meta, slopes, gate, after, q_a, q_b, kv_a, kv_b, own_ref, other_ref, q, kv, far, out, sums):
     y = meta[2]
     block, lanes = q_a.shape
     pairs = lanes // 128
@@ -430,20 +398,16 @@
     chunks = block // tile
     mine = pl.ds(aligned(y * block, block), block)
     part = pl.ds(aligned((1 - y) * block, block), block)
-    copies = copy_all(
-        [(q_a, q.at[mine]), (q_b, q.at[part]), (kv_a, kv.at[mine]), (kv_b, kv.at[part])], sems
-    )
+    q[mine], q[part] = q_a[...], q_b[...]
+    kv[mine], kv[part] = kv_a[...], kv_b[...]
     closed = gate[0]
     row = lax.broadcasted_iota(jnp.int32, far.shape[1:], 0)
     col = lax.broadcasted_iota(jnp.int32, far.shape[1:], 1)
     steps = row - col + 2 * far.shape[2]
     for head in range(2 * pairs):
         far[head] = bias_of(steps, slopes[head], FAR_DILATION) + closed
-    for item in copies:
-        item.wait()
-
-    @pl.loop(0, FAR_DILATION)
-    def _(residue):
+
+    for residue in range(FAR_DILATION):
         starts = far_starts(residue, 2 * chunks)
         for pair in range(pairs):
             o, m, l = attend(
@@ -468,7 +432,7 @@
             ref[block + 16 * n : block + 16 * (n + 1)] = packed[:, n * lanes : (n + 1) * lanes]
 
 
-def remote_attention(meta, slopes, gate, q_a, q_b, kv_a, kv_b):
+def remote_attention(meta, slopes, gate, after, q_a, q_b, kv_a, kv_b):
     block, lanes = q_a.shape
     heads = lanes // HEAD_DIM
     reach = 2 * block // FAR_DILATION
@@ -476,7 +440,7 @@
     return pl.pallas_call(
         remote_kernel,
         out_shape=[shape] * 2,
-        in_specs=[SMEM, SMEM, SMEM] + [ANY] * 4,
+        in_specs=[SMEM, SMEM, SMEM, ANY] + [VMEM] * 4,
         out_specs=[VMEM] * 2,
         scratch_shapes=[
             pltpu.VMEM((2 * block, lanes), BF16),
@@ -484,25 +448,20 @@
             pltpu.VMEM((heads, reach, reach), F32),
             pltpu.VMEM((2 * block, lanes), BF16),
             pltpu.VMEM((2 * block, lanes), F32),
-            pltpu.SemaphoreType.DMA((4,)),
-        ],
-        compiler_params=PARAMS,
+        ],
+        compiler_params=params(12),
         cost_estimate=pl.CostEstimate(flops=10**9, bytes_accessed=2 * 10**6, transcendentals=0),
         name="remote",
-    )(meta, slopes, gate, q_a, q_b, kv_a, kv_b)
-
-
-def finish_kernel(meta, gate, o_in, m_in, l_in, far_in, stay_ref, go_ref, o_s, m_s, l_s, turned, sems):
+    )(meta, slopes, gate, after, q_a, q_b, kv_a, kv_b)
+
+
+def finish_kernel(meta, gate, o_in, m_in, l_in, far_in, stay_ref, go_ref, o_s, m_s, l_s, turned):
     which, tp = meta[0], meta[1]
     block, lanes = o_s.shape
     tile = FAR_DILATION * SUB
     chunks = block // tile
     select = pl.ds(aligned(which * block, block), block)
-    copies = copy_all(
-        [(o_in.at[select], o_s), (m_in.at[select], m_s), (l_in.at[select], l_s)], sems
-    )
-    for item in copies:
-        item.wait()
+    o_s[...], m_s[...], l_s[...] = o_in[select], m_in[select], l_in[select]
     per = lanes // tile
     for s in range(chunks):
         rows = slice(s * tile, (s + 1) * tile)
@@ -541,16 +500,15 @@
             jax.ShapeDtypeStruct((half + 16 * (block // lanes), lanes), BF16),
             jax.ShapeDtypeStruct((half, lanes), BF16),
         ],
-        in_specs=[SMEM, SMEM] + [ANY] * 3 + [VMEM],
+        in_specs=[SMEM, SMEM] + [VMEM] * 4,
         out_specs=[VMEM] * 2,
         scratch_shapes=[
             pltpu.VMEM((block, lanes), F32),
             pltpu.VMEM((block, lanes), F32),
             pltpu.VMEM((block, lanes), F32),
             pltpu.VMEM((2, lanes // 128, block, 128), F32),
-            pltpu.SemaphoreType.DMA((3,)),
-        ],
-        compiler_params=PARAMS,
+        ],
+        compiler_params=params(14),
         cost_estimate=pl.CostEstimate(flops=5 * 10**8, bytes_accessed=2 * 10**6, transcendentals=0),
         name="finish",
     )(meta, gate, *state, far)
@@ -572,11 +530,17 @@
         second = jnp.dot(tp_piece[...], w_other[near_rows, columns], preferred_element_type=F32)
         second += jnp.dot(cross[...], w_other[far_rows, columns], preferred_element_type=F32)
         out_ref[:, columns] = (first.astype(BF16).astype(F32) + second.astype(BF16).astype(F32)).astype(BF16)
-    for ref, place in ((stay, y), (same, 1 - y)):
+    halves = []
+    for ref in (stay, same):
+        both = []
         for n in range(block // lanes):
             packed = ref[half + 16 * n : half + 16 * (n + 1)].astype(F32)
             total = packed[:heads] + packed[heads : 2 * heads] + packed[2 * heads : 3 * heads]
-            sums_ref[place, :, n * lanes : (n + 1) * lanes] = total
+            both.append(total)
+        halves.append(jnp.concatenate(both, axis=1))
+    low = jnp.where(y == 0, halves[0], halves[1])
+    high = jnp.where(y == 0, halves[1], halves[0])
+    sums_ref[...] = jnp.concatenate([low, high], axis=0)
 
 
 def output(meta, stay, same, tp_piece, cross, w_mine, w_other):
@@ -587,11 +551,11 @@
         output_kernel,
         out_shape=[
             jax.ShapeDtypeStruct((half, width), BF16),
-            jax.ShapeDtypeStruct((2, heads, 2 * half), F32),
+            jax.ShapeDtypeStruct((2 * heads, 2 * half), F32),
         ],
         in_specs=[SMEM] + [VMEM] * 6,
         out_specs=[VMEM] * 2,
-        compiler_params=PARAMS,
+        compiler_params=params(16),
         cost_estimate=pl.CostEstimate(
             flops=2 * half * width * 4 * lanes, bytes_accessed=6 * 10**6, transcendentals=0
         ),
@@ -636,7 +600,7 @@
     q_b = lax.ppermute(q_p, "sp", back)
     w_other = lax.ppermute(w_out, "tp", swap)
     state = local_attention(meta_mine, slopes, q_m, q_p, kv_m, kv_p)
-    far_own, far_other = remote_attention(meta_mine, slopes, gate, q_a, q_b, kv_a, kv_b)
+    far_own, far_other = remote_attention(meta_mine, slopes, gate, state[2], q_a, q_b, kv_a, kv_b)
     far_p = lax.ppermute(far_other, "sp", ahead)
     far_m = lax.ppermute(far_own, "sp", ahead)
     state = before_attention(meta_mine, slopes, gate, q_m, q_p, kv_m, kv_p, kv_a, kv_b, state)
@@ -646,7 +610,7 @@
     stay, tp_go = finish(meta_mine, gate, state, far_m)
     tp_piece = lax.ppermute(tp_go, "tp", swap)
     mixed, sums = output(meta_mine, stay, same, tp_piece, cross, w_out, w_other)
-    return mixed, sums.reshape(2 * heads, block)
+    return mixed, sums
 
 
 def solution(mesh):

time: 126 us -> 92.2 us (0.73)
  Pallas kernels: 75.5 us -> 45.6 us
  waiting for transfers between devices: 17.3 us -> 11.9 us
  local copies, waits for them, and re-layouts: 4.42 us -> 7.67 us
  other arithmetic: 1.78 us -> 0.16 us
    pallas_call x1, Pallas kernels: 12.5 us -> 2.74 us  [remote_attention(): pl.pallas_call(remote_kernel, out_shape=[shape] * 2, in_specs=[SMEM, SMEM...]
    ppermute x1, waiting for transfers between devices: 8.19 us -> 0.01 us  [body(): q_a = lax.ppermute(q_m, 'sp', back)]
    pallas_call x2, Pallas kernels: 12.6 us -> 6.87 us  [project(): pl.pallas_call(functools.partial(project_kernel, lanes), out_shape=[jax.S...]
    pallas_call x1, Pallas kernels: 20 us -> 14.5 us  [before_attention(): pl.pallas_call(before_kernel, out_shape=[shape] * 3, in_specs=[SMEM, SMEM...]
    pallas_call x2, Pallas kernels: 8.07 us -> 3.04 us  [finish(): pl.pallas_call(finish_kernel, out_shape=[jax.ShapeDtypeStruct((half + 16...]
    unnamed x20, local copies, waits for them, and re-layouts: 3.09 us -> 7.67 us
    ppermute x1, waiting for transfers between devices: 0.56 us -> 3.87 us  [body(): cross = lax.ppermute(cross_go, ('sp', 'tp'), crossed)]
    ppermute x1, waiting for transfers between devices: 2.02 us -> 4.94 us  [body(): kv_p = lax.ppermute(kv_t, 'sp', beside)]
  transfers between devices with their start and end apart: 13 -> 13, of which waited for: 7 -> 4; matrix products, arithmetic and copies ran while one was open for 1% -> 0% of each run, Pallas kernels for 57% -> 47%
where the time goes in v2:
time: 92.2 us; the launch traced here: 91.7 us
  Pallas kernels  45.6 us (49%)
  starting transfers between devices  25.6 us (28%)
  waiting for transfers between devices  11.9 us (13%)
  local copies, waits for them, and re-layouts  7.67 us (8%)
    pallas_call x1, Pallas kernels, local_attention(): pl.pallas_call(local_kernel, out_shape=[state] * 3, in_specs=[SMEM, SMEM]...  15.6 us
    pallas_call x1, Pallas kernels, before_attention(): pl.pallas_call(before_kernel, out_shape=[shape] * 3, in_specs=[SMEM, SMEM...  14.5 us
    unnamed x20, local copies, waits for them, and re-layouts  7.67 us
    pallas_call x2, Pallas kernels, project(): pl.pallas_call(functools.partial(project_kernel, lanes), out_shape=[jax.S...  6.87 us
    ppermute x1, starting transfers between devices, body(): far_p = lax.ppermute(far_other, 'sp', ahead)  5.19 us
    ppermute x1, waiting for transfers between devices, body(): kv_p = lax.ppermute(kv_t, 'sp', beside)  4.94 us
    ppermute x1, starting transfers between devices, body(): far_m = lax.ppermute(far_own, 'sp', ahead)  4.1 us
    ppermute x1, starting transfers between devices, body(): kv_b = lax.ppermute(kv_p, 'sp', ahead)  3.98 us
  transfers between devices with their start and end apart: 13, of which 4 were waited for; matrix products, arithmetic and copies ran while one was open for 0% of the time, Pallas kernels for 47%

profile of v2, /device:TPU:0, one launch (start us, length us, event | category | flops | bytes accessed | tf_op | source)
XLA Modules:
  0.0 91.7 jit_solution(13569560900736764533)
XLA Ops:
  0.6 0.6 collective-permute-start
  1.2 0.1 collective-permute-start.12
  1.3 0.1 add_add_fusion.1.meta
  1.3 2.3 %collective-permute-done.x_other = bf16[256,2048]{1,0:T(8,128)(2,1)S(1)} collective-permute-done((bf16[256,2048]{1,0:T(8,128)(2,1)}, bf16[256,2048]{1,0:T(8,128)(2,1)S(1)}, u32[]{:S(2)}, u32[]{:S(2)}) %collective-permute-start) | collective-permute-done | bytes 1048608 | tf_op jit(solution)/shard_map/ppermute | solution.py:592
  3.7 1.6 %copy-done = bf16[2048,512]{1,0:T(8,128)(2,1)S(1)} copy-done((bf16[2048,512]{1,0:T(8,128)(2,1)S(1)}, bf16[2048,512]{1,0:T(8,128)(2,1)}, u32[]{:S(2)}) %copy-start) | copy-done | bytes 2097176
  5.3 1.6 %copy-done.2 = bf16[2048,512]{1,0:T(8,128)(2,1)S(1)} copy-done((bf16[2048,512]{1,0:T(8,128)(2,1)S(1)}, bf16[2048,512]{1,0:T(8,128)(2,1)}, u32[]{:S(2)}) %copy-start.2) | copy-done | bytes 2097176
  6.9 1.6 %copy-done.3 = bf16[2048,512]{1,0:T(8,128)(2,1)S(1)} copy-done((bf16[2048,512]{1,0:T(8,128)(2,1)S(1)}, bf16[2048,512]{1,0:T(8,128)(2,1)}, u32[]{:S(2)}) %copy-start.3) | copy-done | bytes 2097176
  8.5 1.2 %copy-done.4 = bf16[256,2048]{1,0:T(8,128)(2,1)S(1)} copy-done((bf16[256,2048]{1,0:T(8,128)(2,1)S(1)}, bf16[256,2048]{1,0:T(8,128)(2,1)}, u32[]{:S(2)}) %copy-start.4) | copy-done | bytes 1048600
  9.7 3.7 %project.3 = (bf16[512,512]{1,0:T(8,128)(2,1)S(1)}, bf16[512,256]{1,0:T(8,128)(2,1)}) custom-call(s32[3]{0:T(128)S(1)} %add_add_fusion.1.meta, bf16[256,2048]{1,0:T(8,128)(2,1)S(1)} %copy-done.4, bf16[256,2048]{1,0:T(8,128)(2,1)S(1)} %collective-permute-done.x_other, bf16[2048,512]{1,0:T(8,128)(2,1)S(1)} %copy-done, bf16[2048,512]{1,0:T(8,128)(2,1)S(1)} %copy-done.2, ...), custom_call_target="tpu_custom_call" | custom-call | flops 1610612736 | bytes 5242880 | tf_op jit(solution)/shard_map/project/pallas_call | solution.py:65
  13.4 2.9 %collective-permute-start.2 = (bf16[512,512]{1,0:T(8,128)(2,1)S(1)}, bf16[512,512]{1,0:T(8,128)(2,1)}, u32[]{:S(2)}, u32[]{:S(2)}) collective-permute-start(bf16[512,512]{1,0:T(8,128)(2,1)S(1)} %get-tuple-element.21), channel_id=1, source_target_pairs={{0,2},{2,0},{4,6},{6,4},{8,10},{10,8},{12,14},{14,12},{1,3},{3,1},... | collective-permute-start | bytes 1572872 | tf_op jit(solution)/shard_map/ppermute | solution.py:595
  16.3 0.1 add_add_fusion.meta
  16.4 0.0 collective-permute-start.1
  16.4 0.0 copy-done.1
  16.4 0.0 copy-done.5
  16.4 3.1 %project.2 = (bf16[512,512]{1,0:T(8,128)(2,1)}, bf16[512,256]{1,0:T(8,128)(2,1)S(1)}) custom-call(s32[3]{0:T(128)S(1)} %add_add_fusion.meta, bf16[256,2048]{1,0:T(8,128)(2,1)S(1)} %copy-done.5, bf16[256,2048]{1,0:T(8,128)(2,1)S(1)} %collective-permute-done.x_other, bf16[2048,512]{1,0:T(8,128)(2,1)S(1)} %copy-done.1, bf16[2048,512]{1,0:T(8,128)(2,1)S(1)} %copy-done.2, ...), custom_call_target="tpu_custom_call" | custom-call | flops 1610612736 | bytes 5242880 | tf_op jit(solution)/shard_map/project/pallas_call | solution.py:65
  19.6 0.7 copy-done.7
  20.3 4.0 %collective-permute-start.3 = (bf16[512,512]{1,0:T(8,128)(2,1)}, bf16[512,512]{1,0:T(8,128)(2,1)S(1)}, u32[]{:S(2)}, u32[]{:S(2)}) collective-permute-start(bf16[512,512]{1,0:T(8,128)(2,1)} %get-tuple-element.20.kv_mine), channel_id=1, source_target_pairs={{0,4},{2,6},{4,8},{6,10},{8,12},{10,14},{1,5},{3,7},{5,9},{7,11},{... | collective-permute-start | bytes 1572872 | tf_op jit(solution)/shard_map/ppermute | solution.py:596
  24.2 4.9 %collective-permute-done.2.kv_part = bf16[512,512]{1,0:T(8,128)(2,1)} collective-permute-done((bf16[512,512]{1,0:T(8,128)(2,1)S(1)}, bf16[512,512]{1,0:T(8,128)(2,1)}, u32[]{:S(2)}, u32[]{:S(2)}) %collective-permute-start.2) | collective-permute-done | bytes 524320 | tf_op jit(solution)/shard_map/ppermute | solution.py:595
  29.2 4.0 %collective-permute-start.4 = (bf16[512,512]{1,0:T(8,128)(2,1)}, bf16[512,512]{1,0:T(8,128)(2,1)S(1)}, u32[]{:S(2)}, u32[]{:S(2)}) collective-permute-start(bf16[512,512]{1,0:T(8,128)(2,1)} %collective-permute-done.2.kv_part), channel_id=1, source_target_pairs={{0,4},{2,6},{4,8},{6,10},{8,12},{10,14},{1,5},{3,7},{5,9},{7,11},{... | collective-permute-start | bytes 1572872 | tf_op jit(solution)/shard_map/ppermute | solution.py:599
  33.2 1.3 %collective-permute-start.5 = (bf16[512,256]{1,0:T(8,128)(2,1)}, bf16[512,256]{1,0:T(8,128)(2,1)S(1)}, u32[]{:S(2)}, u32[]{:S(2)}) collective-permute-start(bf16[512,256]{1,0:T(8,128)(2,1)} %copy-done.7), channel_id=1, source_target_pairs={{4,0},{6,2},{8,4},{10,6},{12,8},{14,10},{5,1},{7,3},{9,5},{11,7},{... | collective-permute-start | bytes 786440 | tf_op jit(solution)/shard_map/ppermute | solution.py:598
  34.5 0.0 collective-permute-done.1.q_part
  34.5 1.3 %collective-permute-start.6 = (bf16[512,256]{1,0:T(8,128)(2,1)S(1)}, bf16[512,256]{1,0:T(8,128)(2,1)S(1)}, u32[]{:S(2)}, u32[]{:S(2)}) collective-permute-start(bf16[512,256]{1,0:T(8,128)(2,1)S(1)} %collective-permute-done.1.q_part), channel_id=1, source_target_pairs={{4,0},{6,2},{8,4},{10,6},{12,8},{14,10},{5,1},{7,3},{9,5},{11,7},{... | collective-permute-start | bytes 786440 | tf_op jit(solution)/shard_map/ppermute | solution.py:600
  35.8 0.0 copy-start.8
  35.8 0.9 %copy-done.8 = bf16[512,256]{1,0:T(8,128)(2,1)S(1)} copy-done((bf16[512,256]{1,0:T(8,128)(2,1)S(1)}, bf16[512,256]{1,0:T(8,128)(2,1)}, u32[]{:S(2)}) %copy-start.8) | copy-done | bytes 262168
  36.8 15.6 %local.1 = (f32[1024,256]{1,0:T(8,128)S(1)}, f32[1024,256]{1,0:T(8,128)S(1)}, f32[1024,256]{1,0:T(8,128)S(1)}) custom-call(s32[3]{0:T(128)S(1)} %add_add_fusion.meta, f32[4]{0:T(128)S(1)} %exponential_multiply_fusion.slopes, bf16[512,256]{1,0:T(8,128)(2,1)S(1)} %copy-done.8, bf16[512,256]{1,0:T(8,128)(2,1)S(1)} %collective-permute-done.1.q_part, ...), custom_call_target="tpu_custom_call" | custom-call | flops 4000000000 | bytes 4000000 | tf_op jit(solution)/shard_map/local/pallas_call | solution.py:247
  52.4 0.0 copy-start.9
  52.4 0.0 collective-permute-done.5.q_a
  52.4 0.0 collective-permute-done.3.kv_a
  52.5 0.0 collective-permute-done.6.q_b
  52.5 0.0 collective-permute-done.4.kv_b
  52.5 2.7 %remote.1 = (bf16[544,256]{1,0:T(8,128)(2,1)S(1)}, bf16[544,256]{1,0:T(8,128)(2,1)S(1)}) custom-call(s32[3]{0:T(128)S(1)} %add_add_fusion.meta, f32[4]{0:T(128)S(1)} %exponential_multiply_fusion.slopes, f32[1]{0:T(128)} %bitcast.2.gate, f32[1024,256]{1,0:T(8,128)S(1)} %get-tuple-element.24.l_in.after, bf16[512,256]{1,0:T(8,128)(2,1)S(1)} %collective-permute-done.5.q_a, ...), custom_call_target="tpu_custom_call" | custom-call | flops 1000000000 | bytes 2000000 | tf_op jit(solution)/shard_map/remote/pallas_call | solution.py:440
  55.2 5.2 %collective-permute-start.8 = (bf16[544,256]{1,0:T(8,128)(2,1)S(1)}, bf16[544,256]{1,0:T(8,128)(2,1)S(1)}, u32[]{:S(2)}, u32[]{:S(2)}) collective-permute-start(bf16[544,256]{1,0:T(8,128)(2,1)S(1)} %get-tuple-element.30), channel_id=1, source_target_pairs={{0,4},{2,6},{4,8},{6,10},{8,12},{10,14},{1,5},{3,7},{5,9},{7,11},{... | collective-permute-start | bytes 835592 | tf_op jit(solution)/shard_map/ppermute | solution.py:604
  60.4 4.1 %collective-permute-start.7 = (bf16[544,256]{1,0:T(8,128)(2,1)S(1)}, bf16[544,256]{1,0:T(8,128)(2,1)S(1)}, u32[]{:S(2)}, u32[]{:S(2)}) collective-permute-start(bf16[544,256]{1,0:T(8,128)(2,1)S(1)} %get-tuple-element.28), channel_id=1, source_target_pairs={{0,4},{2,6},{4,8},{6,10},{8,12},{10,14},{1,5},{3,7},{5,9},{7,11},{... | collective-permute-start | bytes 835592 | tf_op jit(solution)/shard_map/ppermute | solution.py:605
  64.5 0.0 copy-done.9
  64.5 14.5 %before.1 = (f32[1024,256]{1,0:T(8,128)S(1)}, f32[1024,256]{1,0:T(8,128)S(1)}, f32[1024,256]{1,0:T(8,128)S(1)}) custom-call(s32[3]{0:T(128)S(1)} %add_add_fusion.meta, f32[4]{0:T(128)S(1)} %exponential_multiply_fusion.slopes, f32[1]{0:T(128)} %bitcast.2.gate, bf16[512,256]{1,0:T(8,128)(2,1)S(1)} %copy-done.9, ...), custom_call_target="tpu_custom_call" | custom-call | flops 2000000000 | bytes 4000000 | tf_op jit(solution)/shard_map/before/pallas_call | solution.py:342
  79.0 0.0 collective-permute-done.8.far_in
  79.0 1.5 %finish.3 = (bf16[288,256]{1,0:T(8,128)(2,1)S(1)}, bf16[256,256]{1,0:T(8,128)(2,1)S(1)}) custom-call(s32[3]{0:T(128)S(1)} %add_add_fusion.1.meta, f32[1]{0:T(128)} %bitcast.2.gate, f32[1024,256]{1,0:T(8,128)S(1)} %get-tuple-element.25.o_in, f32[1024,256]{1,0:T(8,128)S(1)} %get-tuple-element.26.m_in, f32[1024,256]{1,0:T(8,128)S(1)} %get-tuple-element.27.l_in, ...), custom_call_target="tpu_custom_call" | custom-call | flops 500000000 | bytes 2000000 | tf_op jit(solution)/shard_map/finish/pallas_call | solution.py:497
  80.5 1.6 %collective-permute-start.9 = (bf16[288,256]{1,0:T(8,128)(2,1)S(1)}, bf16[288,256]{1,0:T(8,128)(2,1)S(1)}, u32[]{:S(2)}, u32[]{:S(2)}) collective-permute-start(bf16[288,256]{1,0:T(8,128)(2,1)S(1)} %get-tuple-element.31), channel_id=1, source_target_pairs={{0,2},{2,0},{4,6},{6,4},{8,10},{10,8},{12,14},{14,12},{1,3},{3,1},... | collective-permute-start | bytes 442376 | tf_op jit(solution)/shard_map/ppermute | solution.py:608
  82.1 0.0 collective-permute-done.7.far_in
  82.1 1.5 %finish.2 = (bf16[288,256]{1,0:T(8,128)(2,1)S(1)}, bf16[256,256]{1,0:T(8,128)(2,1)S(1)}) custom-call(s32[3]{0:T(128)S(1)} %add_add_fusion.meta, f32[1]{0:T(128)} %bitcast.2.gate, f32[1024,256]{1,0:T(8,128)S(1)} %get-tuple-element.25.o_in, f32[1024,256]{1,0:T(8,128)S(1)} %get-tuple-element.26.m_in, f32[1024,256]{1,0:T(8,128)S(1)} %get-tuple-element.27.l_in, ...), custom_call_target="tpu_custom_call" | custom-call | flops 500000000 | bytes 2000000 | tf_op jit(solution)/shard_map/finish/pallas_call | solution.py:497
  83.6 0.0 collective-permute-start.10
  83.7 0.6 collective-permute-start.11
  84.3 0.0 collective-permute-done.12.w_other
  84.3 0.7 collective-permute-done.10.tp_piece
  85.0 3.9 %collective-permute-done.11.cross = bf16[256,256]{1,0:T(8,128)(2,1)S(1)} collective-permute-done((bf16[256,256]{1,0:T(8,128)(2,1)S(1)}, bf16[256,256]{1,0:T(8,128)(2,1)S(1)}, u32[]{:S(2)}, u32[]{:S(2)}) %collective-permute-start.11) | collective-permute-done | bytes 131104 | tf_op jit(solution)/shard_map/ppermute | solution.py:609
  88.9 0.0 collective-permute-done.9.same
  88.9 0.0 copy-done.6
  88.9 2.8 %output.1 = (bf16[256,2048]{1,0:T(8,128)(2,1)}, f32[8,512]{1,0:T(8,128)}) custom-call(s32[3]{0:T(128)S(1)} %add_add_fusion.meta, bf16[288,256]{1,0:T(8,128)(2,1)S(1)} %get-tuple-element.29.stay, bf16[288,256]{1,0:T(8,128)(2,1)S(1)} %collective-permute-done.9.same, bf16[256,256]{1,0:T(8,128)(2,1)S(1)} %collective-permute-done.10.tp_piece, ...), custom_call_target="tpu_custom_call" | custom-call | flops 1073741824 | bytes 6000000 | tf_op jit(solution)/shard_map/output/pallas_call | solution.py:550
  (9 shorter events, 0.0 us)
Async XLA Ops:
  0.6 3.1 %collective-permute-start = (bf16[256,2048]{1,0:T(8,128)(2,1)}, bf16[256,2048]{1,0:T(8,128)(2,1)S(1)}, u32[]{:S(2)}, u32[]{:S(2)}) collective-permute-start(bf16[256,2048]{1,0:T(8,128)(2,1)} %x_own.3), channel_id=1, source_target_pairs={{0,1},{1,0},{2,3},{3,2},{4,5},{5,4},{6,7},{7,6},{8,9},{9,8},{10,11... | collective-permute-start | bytes 3145736 | tf_op jit(solution)/shard_map/ppermute | solution.py:592
  1.2 83.1 %collective-permute-start.12 = (bf16[512,2048]{1,0:T(8,128)(2,1)}, bf16[512,2048]{1,0:T(8,128)(2,1)S(1)}, u32[]{:S(2)}, u32[]{:S(2)}) collective-permute-start(bf16[512,2048]{1,0:T(8,128)(2,1)} %w_mine.1), channel_id=1, source_target_pairs={{0,1},{1,0},{2,3},{3,2},{4,5},{5,4},{6,7},{7,6},{8,9},{9,8},{10,11... | collective-permute-start | bytes 6291464 | tf_op jit(solution)/shard_map/ppermute | solution.py:601
  3.7 1.6 %copy-start = (bf16[2048,512]{1,0:T(8,128)(2,1)S(1)}, bf16[2048,512]{1,0:T(8,128)(2,1)}, u32[]{:S(2)}) copy-start(bf16[2048,512]{1,0:T(8,128)(2,1)} %w_q.3) | copy-start | bytes 6291460
  5.3 1.6 %copy-start.2 = (bf16[2048,512]{1,0:T(8,128)(2,1)S(1)}, bf16[2048,512]{1,0:T(8,128)(2,1)}, u32[]{:S(2)}) copy-start(bf16[2048,512]{1,0:T(8,128)(2,1)} %w_k.3) | copy-start | bytes 6291460
  6.9 1.6 %copy-start.3 = (bf16[2048,512]{1,0:T(8,128)(2,1)S(1)}, bf16[2048,512]{1,0:T(8,128)(2,1)}, u32[]{:S(2)}) copy-start(bf16[2048,512]{1,0:T(8,128)(2,1)} %w_v.3) | copy-start | bytes 6291460
  8.5 1.2 %copy-start.4 = (bf16[256,2048]{1,0:T(8,128)(2,1)S(1)}, bf16[256,2048]{1,0:T(8,128)(2,1)}, u32[]{:S(2)}) copy-start(bf16[256,2048]{1,0:T(8,128)(2,1)} %x_own.3) | copy-start | bytes 3145732
  9.7 6.7 %copy-start.1 = (bf16[2048,512]{1,0:T(8,128)(2,1)S(1)}, bf16[2048,512]{1,0:T(8,128)(2,1)}, u32[]{:S(2)}) copy-start(bf16[2048,512]{1,0:T(8,128)(2,1)} %w_q.3) | copy-start | bytes 6291460
  9.7 6.7 %copy-start.5 = (bf16[256,2048]{1,0:T(8,128)(2,1)S(1)}, bf16[256,2048]{1,0:T(8,128)(2,1)}, u32[]{:S(2)}) copy-start(bf16[256,2048]{1,0:T(8,128)(2,1)} %x_own.3) | copy-start | bytes 3145732
  13.4 15.8 %collective-permute-start.2 = (bf16[512,512]{1,0:T(8,128)(2,1)S(1)}, bf16[512,512]{1,0:T(8,128)(2,1)}, u32[]{:S(2)}, u32[]{:S(2)}) collective-permute-start(bf16[512,512]{1,0:T(8,128)(2,1)S(1)} %get-tuple-element.21), channel_id=1, source_target_pairs={{0,2},{2,0},{4,6},{6,4},{8,10},{10,8},{12,14},{14,12},{1,3},{3,1},... | collective-permute-start | bytes 1572872 | tf_op jit(solution)/shard_map/ppermute | solution.py:595
  16.4 18.1 %collective-permute-start.1 = (bf16[512,256]{1,0:T(8,128)(2,1)}, bf16[512,256]{1,0:T(8,128)(2,1)S(1)}, u32[]{:S(2)}, u32[]{:S(2)}) collective-permute-start(bf16[512,256]{1,0:T(8,128)(2,1)} %get-tuple-element.19), channel_id=1, source_target_pairs={{0,2},{2,0},{4,6},{6,4},{8,10},{10,8},{12,14},{14,12},{1,3},{3,1},... | collective-permute-start | bytes 786440 | tf_op jit(solution)/shard_map/ppermute | solution.py:597
  19.6 0.7 copy-start.7
  20.3 32.2 %collective-permute-start.3 = (bf16[512,512]{1,0:T(8,128)(2,1)}, bf16[512,512]{1,0:T(8,128)(2,1)S(1)}, u32[]{:S(2)}, u32[]{:S(2)}) collective-permute-start(bf16[512,512]{1,0:T(8,128)(2,1)} %get-tuple-element.20.kv_mine), channel_id=1, source_target_pairs={{0,4},{2,6},{4,8},{6,10},{8,12},{10,14},{1,5},{3,7},{5,9},{7,11},{... | collective-permute-start | bytes 1572872 | tf_op jit(solution)/shard_map/ppermute | solution.py:596
  29.2 23.3 %collective-permute-start.4 = (bf16[512,512]{1,0:T(8,128)(2,1)}, bf16[512,512]{1,0:T(8,128)(2,1)S(1)}, u32[]{:S(2)}, u32[]{:S(2)}) collective-permute-start(bf16[512,512]{1,0:T(8,128)(2,1)} %collective-permute-done.2.kv_part), channel_id=1, source_target_pairs={{0,4},{2,6},{4,8},{6,10},{8,12},{10,14},{1,5},{3,7},{5,9},{7,11},{... | collective-permute-start | bytes 1572872 | tf_op jit(solution)/shard_map/ppermute | solution.py:599
  33.2 19.2 %collective-permute-start.5 = (bf16[512,256]{1,0:T(8,128)(2,1)}, bf16[512,256]{1,0:T(8,128)(2,1)S(1)}, u32[]{:S(2)}, u32[]{:S(2)}) collective-permute-start(bf16[512,256]{1,0:T(8,128)(2,1)} %copy-done.7), channel_id=1, source_target_pairs={{4,0},{6,2},{8,4},{10,6},{12,8},{14,10},{5,1},{7,3},{9,5},{11,7},{... | collective-permute-start | bytes 786440 | tf_op jit(solution)/shard_map/ppermute | solution.py:598
  34.5 17.9 %collective-permute-start.6 = (bf16[512,256]{1,0:T(8,128)(2,1)S(1)}, bf16[512,256]{1,0:T(8,128)(2,1)S(1)}, u32[]{:S(2)}, u32[]{:S(2)}) collective-permute-start(bf16[512,256]{1,0:T(8,128)(2,1)S(1)} %collective-permute-done.1.q_part), channel_id=1, source_target_pairs={{4,0},{6,2},{8,4},{10,6},{12,8},{14,10},{5,1},{7,3},{9,5},{11,7},{... | collective-permute-start | bytes 786440 | tf_op jit(solution)/shard_map/ppermute | solution.py:600
  35.8 1.0 %copy-start.8 = (bf16[512,256]{1,0:T(8,128)(2,1)S(1)}, bf16[512,256]{1,0:T(8,128)(2,1)}, u32[]{:S(2)}) copy-start(bf16[512,256]{1,0:T(8,128)(2,1)} %copy-done.7) | copy-start | bytes 786436
  52.4 12.1 %copy-start.9 = (bf16[512,256]{1,0:T(8,128)(2,1)S(1)}, bf16[512,256]{1,0:T(8,128)(2,1)}, u32[]{:S(2)}) copy-start(bf16[512,256]{1,0:T(8,128)(2,1)} %copy-done.7) | copy-start | bytes 786436
  55.2 23.8 %collective-permute-start.8 = (bf16[544,256]{1,0:T(8,128)(2,1)S(1)}, bf16[544,256]{1,0:T(8,128)(2,1)S(1)}, u32[]{:S(2)}, u32[]{:S(2)}) collective-permute-start(bf16[544,256]{1,0:T(8,128)(2,1)S(1)} %get-tuple-element.30), channel_id=1, source_target_pairs={{0,4},{2,6},{4,8},{6,10},{8,12},{10,14},{1,5},{3,7},{5,9},{7,11},{... | collective-permute-start | bytes 835592 | tf_op jit(solution)/shard_map/ppermute | solution.py:604
  60.4 21.7 %collective-permute-start.7 = (bf16[544,256]{1,0:T(8,128)(2,1)S(1)}, bf16[544,256]{1,0:T(8,128)(2,1)S(1)}, u32[]{:S(2)}, u32[]{:S(2)}) collective-permute-start(bf16[544,256]{1,0:T(8,128)(2,1)S(1)} %get-tuple-element.28), channel_id=1, source_target_pairs={{0,4},{2,6},{4,8},{6,10},{8,12},{10,14},{1,5},{3,7},{5,9},{7,11},{... | collective-permute-start | bytes 835592 | tf_op jit(solution)/shard_map/ppermute | solution.py:605
  80.5 8.4 %copy-start.6 = (bf16[512,2048]{1,0:T(8,128)(2,1)S(1)}, bf16[512,2048]{1,0:T(8,128)(2,1)}, u32[]{:S(2)}) copy-start(bf16[512,2048]{1,0:T(8,128)(2,1)} %w_mine.1) | copy-start | bytes 6291460
  80.5 8.4 %collective-permute-start.9 = (bf16[288,256]{1,0:T(8,128)(2,1)S(1)}, bf16[288,256]{1,0:T(8,128)(2,1)S(1)}, u32[]{:S(2)}, u32[]{:S(2)}) collective-permute-start(bf16[288,256]{1,0:T(8,128)(2,1)S(1)} %get-tuple-element.31), channel_id=1, source_target_pairs={{0,2},{2,0},{4,6},{6,4},{8,10},{10,8},{12,14},{14,12},{1,3},{3,1},... | collective-permute-start | bytes 442376 | tf_op jit(solution)/shard_map/ppermute | solution.py:608
  83.6 1.4 %collective-permute-start.10 = (bf16[256,256]{1,0:T(8,128)(2,1)S(1)}, bf16[256,256]{1,0:T(8,128)(2,1)S(1)}, u32[]{:S(2)}, u32[]{:S(2)}) collective-permute-start(bf16[256,256]{1,0:T(8,128)(2,1)S(1)} %get-tuple-element.32), channel_id=1, source_target_pairs={{0,1},{1,0},{2,3},{3,2},{4,5},{5,4},{6,7},{7,6},{8,9},{9,8},{10,11... | collective-permute-start | bytes 393224 | tf_op jit(solution)/shard_map/ppermute | solution.py:611
  83.7 5.2 %collective-permute-start.11 = (bf16[256,256]{1,0:T(8,128)(2,1)S(1)}, bf16[256,256]{1,0:T(8,128)(2,1)S(1)}, u32[]{:S(2)}, u32[]{:S(2)}) collective-permute-start(bf16[256,256]{1,0:T(8,128)(2,1)S(1)} %get-tuple-element.33), channel_id=1, source_target_pairs={{0,3},{1,2},{2,1},{3,0},{4,7},{5,6},{6,5},{7,4},{8,11},{9,10},{10,... | collective-permute-start | bytes 393224 | tf_op jit(solution)/shard_map/ppermute | solution.py:609

commit v3 on v0

v3 whole, which is shorter than its diff:
```python
import functools
import math

import jax
import jax.numpy as jnp
from jax import lax
from jax.experimental import pallas as pl
from jax.experimental.pallas import tpu as pltpu
from jax.sharding import PartitionSpec as P


HEADS = 16
HEAD_DIM = 64
WINDOW_KEY_STEPS = 128
MIDDLE_DILATION = 4
FAR_DILATION = 16
REACH = 2048
ALIBI_EXP = 16.0

LOG2E = math.log2(math.e)
LN2 = math.log(2.0)
MASKED = -1e30
FLOOR = -1e25
F32 = jnp.float32
BF16 = jnp.bfloat16
ANY = pl.BlockSpec(memory_space=pl.ANY)
VMEM = pl.BlockSpec(memory_space=pltpu.VMEM)
MIB = 1024 * 1024


def params(limit):
    return pltpu.CompilerParams(vmem_limit_bytes=limit * MIB)


SUB = 16


def aligned(value, multiple):
    return value if isinstance(value, int) else pl.multiple_of(value, multiple)


def places():
    place = lax.axis_index("sp")
    return place % 2, place // 2, lax.axis_index("tp")


def call(kernel, results, inputs, scratch=(), limit=12, flops=10**9, loose=0):
    return pl.pallas_call(
        kernel,
        out_shape=[jax.ShapeDtypeStruct(shape, kind) for shape, kind in results],
        in_specs=[VMEM] * (len(inputs) - loose) + [ANY] * loose,
        out_specs=[VMEM] * len(results),
        scratch_shapes=list(scratch),
        compiler_params=params(limit),
        cost_estimate=pl.CostEstimate(flops=flops, bytes_accessed=10**6, transcendentals=0),
    )(*inputs)


def project_kernel(first, weights, *refs):
    x_own, x_other = refs[:2]
    ws = refs[2 : 2 + weights]
    outs, acc = refs[2 + weights : -1], refs[-1]
    y, _, tp = places()
    rows = x_own.shape[0]
    slot = 0
    for w in ws:
        for start in first:
            for half, x in enumerate((x_own, x_other)):
                result = jnp.dot(x[...], w[:, start : start + 256], preferred_element_type=F32)
                acc[slot, 0], acc[slot, 1] = result[:, :128], result[:, 128:]
                place = (tp if half == 0 else 1 - tp) * rows
                index = slot // 2 if len(first) > 1 or weights > 1 else 0
                for side, out in enumerate(outs):
                    source = 1 - y if side == 0 else y
                    for residue in range(FAR_DILATION):
                        chunk = acc[slot, source, pl.ds(residue, SUB, stride=FAR_DILATION), :].astype(BF16)
                        where = pl.ds(aligned(place + residue * SUB, SUB), SUB)
                        out[where, index * 128 : (index + 1) * 128] = chunk
                slot += 1


def project(x_own, x_other, weights, first):
    rows, width = x_own.shape
    shape = ((2 * rows, 256), BF16)
    slots = 2 * len(first) * len(weights)
    return call(
        functools.partial(project_kernel, first, len(weights)),
        [shape, shape],
        [x_own, x_other, *weights],
        [pltpu.VMEM((slots, 2, rows, 128), F32)],
        limit=10,
        flops=2 * slots * rows * width * 256,
    )


def attend(queries, keys, values, bias):
    rows = queries.shape[0]
    low = lax.broadcasted_iota(jnp.int32, (rows, 128), 1) < HEAD_DIM
    zero = jnp.zeros_like(queries)
    stacked = jnp.concatenate([jnp.where(low, queries, zero), jnp.where(low, zero, queries)], axis=0)
    scores = lax.dot_general(
        stacked, keys, (((1,), (1,)), ((), ())), preferred_element_type=F32
    )
    scores = scores * (HEAD_DIM**-0.5 * LOG2E) + bias
    maxima = jnp.maximum(jnp.max(scores, axis=1, keepdims=True), FLOOR)
    weights = jnp.exp2(scores - maxima)
    totals = jnp.sum(weights, axis=1, keepdims=True)
    summed = jnp.dot(weights.astype(BF16), values, preferred_element_type=F32)
    pick = lambda item: jnp.where(low, item[:rows], item[rows:])
    return pick(summed), pick(maxima), pick(totals)


def merge(first, second):
    o1, m1, l1 = first
    o2, m2, l2 = second
    top = jnp.maximum(m1, m2)
    a, b = jnp.exp2(m1 - top), jnp.exp2(m2 - top)
    return o1 * a + o2 * b, top, l1 * a + l2 * b


def near_distance(keys_before, keys_own):
    tile = FAR_DILATION * SUB
    token = lambda n: FAR_DILATION * (n % SUB) + n // SUB
    shape = (tile, (tile if keys_before else 0) + (tile if keys_own else 0))
    row = token(lax.broadcasted_iota(jnp.int32, shape, 0))
    col = lax.broadcasted_iota(jnp.int32, shape, 1)
    if keys_before:
        key = jnp.where(col < tile, token(col) - tile, token(col - tile))
    else:
        key = token(col)
    return row - key


def middle_distance(keys_before, keys_own, chunks):
    group = FAR_DILATION // MIDDLE_DILATION
    size = chunks * group * SUB
    step = lambda n: (n // (group * SUB)) * (group * SUB) + group * (n % SUB) + (n // SUB) % group
    shape = (size, (size if keys_before else 0) + (size if keys_own else 0))
    row = step(lax.broadcasted_iota(jnp.int32, shape, 0))
    col = lax.broadcasted_iota(jnp.int32, shape, 1)
    if keys_before:
        key = jnp.where(col < size, step(col) - size, step(col - size))
    else:
        key = step(col)
    return row - key


def bias_of(distance, slope, stride):
    allowed = (distance >= 0) & (distance <= WINDOW_KEY_STEPS)
    return jnp.where(allowed, distance.astype(F32) * (slope * (-float(stride))), MASKED)


def rows_of(ref, starts, lanes):
    return jnp.concatenate([ref[pl.ds(aligned(s, SUB), SUB), lanes] for s in starts], axis=0)


def middle_starts(block, residue, chunks):
    tile = FAR_DILATION * SUB
    group = FAR_DILATION // MIDDLE_DILATION
    return [
        (block * chunks + s) * tile + (residue + MIDDLE_DILATION * b) * SUB
        for s in range(chunks)
        for b in range(group)
    ]


def far_starts(residue, chunks):
    return [g * FAR_DILATION * SUB + residue * SUB for g in range(chunks)]


def fold_in(refs, starts, lanes, new):
    size = SUB
    for n, start in enumerate(starts):
        where = (pl.ds(aligned(start, SUB), size), lanes)
        old = tuple(ref[where] for ref in refs)
        piece = tuple(item[n * size : (n + 1) * size] for item in new)
        for ref, value in zip(refs, merge(old, piece)):
            ref[where] = value


def pair_lanes(pair, offset=0):
    return slice(offset + pair * 128, offset + (pair + 1) * 128)


def bias_kernel(near, mid, far):
    heads = near.shape[0]
    y, _, tp = places()
    tile = FAR_DILATION * SUB
    chunks = mid.shape[1] // (tile // MIDDLE_DILATION)
    near_steps = near_distance(True, True)
    mid_steps = middle_distance(True, True, chunks)
    row = lax.broadcasted_iota(jnp.int32, far.shape[2:], 0)
    col = lax.broadcasted_iota(jnp.int32, far.shape[2:], 1)
    far_slope = lambda head, shape: jnp.exp2(
        jnp.full(shape, -ALIBI_EXP / HEADS, F32)
        * (tp * 2 * heads + (head // 2) * 4 + y * 2 + head % 2 + 1).astype(F32)
    ) * LOG2E
    for head in range(heads):
        slope = far_slope(head, (1, 1))
        near[head] = bias_of(near_steps, slope, 1)
        mid[head] = bias_of(mid_steps, slope, MIDDLE_DILATION)
        for back in range(3):
            far[back, head] = bias_of(row - col + back * far.shape[3], slope, FAR_DILATION)


def biases(block, heads):
    tile = FAR_DILATION * SUB
    size = block // MIDDLE_DILATION
    reach = 2 * block // FAR_DILATION
    return call(
        bias_kernel,
        [((heads, tile, 2 * tile), F32), ((heads, size, 2 * size), F32), ((3, heads, reach, reach), F32)],
        [],
        limit=8,
        flops=10**9,
        loose=0,
    )


def stacked(ref, pair, rows, columns, extra=None):
    both = jnp.concatenate([ref[2 * pair, rows, columns], ref[2 * pair + 1, rows, columns]], axis=0)
    return both if extra is None else both + extra


def closed_gate():
    _, z, _ = places()
    return jnp.where(z > 0, 0.0, MASKED).astype(F32)


def place_pair(target, mine, part):
    y, _, _ = places()
    block = mine.shape[0]
    target[pl.ds(aligned(y * block, block), block)] = mine[...]
    target[pl.ds(aligned((1 - y) * block, block), block)] = part[...]


KEYS, VALUES = slice(0, 128), slice(128, 256)


def block_kernel(near, mid, q, kv0, kv1, *rest):
    o_ref, m_ref, l_ref = rest[-3:]
    block = q.shape[0]
    tile = FAR_DILATION * SUB
    chunks = block // tile
    refs = (o_ref, m_ref, l_ref)
    step = 64
    size = mid.shape[1]
    for pair, kv in enumerate((kv0, kv1)):
        for index in range(chunks):
            first = max(index - 1, 0) * tile
            width = tile if index == 0 else 2 * tile
            columns = slice(2 * tile - width, 2 * tile)
            for inner in range(tile // step):
                start = index * tile + inner * step
                result = attend(
                    q[start : start + step, pair_lanes(pair)],
                    kv[first : first + width, KEYS],
                    kv[first : first + width, VALUES],
                    stacked(near, pair, slice(inner * step, (inner + 1) * step), columns),
                )
                for ref, value in zip(refs, result):
                    ref[start : start + step, pair_lanes(pair)] = value
        for residue in range(MIDDLE_DILATION):
            starts = middle_starts(0, residue, chunks)
            result = attend(
                rows_of(q, starts, pair_lanes(pair)),
                rows_of(kv, starts, KEYS),
                rows_of(kv, starts, VALUES),
                stacked(mid, pair, slice(0, size), slice(size, 2 * size)),
            )
            fold_in(refs, starts, pair_lanes(pair), result)


def block_attention(bias, q, kv0, kv1, after=()):
    return call(
        block_kernel,
        [(q.shape, F32)] * 3,
        [bias[0], bias[1], q, kv0, kv1, *after],
        limit=10,
        flops=4 * 10**9,
        loose=len(after),
    )


def windows(refs, q, kvs, near, mid, far, before, closed):
    block = q.shape[0] // 2
    tile = FAR_DILATION * SUB
    chunks = block // tile
    back = 1 if before else 0
    query_tile = 0 if before else chunks
    key_tile = (2 * chunks - 1 if before else chunks - 1) * tile
    step = 64
    size = mid.shape[1]
    for pair in range(len(kvs)):
        kv = kvs[pair]
        for residue in range(FAR_DILATION):
            starts = far_starts(residue, 2 * chunks)
            result = attend(
                rows_of(q, starts, pair_lanes(pair)),
                rows_of(kv, starts, KEYS),
                rows_of(kv, starts, VALUES),
                jnp.concatenate([far[back, 2 * pair], far[back, 2 * pair + 1]], axis=0) + closed,
            )
            fold_in(refs, starts, pair_lanes(pair), result)
        for inner in range(tile // step):
            start = query_tile * tile + inner * step
            result = attend(
                q[start : start + step, pair_lanes(pair)],
                kv[key_tile : key_tile + tile, KEYS],
                kv[key_tile : key_tile + tile, VALUES],
                stacked(near, pair, slice(inner * step, (inner + 1) * step), slice(0, tile), closed),
            )
            where = (slice(start, start + step), pair_lanes(pair))
            old = tuple(ref[where] for ref in refs)
            for ref, value in zip(refs, merge(old, result)):
                ref[where] = value
        for residue in range(MIDDLE_DILATION):
            starts = middle_starts(0 if before else 1, residue, chunks)
            key_starts = middle_starts(1 if before else 0, residue, chunks)
            result = attend(
                rows_of(q, starts, pair_lanes(pair)),
                rows_of(kv, key_starts, KEYS),
                rows_of(kv, key_starts, VALUES),
                stacked(mid, pair, slice(0, size), slice(0, size), closed),
            )
            fold_in(refs, starts, pair_lanes(pair), result)


def pair_kernel(near, mid, far, q_mine, q_part, *rest):
    kv_mine, kv_part, mine, part = rest[:2], rest[2:4], rest[4:7], rest[7:10]
    *refs, q_ref, kv = rest[-5:]
    place_pair(q_ref, q_mine, q_part)
    for n in range(2):
        place_pair(kv.at[n], kv_mine[n], kv_part[n])
    for ref, first, second in zip(refs, mine, part):
        place_pair(ref, first, second)
    windows(refs, q_ref, [kv.at[0], kv.at[1]], near, mid, far, False, 0.0)


def pair_attention(bias, q_mine, q_part, kv_mine, kv_part, mine, part, after=()):
    block, lanes = q_mine.shape
    return call(
        pair_kernel,
        [((2 * block, lanes), F32)] * 3 + [((2 * block, lanes), BF16)],
        [*bias, q_mine, q_part, *kv_mine, *kv_part, *mine, *part, *after],
        [pltpu.VMEM((2, 2 * block, 256), BF16)],
        limit=16,
        flops=4 * 10**9,
        loose=len(after),
    )


def before_kernel(near, mid, far, q, kv_a0, kv_b0, kv_a1, kv_b1, o_in, m_in, l_in, *rest):
    o_ref, m_ref, l_ref, past = rest[-4:]
    place_pair(past.at[0], kv_a0, kv_b0)
    place_pair(past.at[1], kv_a1, kv_b1)
    o_ref[...], m_ref[...], l_ref[...] = o_in[...], m_in[...], l_in[...]
    windows((o_ref, m_ref, l_ref), q, [past.at[0], past.at[1]], near, mid, far, True, closed_gate())


def before_attention(bias, q, past, state, after=()):
    return call(
        before_kernel,
        [(q.shape, F32)] * 3,
        [*bias, q, *past, *state, *after],
        [pltpu.VMEM((2, q.shape[0], 256), BF16)],
        limit=16,
        flops=4 * 10**9,
        loose=len(after),
    )


def part_row(shape, block):
    row = lax.broadcasted_iota(jnp.int32, shape, 0) - 8 * block
    lane = lax.broadcasted_iota(jnp.int32, shape, 1)
    return row, lane


def pack_sums(blocks):
    total = 0.0
    for n, sums in enumerate(blocks):
        row, lane = part_row((16, 128), n)
        for part in range(3):
            piece = sums.astype(BF16)
            sums = sums - piece.astype(F32)
            pick = (row // 2 == part) & (row >= 0) & (lane == (row % 2) * HEAD_DIM)
            total = total + lax.dot_general(
                jnp.where(pick, 1.0, 0.0).astype(BF16), piece, (((1,), (1,)), ((), ())), preferred_element_type=F32
            )
    return total.astype(BF16)


def unpack_sums(packed, block):
    row, lane = part_row((16, 128), block)
    pick = (row >= 0) & (row < 6) & (lane // HEAD_DIM == row % 2)
    return lax.dot_general(
        packed, jnp.where(pick, 1.0, 0.0).astype(BF16), (((0,), (0,)), ((), ())), preferred_element_type=F32
    )


def store_packed(ref, first, packed):
    for n in range(packed.shape[1] // 128):
        ref[first + 16 * n : first + 16 * (n + 1)] = packed[:, n * 128 : (n + 1) * 128]


def load_packed(ref, first, count):
    return jnp.concatenate([ref[first + 16 * n : first + 16 * (n + 1)] for n in range(count)], axis=1)


def remote_kernel(pair, far, q_a, q_b, kv_a, kv_b, *rest):
    out_ref, q, kv, sums = rest[-4:]
    block = q_a.shape[0]
    tile = FAR_DILATION * SUB
    chunks = block // tile
    place_pair(q, q_a.at[:, pair_lanes(pair)], q_b.at[:, pair_lanes(pair)])
    place_pair(kv, kv_a, kv_b)
    closed = closed_gate()
    bias = jnp.concatenate([far[2, 2 * pair], far[2, 2 * pair + 1]], axis=0) + closed
    for residue in range(FAR_DILATION):
        starts = far_starts(residue, 2 * chunks)
        o, m, l = attend(rows_of(q, starts, KEYS), rows_of(kv, starts, KEYS), rows_of(kv, starts, VALUES), bias)
        some = l > 0.0
        safe = jnp.where(some, l, 1.0)
        o = o / safe
        s = jnp.where(some, m + jnp.log2(safe), FLOOR)
        for n, start in enumerate(starts):
            where = pl.ds(start, SUB)
            out_ref[where] = o[n * SUB : (n + 1) * SUB].astype(BF16)
            sums[where] = s[n * SUB : (n + 1) * SUB]
    store_packed(out_ref, 2 * block, pack_sums([sums[:block], sums[block:]]))


def remote_attention(pair, far, q_a, q_b, kv_a, kv_b, after=()):
    block = q_a.shape[0]
    return call(
        functools.partial(remote_kernel, pair),
        [((2 * block + 16 * (block // 128), 128), BF16)],
        [far, q_a, q_b, kv_a, kv_b, *after],
        [pltpu.VMEM((2 * block, 128), BF16), pltpu.VMEM((2 * block, 256), BF16), pltpu.VMEM((2 * block, 128), F32)],
        limit=8,
        flops=10**9,
        loose=len(after),
    )[0]


def finish_kernel(pair, o_in, m_in, l_in, far_in, *rest):
    stay_ref, go_ref, same_ref, cross_ref, sums_ref, o_s, turned = rest[-7:]
    y, _, tp = places()
    rows = o_in.shape[0]
    block = rows // 2
    half = block // 2
    tile = FAR_DILATION * SUB
    lanes = pair_lanes(pair)
    closed = closed_gate()
    packed = load_packed(far_in, rows, block // 128)
    for b in range(2):
        far_sums = unpack_sums(packed, b) + closed
        select = slice(b * block, (b + 1) * block)
        o, m, l = merge(
            (o_in[select, lanes], m_in[select, lanes], l_in[select, lanes]),
            (far_in[select].astype(F32), far_sums, jnp.ones_like(far_sums)),
        )
        o_s[0, select] = o / l
        o_s[1, select] = (m + jnp.log2(l)) * LN2
    for item in range(2):
        for s in range(rows // tile):
            for residue in range(FAR_DILATION):
                turned[item, pl.ds(s * tile + residue, SUB, stride=FAR_DILATION), :] = o_s[
                    item, s * tile + residue * SUB : s * tile + (residue + 1) * SUB
                ]
    own, other = y * block, (1 - y) * block
    for ref, start in (
        (stay_ref, own + tp * half),
        (go_ref, own + (1 - tp) * half),
        (same_ref, other + tp * half),
        (cross_ref, other + (1 - tp) * half),
    ):
        ref[:half] = turned[0, pl.ds(aligned(start, half), half), :].astype(BF16)
    sums_ref[...] = pack_sums([turned[1, pl.ds(aligned(own, block), block), :]])
    store_packed(same_ref, half, pack_sums([turned[1, pl.ds(aligned(other, block), block), :]]))


def finish(pair, state, far, after=()):
    rows = state[0].shape[0]
    block, half = rows // 2, rows // 4
    piece = ((half, 128), BF16)
    return call(
        functools.partial(finish_kernel, pair),
        [piece, piece, ((half + 16 * (block // 128), 128), BF16), piece, ((16, block), BF16)],
        [*state, far, *after],
        [pltpu.VMEM((2, rows, 128), F32), pltpu.VMEM((2, rows, 128), F32)],
        limit=8,
        flops=10**9,
        loose=len(after),
    )


def output_kernel(*refs):
    pieces, (w_mine, w_other, out_ref, sums_ref) = (refs[:5], refs[5:10]), refs[10:]
    y, _, _ = places()
    half, width = out_ref.shape
    block = 2 * half
    low = y == 0
    order = lambda mine, part: (jnp.where(low, mine, part), jnp.where(low, part, mine))
    hidden = []
    for first, second in ((0, 1), (2, 3)):
        blocks = []
        for piece in pieces:
            blocks += order(piece[first][:half], piece[second][:half])
        hidden.append(jnp.concatenate(blocks, axis=1))
    step = 512
    for start in range(0, width, step):
        columns = slice(start, start + step)
        first = jnp.dot(hidden[0], w_mine[:, columns], preferred_element_type=F32)
        second = jnp.dot(hidden[1], w_other[:, columns], preferred_element_type=F32)
        out_ref[:, columns] = (first.astype(BF16).astype(F32) + second.astype(BF16).astype(F32)).astype(BF16)
    heads = []
    for piece in pieces:
        sums = []
        for packed in (piece[4][...], load_packed(piece[1], half, block // 128)):
            packed = packed.astype(F32)
            sums.append(packed[0:2] + packed[2:4] + packed[4:6])
        heads += order(*sums)
    sums_ref[...] = jnp.concatenate(heads, axis=0)


def output(pieces, w_mine, w_other):
    half = pieces[0][0].shape[0]
    width = w_mine.shape[1]
    return call(
        output_kernel,
        [((half, width), BF16), ((8, 2 * half), F32)],
        [*pieces[0], *pieces[1], w_mine, w_other],
        limit=12,
        flops=2 * half * width * 1024,
    )


def layer(tokens, w_query, w_key, w_value, w_out):
    half, _ = tokens.shape
    block = 2 * half
    width = w_query.shape[1]
    heads = width // 2 // HEAD_DIM
    count = lax.axis_size("sp")
    assert lax.axis_size("tp") == 2 and count % 2 == 0
    assert REACH == 4 * block and half == FAR_DILATION * SUB and width == 512
    ahead = [(n, (n + 2) % count) for n in range(count)]
    back = [(n + 2, n) for n in range(count - 2)]
    beside = [(n, n ^ 1) for n in range(count)]
    swap = [(0, 1), (1, 0)]
    crossed = [(2 * n + c, 2 * (n ^ 1) + 1 - c) for n in range(count) for c in range(2)]

    x_other = lax.ppermute(tokens, "tp", swap)
    kv_t0, kv_m0 = project(tokens, x_other, [w_key, w_value], [0])
    kv_p0 = lax.ppermute(kv_t0, "sp", beside)
    kv_a0 = lax.ppermute(kv_m0, "sp", ahead)
    q_t, q_m = project(tokens, x_other, [w_query], [0, 256])
    q_p = lax.ppermute(q_t, "sp", beside)
    q_a = lax.ppermute(q_m, "sp", back)
    kv_t1, kv_m1 = project(tokens, x_other, [w_key, w_value], [256])
    kv_p1 = lax.ppermute(kv_t1, "sp", beside)
    kv_a1 = lax.ppermute(kv_m1, "sp", ahead)
    kv_b0 = lax.ppermute(kv_p0, "sp", ahead)
    q_b = lax.ppermute(q_p, "sp", back)
    kv_b1 = lax.ppermute(kv_p1, "sp", ahead)
    w_other = lax.ppermute(w_out, "tp", swap)
    bias = biases(block, heads)
    mine = block_attention(bias, q_m, kv_m0, kv_m1)
    part = block_attention(bias, q_p, kv_p0, kv_p1, mine[:1])
    far0 = remote_attention(0, bias[2], q_a, q_b, kv_a0, kv_b0)
    far_p = lax.ppermute(far0, "sp", ahead)
    *state, q = pair_attention(bias, q_m, q_p, (kv_m0, kv_m1), (kv_p0, kv_p1), mine, part)
    far1 = remote_attention(1, bias[2], q_a, q_b, kv_a1, kv_b1)
    far_m = lax.ppermute(far1, "sp", ahead)
    state = before_attention(bias, q, (kv_a0, kv_b0, kv_a1, kv_b1), state)
    pieces = []
    for pair, far in enumerate((far_p, far_m)):
        stay, go, same, cross, sums = finish(pair, state, far)
        same = lax.ppermute(same, "sp", beside)
        cross = lax.ppermute(cross, ("sp", "tp"), crossed)
        go = lax.ppermute(go, "tp", swap)
        pieces.append((stay, same, go, cross, sums))
    return output(pieces, w_out, w_other)


def solution(mesh):
    in_specs = (
        P(("grp", "sp", "tp"), None),
        P(None, "tp"),
        P(None, "tp"),
        P(None, "tp"),
        P("tp", None),
    )
    out_specs = (P(("grp", "sp", "tp"), None), P("tp", ("grp", "sp")))
    return jax.shard_map(layer, mesh=mesh, in_specs=in_specs, out_specs=out_specs, check_vma=False)
```

time: 259 us -> 77.7 us (0.30)
  local copies, waits for them, and re-layouts: 87.4 us -> 0.02 us
  waiting for transfers between devices: 89.4 us -> 29.8 us
  matrix products: 32.9 us -> 0 us
  Pallas kernels: 0 us -> 26.3 us
  between operations: 14.5 us -> 0.78 us
  other arithmetic: 12.2 us -> 0 us
    ppermute x4 -> x19, waiting for transfers between devices: 68 us -> 29.8 us  [the longest x1 6.52 us: layer(): kv_b1 = lax.ppermute(kv_p1, 'sp', ahead)]
    dot_general x10 -> x0, matrix products: 32.9 us -> none  [the longest x3 11.9 us: dilated_attention(): jnp.einsum('hrbqk,hbkre->hbqre', weights.astype(jnp.bfloat16), spans[1],...]
    unnamed x61 -> x10, local copies, waits for them, and re-layouts: 28.1 us -> 0.02 us
    pallas_call x0 -> x13, Pallas kernels: none -> 26.3 us  [call(): pl.pallas_call(kernel, out_shape=[jax.ShapeDtypeStruct(shape, kind) for s...]
    slice x4 -> x0, local copies, waits for them, and re-layouts: 19.6 us -> none  [the longest x3 13.7 us: dilated_attention(): spans[1]]
    reduce_scatter x1 -> x0, waiting for transfers between devices: 13.8 us -> none  [body(): lax.psum_scatter(jnp.dot(hidden, w_out, preferred_element_type=jnp.float3...]
    concatenate x1 -> x0, local copies, waits for them, and re-layouts: 12.2 us -> none  [body(): window_rows = jnp.concatenate(pieces, axis=2)]
    reshape x3 -> x0, local copies, waits for them, and re-layouts: 9.04 us -> none  [dilated_attention(): outputs = outputs.reshape(heads, length, depth)]
  transfers between devices with their start and end apart: 6 -> 19, of which waited for: 6 -> 10; matrix products, arithmetic and copies ran while one was open for 9% -> 0% of each run, Pallas kernels for 0% -> 31%
where the time goes in v3:
time: 77.7 us; the launch traced here: 77.5 us
  waiting for transfers between devices  29.8 us (38%)
  Pallas kernels  26.3 us (34%)
  starting transfers between devices  20.6 us (27%)
  between operations  0.78 us (1%)
    pallas_call x13, Pallas kernels, call(): pl.pallas_call(kernel, out_shape=[jax.ShapeDtypeStruct(shape, kind) for s...  26.3 us
    ppermute x1, waiting for transfers between devices, layer(): kv_b1 = lax.ppermute(kv_p1, 'sp', ahead)  6.52 us
    ppermute x1, waiting for transfers between devices, layer(): far_m = lax.ppermute(far1, 'sp', ahead)  5.85 us
    ppermute x1, waiting for transfers between devices, layer(): q_b = lax.ppermute(q_p, 'sp', back)  4.26 us
    ppermute x1, waiting for transfers between devices, layer(): kv_p1 = lax.ppermute(kv_t1, 'sp', beside)  3.78 us
    ppermute x2, starting transfers between devices, layer(): cross = lax.ppermute(cross, ('sp', 'tp'), crossed)  3.21 us
    ppermute x1, starting transfers between devices, layer(): q_p = lax.ppermute(q_t, 'sp', beside)  2.94 us
    ppermute x2, waiting for transfers between devices, layer(): cross = lax.ppermute(cross, ('sp', 'tp'), crossed)  2.86 us
  transfers between devices with their start and end apart: 19, of which 10 were waited for; matrix products, arithmetic and copies ran while one was open for 0% of the time, Pallas kernels for 31%

profile of v3, /device:TPU:0, one launch (start us, length us, event | category | flops | bytes accessed | tf_op | source)
XLA Modules:
  0.0 77.5 jit_solution(6126156409607153114)
XLA Ops:
  0.6 0.6 collective-permute-start
  1.2 0.1 collective-permute-start.18
  1.3 0.5 shard_map.68
  1.8 0.0 copy-start.1
  1.8 0.0 copy-start.2
  1.8 1.9 %collective-permute-done.refs_1_ = bf16[256,2048]{1,0:T(8,128)(2,1)S(1)} collective-permute-done((bf16[256,2048]{1,0:T(8,128)(2,1)}, bf16[256,2048]{1,0:T(8,128)(2,1)S(1)}, u32[]{:S(2)}, u32[]{:S(2)}) %collective-permute-start) | collective-permute-done | bytes 1048608 | tf_op jit(solution)/shard_map/ppermute | solution.py:553
  3.7 1.7 %shard_map.69 = (bf16[512,256]{1,0:T(8,128)(2,1)S(1)}, bf16[512,256]{1,0:T(8,128)(2,1)S(1)}) custom-call(bf16[256,2048]{1,0:T(8,128)(2,1)S(1)} %copy-done, bf16[256,2048]{1,0:T(8,128)(2,1)S(1)} %collective-permute-done.refs_1_, bf16[2048,512]{1,0:T(8,128)(2,1)S(1)} %copy-done.4), custom_call_target="tpu_custom_call" | custom-call | flops 1073741824 | bytes 1000000 | tf_op jit(solution)/shard_map/pallas_call | solution.py:48
  5.4 2.9 %collective-permute-start.1 = (bf16[512,256]{1,0:T(8,128)(2,1)S(1)}, bf16[512,256]{1,0:T(8,128)(2,1)S(1)}, u32[]{:S(2)}, u32[]{:S(2)}) collective-permute-start(bf16[512,256]{1,0:T(8,128)(2,1)S(1)} %get-tuple-element.38), channel_id=1, source_target_pairs={{0,2},{2,0},{4,6},{6,4},{8,10},{10,8},{12,14},{14,12},{1,3},{3,1},... | collective-permute-start | bytes 786440 | tf_op jit(solution)/shard_map/ppermute | solution.py:558
  8.3 1.7 %shard_map.70 = (bf16[512,256]{1,0:T(8,128)(2,1)S(1)}, bf16[512,256]{1,0:T(8,128)(2,1)S(1)}) custom-call(bf16[256,2048]{1,0:T(8,128)(2,1)S(1)} %copy-done, bf16[256,2048]{1,0:T(8,128)(2,1)S(1)} %collective-permute-done.refs_1_, bf16[2048,512]{1,0:T(8,128)(2,1)S(1)} %copy-done.1, bf16[2048,512]{1,0:T(8,128)(2,1)S(1)} %copy-done.2), custom_call_target="tpu_custom_call" | custom-call | flops 1073741824 | bytes 1000000 | tf_op jit(solution)/shard_map/pallas_call | solution.py:48
  10.0 0.1 collective-permute-start.2
  10.1 1.7 %shard_map.71 = (bf16[512,256]{1,0:T(8,128)(2,1)S(1)}, bf16[512,256]{1,0:T(8,128)(2,1)S(1)}) custom-call(bf16[256,2048]{1,0:T(8,128)(2,1)S(1)} %copy-done, bf16[256,2048]{1,0:T(8,128)(2,1)S(1)} %collective-permute-done.refs_1_, bf16[2048,512]{1,0:T(8,128)(2,1)S(1)} %copy-done.1, bf16[2048,512]{1,0:T(8,128)(2,1)S(1)} %copy-done.2), custom_call_target="tpu_custom_call" | custom-call | flops 1073741824 | bytes 1000000 | tf_op jit(solution)/shard_map/pallas_call | solution.py:48
  11.7 2.1 %collective-permute-start.3 = (bf16[512,256]{1,0:T(8,128)(2,1)S(1)}, bf16[512,256]{1,0:T(8,128)(2,1)S(1)}, u32[]{:S(2)}, u32[]{:S(2)}) collective-permute-start(bf16[512,256]{1,0:T(8,128)(2,1)S(1)} %get-tuple-element.42), channel_id=1, source_target_pairs={{0,2},{2,0},{4,6},{6,4},{8,10},{10,8},{12,14},{14,12},{1,3},{3,1},... | collective-permute-start | bytes 786440 | tf_op jit(solution)/shard_map/ppermute | solution.py:561
  13.8 1.6 %collective-permute-start.4 = (bf16[512,256]{1,0:T(8,128)(2,1)S(1)}, bf16[512,256]{1,0:T(8,128)(2,1)S(1)}, u32[]{:S(2)}, u32[]{:S(2)}) collective-permute-start(bf16[512,256]{1,0:T(8,128)(2,1)S(1)} %get-tuple-element.39.kv0.rest_0_), channel_id=1, source_target_pairs={{0,4},{2,6},{4,8},{6,10},{8,12},{10,14},{12,0},{14,2},{1,5},{3,7},... | collective-permute-start | bytes 786440 | tf_op jit(solution)/shard_map/ppermute | solution.py:556
  15.4 3.7 %shard_map.72 = (f32[512,256]{1,0:T(8,128)S(1)}, f32[512,256]{1,0:T(8,128)S(1)}, f32[512,256]{1,0:T(8,128)S(1)}) custom-call(f32[4,256,512]{2,1,0:T(8,128)S(1)} %get-tuple-element.34.near, f32[4,128,256]{2,1,0:T(8,128)S(1)} %get-tuple-element.35.mid, bf16[512,256]{1,0:T(8,128)(2,1)S(1)} %get-tuple-element.37.q.q_mine, ...), custom_call_target="tpu_custom_call" | custom-call | flops 4000000000 | bytes 1000000 | tf_op jit(solution)/shard_map/pallas_call | solution.py:48
  19.1 0.0 collective-permute-done.1.q.q_part
  19.1 1.6 %collective-permute-start.6 = (bf16[512,256]{1,0:T(8,128)(2,1)S(1)}, bf16[512,256]{1,0:T(8,128)(2,1)S(1)}, u32[]{:S(2)}, u32[]{:S(2)}) collective-permute-start(bf16[512,256]{1,0:T(8,128)(2,1)S(1)} %get-tuple-element.40.kv1.rest_1_), channel_id=1, source_target_pairs={{0,4},{2,6},{4,8},{6,10},{8,12},{10,14},{12,0},{14,2},{1,5},{3,7},... | collective-permute-start | bytes 786440 | tf_op jit(solution)/shard_map/ppermute | solution.py:562
  20.7 0.3 collective-permute-done.2.kv0.rest_2_
  21.1 1.3 %collective-permute-start.8 = (bf16[512,256]{1,0:T(8,128)(2,1)S(1)}, bf16[512,256]{1,0:T(8,128)(2,1)S(1)}, u32[]{:S(2)}, u32[]{:S(2)}) collective-permute-start(bf16[512,256]{1,0:T(8,128)(2,1)S(1)} %get-tuple-element.37.q.q_mine), channel_id=1, source_target_pairs={{4,0},{6,2},{8,4},{10,6},{12,8},{14,10},{5,1},{7,3},{9,5},{11,7},{... | collective-permute-start | bytes 786440 | tf_op jit(solution)/shard_map/ppermute | solution.py:559
  22.4 3.8 %collective-permute-done.3.kv1.rest_3_ = bf16[512,256]{1,0:T(8,128)(2,1)S(1)} collective-permute-done((bf16[512,256]{1,0:T(8,128)(2,1)S(1)}, bf16[512,256]{1,0:T(8,128)(2,1)S(1)}, u32[]{:S(2)}, u32[]{:S(2)}) %collective-permute-start.3) | collective-permute-done | bytes 262176 | tf_op jit(solution)/shard_map/ppermute | solution.py:561
  26.2 1.8 %collective-permute-start.5 = (bf16[512,256]{1,0:T(8,128)(2,1)S(1)}, bf16[512,256]{1,0:T(8,128)(2,1)S(1)}, u32[]{:S(2)}, u32[]{:S(2)}) collective-permute-start(bf16[512,256]{1,0:T(8,128)(2,1)S(1)} %collective-permute-done.2.kv0.rest_2_), channel_id=1, source_target_pairs={{0,4},{2,6},{4,8},{6,10},{8,12},{10,14},{12,0},{14,2},{1,5},{3,7},... | collective-permute-start | bytes 786440 | tf_op jit(solution)/shard_map/ppermute | solution.py:563
  28.0 3.7 %shard_map.73 = (f32[512,256]{1,0:T(8,128)S(1)}, f32[512,256]{1,0:T(8,128)S(1)}, f32[512,256]{1,0:T(8,128)S(1)}) custom-call(f32[4,256,512]{2,1,0:T(8,128)S(1)} %get-tuple-element.34.near, f32[4,128,256]{2,1,0:T(8,128)S(1)} %get-tuple-element.35.mid, bf16[512,256]{1,0:T(8,128)(2,1)S(1)} %collective-permute-done.1.q.q_part, ...), custom_call_target="tpu_custom_call" | custom-call | flops 4000000000 | bytes 1000000 | tf_op jit(solution)/shard_map/pallas_call | solution.py:48
  31.7 0.0 collective-permute-done.6.kv_a1.kv_a
  31.7 1.6 %collective-permute-start.7 = (bf16[512,256]{1,0:T(8,128)(2,1)S(1)}, bf16[512,256]{1,0:T(8,128)(2,1)S(1)}, u32[]{:S(2)}, u32[]{:S(2)}) collective-permute-start(bf16[512,256]{1,0:T(8,128)(2,1)S(1)} %collective-permute-done.3.kv1.rest_3_), channel_id=1, source_target_pairs={{0,4},{2,6},{4,8},{6,10},{8,12},{10,14},{12,0},{14,2},{1,5},{3,7},... | collective-permute-start | bytes 786440 | tf_op jit(solution)/shard_map/ppermute | solution.py:565
  33.3 2.4 %collective-permute-done.8.q_a = bf16[512,256]{1,0:T(8,128)(2,1)S(1)} collective-permute-done((bf16[512,256]{1,0:T(8,128)(2,1)S(1)}, bf16[512,256]{1,0:T(8,128)(2,1)S(1)}, u32[]{:S(2)}, u32[]{:S(2)}) %collective-permute-start.8) | collective-permute-done | bytes 262176 | tf_op jit(solution)/shard_map/ppermute | solution.py:559
  35.7 1.5 %collective-permute-start.9 = (bf16[512,256]{1,0:T(8,128)(2,1)S(1)}, bf16[512,256]{1,0:T(8,128)(2,1)S(1)}, u32[]{:S(2)}, u32[]{:S(2)}) collective-permute-start(bf16[512,256]{1,0:T(8,128)(2,1)S(1)} %collective-permute-done.1.q.q_part), channel_id=1, source_target_pairs={{4,0},{6,2},{8,4},{10,6},{12,8},{14,10},{5,1},{7,3},{9,5},{11,7},{... | collective-permute-start | bytes 786440 | tf_op jit(solution)/shard_map/ppermute | solution.py:564
  37.2 3.4 %shard_map.74 = (f32[1024,256]{1,0:T(8,128)S(1)}, f32[1024,256]{1,0:T(8,128)S(1)}, f32[1024,256]{1,0:T(8,128)S(1)}, bf16[1024,256]{1,0:T(8,128)(2,1)S(1)}) custom-call(f32[4,256,512]{2,1,0:T(8,128)S(1)} %get-tuple-element.34.near, f32[4,128,256]{2,1,0:T(8,128)S(1)} %get-tuple-element.35.mid, f32[3,4,64,64]{3,2,1,0:T(8,128)S(1)} %get-tuple-element.36.far, ...), custom_call_target="tpu_custom_call" | custom-call | flops 4000000000 | bytes 1000000 | tf_op jit(solution)/shard_map/pallas_call | solution.py:48
  40.6 6.5 %collective-permute-done.7.kv_b1.kv_b = bf16[512,256]{1,0:T(8,128)(2,1)S(1)} collective-permute-done((bf16[512,256]{1,0:T(8,128)(2,1)S(1)}, bf16[512,256]{1,0:T(8,128)(2,1)S(1)}, u32[]{:S(2)}, u32[]{:S(2)}) %collective-permute-start.7) | collective-permute-done | bytes 262176 | tf_op jit(solution)/shard_map/ppermute | solution.py:565
  47.1 4.3 %collective-permute-done.9.q_b = bf16[512,256]{1,0:T(8,128)(2,1)S(1)} collective-permute-done((bf16[512,256]{1,0:T(8,128)(2,1)S(1)}, bf16[512,256]{1,0:T(8,128)(2,1)S(1)}, u32[]{:S(2)}, u32[]{:S(2)}) %collective-permute-start.9) | collective-permute-done | bytes 262176 | tf_op jit(solution)/shard_map/ppermute | solution.py:564
  51.3 1.2 %shard_map.78 = bf16[1088,128]{1,0:T(8,128)(2,1)S(1)} custom-call(f32[3,4,64,64]{3,2,1,0:T(8,128)S(1)} %get-tuple-element.36.far, bf16[512,256]{1,0:T(8,128)(2,1)S(1)} %collective-permute-done.8.q_a, bf16[512,256]{1,0:T(8,128)(2,1)S(1)} %collective-permute-done.9.q_b, bf16[512,256]{1,0:T(8,128)(2,1)S(1)} %collective-permute-done.6.kv_a1.kv_a, ...), custom_call_target="tpu_custom_call" | custom-call | flops 1000000000 | bytes 1000000 | tf_op jit(solution)/shard_map/pallas_call | solution.py:48
  52.6 0.5 collective-permute-start.14
  53.1 0.0 collective-permute-done.4.kv_a0.kv_a
  53.1 0.0 collective-permute-done.5.kv_b0.kv_b
  53.1 1.2 %shard_map.76 = bf16[1088,128]{1,0:T(8,128)(2,1)S(1)} custom-call(f32[3,4,64,64]{3,2,1,0:T(8,128)S(1)} %get-tuple-element.36.far, bf16[512,256]{1,0:T(8,128)(2,1)S(1)} %collective-permute-done.8.q_a, bf16[512,256]{1,0:T(8,128)(2,1)S(1)} %collective-permute-done.9.q_b, bf16[512,256]{1,0:T(8,128)(2,1)S(1)} %collective-permute-done.4.kv_a0.kv_a, ...), custom_call_target="tpu_custom_call" | custom-call | flops 1000000000 | bytes 1000000 | tf_op jit(solution)/shard_map/pallas_call | solution.py:48
  54.3 0.6 collective-permute-start.10
  54.9 3.1 %shard_map.75 = (f32[1024,256]{1,0:T(8,128)S(1)}, f32[1024,256]{1,0:T(8,128)S(1)}, f32[1024,256]{1,0:T(8,128)S(1)}) custom-call(f32[4,256,512]{2,1,0:T(8,128)S(1)} %get-tuple-element.34.near, f32[4,128,256]{2,1,0:T(8,128)S(1)} %get-tuple-element.35.mid, f32[3,4,64,64]{3,2,1,0:T(8,128)S(1)} %get-tuple-element.36.far, ...), custom_call_target="tpu_custom_call" | custom-call | flops 4000000000 | bytes 1000000 | tf_op jit(solution)/shard_map/pallas_call | solution.py:48
  58.1 5.9 %collective-permute-done.14.far_in = bf16[1088,128]{1,0:T(8,128)(2,1)S(1)} collective-permute-done((bf16[1088,128]{1,0:T(8,128)(2,1)S(1)}, bf16[1088,128]{1,0:T(8,128)(2,1)S(1)}, u32[]{:S(2)}, u32[]{:S(2)}) %collective-permute-start.14) | collective-permute-done | bytes 278560 | tf_op jit(solution)/shard_map/ppermute | solution.py:574
  63.9 1.1 %shard_map.79 = (bf16[256,128]{1,0:T(8,128)(2,1)S(1)}, bf16[256,128]{1,0:T(8,128)(2,1)S(1)}, bf16[320,128]{1,0:T(8,128)(2,1)S(1)}, bf16[256,128]{1,0:T(8,128)(2,1)S(1)}, bf16[16,512]{1,0:T(8,128)(2,1)S(1)}) custom-call(f32[1024,256]{1,0:T(8,128)S(1)} %get-tuple-element.53.o_in, f32[1024,256]{1,0:T(8,128)S(1)} %get-tuple-element.54.m_in, ...), custom_call_target="tpu_custom_call" | custom-call | flops 1000000000 | bytes 1000000 | tf_op jit(solution)/shard_map/pallas_call | solution.py:48
  65.0 0.6 collective-permute-start.15
  65.6 1.6 %collective-permute-start.17 = (bf16[256,128]{1,0:T(8,128)(2,1)S(1)}, bf16[256,128]{1,0:T(8,128)(2,1)S(1)}, u32[]{:S(2)}, u32[]{:S(2)}) collective-permute-start(bf16[256,128]{1,0:T(8,128)(2,1)S(1)} %get-tuple-element.64), channel_id=1, source_target_pairs={{0,3},{1,2},{2,1},{3,0},{4,7},{5,6},{6,5},{7,4},{8,11},{9,10},{10,... | collective-permute-start | bytes 196616 | tf_op jit(solution)/shard_map/ppermute | solution.py:580
  67.2 1.8 %collective-permute-done.10.far_in = bf16[1088,128]{1,0:T(8,128)(2,1)S(1)} collective-permute-done((bf16[1088,128]{1,0:T(8,128)(2,1)S(1)}, bf16[1088,128]{1,0:T(8,128)(2,1)S(1)}, u32[]{:S(2)}, u32[]{:S(2)}) %collective-permute-start.10) | collective-permute-done | bytes 278560 | tf_op jit(solution)/shard_map/ppermute | solution.py:571
  68.9 1.1 %shard_map.77 = (bf16[256,128]{1,0:T(8,128)(2,1)S(1)}, bf16[256,128]{1,0:T(8,128)(2,1)S(1)}, bf16[320,128]{1,0:T(8,128)(2,1)S(1)}, bf16[256,128]{1,0:T(8,128)(2,1)S(1)}, bf16[16,512]{1,0:T(8,128)(2,1)S(1)}) custom-call(f32[1024,256]{1,0:T(8,128)S(1)} %get-tuple-element.53.o_in, f32[1024,256]{1,0:T(8,128)S(1)} %get-tuple-element.54.m_in, ...), custom_call_target="tpu_custom_call" | custom-call | flops 1000000000 | bytes 1000000 | tf_op jit(solution)/shard_map/pallas_call | solution.py:48
  70.0 0.6 collective-permute-start.11
  70.6 1.6 %collective-permute-start.13 = (bf16[256,128]{1,0:T(8,128)(2,1)S(1)}, bf16[256,128]{1,0:T(8,128)(2,1)S(1)}, u32[]{:S(2)}, u32[]{:S(2)}) collective-permute-start(bf16[256,128]{1,0:T(8,128)(2,1)S(1)} %get-tuple-element.59), channel_id=1, source_target_pairs={{0,3},{1,2},{2,1},{3,0},{4,7},{5,6},{6,5},{7,4},{8,11},{9,10},{10,... | collective-permute-start | bytes 196616 | tf_op jit(solution)/shard_map/ppermute | solution.py:580
  72.2 2.9 %collective-permute-done.13.refs_3_ = bf16[256,128]{1,0:T(8,128)(2,1)S(1)} collective-permute-done((bf16[256,128]{1,0:T(8,128)(2,1)S(1)}, bf16[256,128]{1,0:T(8,128)(2,1)S(1)}, u32[]{:S(2)}, u32[]{:S(2)}) %collective-permute-start.13) | collective-permute-done | bytes 65568 | tf_op jit(solution)/shard_map/ppermute | solution.py:580
  75.0 0.0 collective-permute-done.15.refs_6_
  75.0 0.1 collective-permute-done.11.refs_1_
  75.2 0.0 collective-permute-done.18.refs_11_
  75.2 2.3 %shard_map.80 = (bf16[256,2048]{1,0:T(8,128)(2,1)}, f32[8,512]{1,0:T(8,128)}) custom-call(bf16[256,128]{1,0:T(8,128)(2,1)S(1)} %get-tuple-element.56.refs_0_, bf16[320,128]{1,0:T(8,128)(2,1)S(1)} %collective-permute-done.11.refs_1_, bf16[256,128]{1,0:T(8,128)(2,1)S(1)} %collective-permute-done.12.refs_2_, ...), custom_call_target="tpu_custom_call" | custom-call | flops 1073741824 | bytes 1000000 | tf_op jit(solution)/shard_map/pallas_call | solution.py:48
  (13 shorter events, 0.0 us)
Async XLA Ops:
  0.6 3.1 %copy-start = (bf16[256,2048]{1,0:T(8,128)(2,1)S(1)}, bf16[256,2048]{1,0:T(8,128)(2,1)}, u32[]{:S(2)}) copy-start(bf16[256,2048]{1,0:T(8,128)(2,1)} %refs_0_.5) | copy-start | bytes 3145732
  0.6 3.1 %copy-start.4 = (bf16[2048,512]{1,0:T(8,128)(2,1)S(1)}, bf16[2048,512]{1,0:T(8,128)(2,1)}, u32[]{:S(2)}) copy-start(bf16[2048,512]{1,0:T(8,128)(2,1)} %refs_2_.3) | copy-start | bytes 6291460
  0.6 3.1 %collective-permute-start = (bf16[256,2048]{1,0:T(8,128)(2,1)}, bf16[256,2048]{1,0:T(8,128)(2,1)S(1)}, u32[]{:S(2)}, u32[]{:S(2)}) collective-permute-start(bf16[256,2048]{1,0:T(8,128)(2,1)} %refs_0_.5), channel_id=1, source_target_pairs={{0,1},{1,0},{2,3},{3,2},{4,5},{5,4},{6,7},{7,6},{8,9},{9,8},{10,11... | collective-permute-start | bytes 3145736 | tf_op jit(solution)/shard_map/ppermute | solution.py:553
  1.2 74.0 %collective-permute-start.18 = (bf16[512,2048]{1,0:T(8,128)(2,1)}, bf16[512,2048]{1,0:T(8,128)(2,1)S(1)}, u32[]{:S(2)}, u32[]{:S(2)}) collective-permute-start(bf16[512,2048]{1,0:T(8,128)(2,1)} %refs_10_.1), channel_id=1, source_target_pairs={{0,1},{1,0},{2,3},{3,2},{4,5},{5,4},{6,7},{7,6},{8,9},{9,8},{10,11... | collective-permute-start | bytes 6291464 | tf_op jit(solution)/shard_map/ppermute | solution.py:566
  1.8 6.5 %copy-start.1 = (bf16[2048,512]{1,0:T(8,128)(2,1)S(1)}, bf16[2048,512]{1,0:T(8,128)(2,1)}, u32[]{:S(2)}) copy-start(bf16[2048,512]{1,0:T(8,128)(2,1)} %refs_2_.5) | copy-start | bytes 6291460
  1.8 6.5 %copy-start.2 = (bf16[2048,512]{1,0:T(8,128)(2,1)S(1)}, bf16[2048,512]{1,0:T(8,128)(2,1)}, u32[]{:S(2)}) copy-start(bf16[2048,512]{1,0:T(8,128)(2,1)} %refs_3_.3) | copy-start | bytes 6291460
  5.4 13.7 %collective-permute-start.1 = (bf16[512,256]{1,0:T(8,128)(2,1)S(1)}, bf16[512,256]{1,0:T(8,128)(2,1)S(1)}, u32[]{:S(2)}, u32[]{:S(2)}) collective-permute-start(bf16[512,256]{1,0:T(8,128)(2,1)S(1)} %get-tuple-element.38), channel_id=1, source_target_pairs={{0,2},{2,0},{4,6},{6,4},{8,10},{10,8},{12,14},{14,12},{1,3},{3,1},... | collective-permute-start | bytes 786440 | tf_op jit(solution)/shard_map/ppermute | solution.py:558
  10.0 11.1 %collective-permute-start.2 = (bf16[512,256]{1,0:T(8,128)(2,1)S(1)}, bf16[512,256]{1,0:T(8,128)(2,1)S(1)}, u32[]{:S(2)}, u32[]{:S(2)}) collective-permute-start(bf16[512,256]{1,0:T(8,128)(2,1)S(1)} %get-tuple-element.41), channel_id=1, source_target_pairs={{0,2},{2,0},{4,6},{6,4},{8,10},{10,8},{12,14},{14,12},{1,3},{3,1},... | collective-permute-start | bytes 786440 | tf_op jit(solution)/shard_map/ppermute | solution.py:555
  11.7 14.4 %collective-permute-start.3 = (bf16[512,256]{1,0:T(8,128)(2,1)S(1)}, bf16[512,256]{1,0:T(8,128)(2,1)S(1)}, u32[]{:S(2)}, u32[]{:S(2)}) collective-permute-start(bf16[512,256]{1,0:T(8,128)(2,1)S(1)} %get-tuple-element.42), channel_id=1, source_target_pairs={{0,2},{2,0},{4,6},{6,4},{8,10},{10,8},{12,14},{14,12},{1,3},{3,1},... | collective-permute-start | bytes 786440 | tf_op jit(solution)/shard_map/ppermute | solution.py:561
  13.8 39.3 %collective-permute-start.4 = (bf16[512,256]{1,0:T(8,128)(2,1)S(1)}, bf16[512,256]{1,0:T(8,128)(2,1)S(1)}, u32[]{:S(2)}, u32[]{:S(2)}) collective-permute-start(bf16[512,256]{1,0:T(8,128)(2,1)S(1)} %get-tuple-element.39.kv0.rest_0_), channel_id=1, source_target_pairs={{0,4},{2,6},{4,8},{6,10},{8,12},{10,14},{12,0},{14,2},{1,5},{3,7},... | collective-permute-start | bytes 786440 | tf_op jit(solution)/shard_map/ppermute | solution.py:556
  19.1 12.6 %collective-permute-start.6 = (bf16[512,256]{1,0:T(8,128)(2,1)S(1)}, bf16[512,256]{1,0:T(8,128)(2,1)S(1)}, u32[]{:S(2)}, u32[]{:S(2)}) collective-permute-start(bf16[512,256]{1,0:T(8,128)(2,1)S(1)} %get-tuple-element.40.kv1.rest_1_), channel_id=1, source_target_pairs={{0,4},{2,6},{4,8},{6,10},{8,12},{10,14},{12,0},{14,2},{1,5},{3,7},... | collective-permute-start | bytes 786440 | tf_op jit(solution)/shard_map/ppermute | solution.py:562
  21.1 14.6 %collective-permute-start.8 = (bf16[512,256]{1,0:T(8,128)(2,1)S(1)}, bf16[512,256]{1,0:T(8,128)(2,1)S(1)}, u32[]{:S(2)}, u32[]{:S(2)}) collective-permute-start(bf16[512,256]{1,0:T(8,128)(2,1)S(1)} %get-tuple-element.37.q.q_mine), channel_id=1, source_target_pairs={{4,0},{6,2},{8,4},{10,6},{12,8},{14,10},{5,1},{7,3},{9,5},{11,7},{... | collective-permute-start | bytes 786440 | tf_op jit(solution)/shard_map/ppermute | solution.py:559
  26.2 26.9 %collective-permute-start.5 = (bf16[512,256]{1,0:T(8,128)(2,1)S(1)}, bf16[512,256]{1,0:T(8,128)(2,1)S(1)}, u32[]{:S(2)}, u32[]{:S(2)}) collective-permute-start(bf16[512,256]{1,0:T(8,128)(2,1)S(1)} %collective-permute-done.2.kv0.rest_2_), channel_id=1, source_target_pairs={{0,4},{2,6},{4,8},{6,10},{8,12},{10,14},{12,0},{14,2},{1,5},{3,7},... | collective-permute-start | bytes 786440 | tf_op jit(solution)/shard_map/ppermute | solution.py:563
  31.7 15.4 %collective-permute-start.7 = (bf16[512,256]{1,0:T(8,128)(2,1)S(1)}, bf16[512,256]{1,0:T(8,128)(2,1)S(1)}, u32[]{:S(2)}, u32[]{:S(2)}) collective-permute-start(bf16[512,256]{1,0:T(8,128)(2,1)S(1)} %collective-permute-done.3.kv1.rest_3_), channel_id=1, source_target_pairs={{0,4},{2,6},{4,8},{6,10},{8,12},{10,14},{12,0},{14,2},{1,5},{3,7},... | collective-permute-start | bytes 786440 | tf_op jit(solution)/shard_map/ppermute | solution.py:565
  35.7 15.6 %collective-permute-start.9 = (bf16[512,256]{1,0:T(8,128)(2,1)S(1)}, bf16[512,256]{1,0:T(8,128)(2,1)S(1)}, u32[]{:S(2)}, u32[]{:S(2)}) collective-permute-start(bf16[512,256]{1,0:T(8,128)(2,1)S(1)} %collective-permute-done.1.q.q_part), channel_id=1, source_target_pairs={{4,0},{6,2},{8,4},{10,6},{12,8},{14,10},{5,1},{7,3},{9,5},{11,7},{... | collective-permute-start | bytes 786440 | tf_op jit(solution)/shard_map/ppermute | solution.py:564
  52.6 11.3 %collective-permute-start.14 = (bf16[1088,128]{1,0:T(8,128)(2,1)S(1)}, bf16[1088,128]{1,0:T(8,128)(2,1)S(1)}, u32[]{:S(2)}, u32[]{:S(2)}) collective-permute-start(bf16[1088,128]{1,0:T(8,128)(2,1)S(1)} %shard_map.78), channel_id=1, source_target_pairs={{0,4},{2,6},{4,8},{6,10},{8,12},{10,14},{12,0},{14,2},{1,5},{3,7},... | collective-permute-start | bytes 835592 | tf_op jit(solution)/shard_map/ppermute | solution.py:574
  54.3 14.6 %collective-permute-start.10 = (bf16[1088,128]{1,0:T(8,128)(2,1)S(1)}, bf16[1088,128]{1,0:T(8,128)(2,1)S(1)}, u32[]{:S(2)}, u32[]{:S(2)}) collective-permute-start(bf16[1088,128]{1,0:T(8,128)(2,1)S(1)} %shard_map.76), channel_id=1, source_target_pairs={{0,4},{2,6},{4,8},{6,10},{8,12},{10,14},{12,0},{14,2},{1,5},{3,7},... | collective-permute-start | bytes 835592 | tf_op jit(solution)/shard_map/ppermute | solution.py:571
  65.0 10.2 %copy-start.3 = (bf16[512,2048]{1,0:T(8,128)(2,1)S(1)}, bf16[512,2048]{1,0:T(8,128)(2,1)}, u32[]{:S(2)}) copy-start(bf16[512,2048]{1,0:T(8,128)(2,1)} %refs_10_.1) | copy-start | bytes 6291460
  65.0 10.1 %collective-permute-start.15 = (bf16[320,128]{1,0:T(8,128)(2,1)S(1)}, bf16[320,128]{1,0:T(8,128)(2,1)S(1)}, u32[]{:S(2)}, u32[]{:S(2)}) collective-permute-start(bf16[320,128]{1,0:T(8,128)(2,1)S(1)} %get-tuple-element.62), channel_id=1, source_target_pairs={{0,2},{2,0},{4,6},{6,4},{8,10},{10,8},{12,14},{14,12},{1,3},{3,1},... | collective-permute-start | bytes 245768 | tf_op jit(solution)/shard_map/ppermute | solution.py:579
  65.6 5.0 %collective-permute-start.16 = (bf16[256,128]{1,0:T(8,128)(2,1)S(1)}, bf16[256,128]{1,0:T(8,128)(2,1)S(1)}, u32[]{:S(2)}, u32[]{:S(2)}) collective-permute-start(bf16[256,128]{1,0:T(8,128)(2,1)S(1)} %get-tuple-element.63), channel_id=1, source_target_pairs={{0,1},{1,0},{2,3},{3,2},{4,5},{5,4},{6,7},{7,6},{8,9},{9,8},{10,11... | collective-permute-start | bytes 196616 | tf_op jit(solution)/shard_map/ppermute | solution.py:581
  65.6 5.0 %collective-permute-start.17 = (bf16[256,128]{1,0:T(8,128)(2,1)S(1)}, bf16[256,128]{1,0:T(8,128)(2,1)S(1)}, u32[]{:S(2)}, u32[]{:S(2)}) collective-permute-start(bf16[256,128]{1,0:T(8,128)(2,1)S(1)} %get-tuple-element.64), channel_id=1, source_target_pairs={{0,3},{1,2},{2,1},{3,0},{4,7},{5,6},{6,5},{7,4},{8,11},{9,10},{10,... | collective-permute-start | bytes 196616 | tf_op jit(solution)/shard_map/ppermute | solution.py:580
  70.0 5.2 %collective-permute-start.11 = (bf16[320,128]{1,0:T(8,128)(2,1)S(1)}, bf16[320,128]{1,0:T(8,128)(2,1)S(1)}, u32[]{:S(2)}, u32[]{:S(2)}) collective-permute-start(bf16[320,128]{1,0:T(8,128)(2,1)S(1)} %get-tuple-element.57), channel_id=1, source_target_pairs={{0,2},{2,0},{4,6},{6,4},{8,10},{10,8},{12,14},{14,12},{1,3},{3,1},... | collective-permute-start | bytes 245768 | tf_op jit(solution)/shard_map/ppermute | solution.py:579
  70.6 1.6 %collective-permute-start.12 = (bf16[256,128]{1,0:T(8,128)(2,1)S(1)}, bf16[256,128]{1,0:T(8,128)(2,1)S(1)}, u32[]{:S(2)}, u32[]{:S(2)}) collective-permute-start(bf16[256,128]{1,0:T(8,128)(2,1)S(1)} %get-tuple-element.58), channel_id=1, source_target_pairs={{0,1},{1,0},{2,3},{3,2},{4,5},{5,4},{6,7},{7,6},{8,9},{9,8},{10,11... | collective-permute-start | bytes 196616 | tf_op jit(solution)/shard_map/ppermute | solution.py:581
  70.6 4.5 %collective-permute-start.13 = (bf16[256,128]{1,0:T(8,128)(2,1)S(1)}, bf16[256,128]{1,0:T(8,128)(2,1)S(1)}, u32[]{:S(2)}, u32[]{:S(2)}) collective-permute-start(bf16[256,128]{1,0:T(8,128)(2,1)S(1)} %get-tuple-element.59), channel_id=1, source_target_pairs={{0,3},{1,2},{2,1},{3,0},{4,7},{5,6},{6,5},{7,4},{8,11},{9,10},{10,... | collective-permute-start | bytes 196616 | tf_op jit(solution)/shard_map/ppermute | solution.py:580

commit v4 on v3

--- a/solution.py
+++ b/solution.py
@@ -25,6 +25,7 @@
 BF16 = jnp.bfloat16
 ANY = pl.BlockSpec(memory_space=pl.ANY)
 VMEM = pl.BlockSpec(memory_space=pltpu.VMEM)
+
 MIB = 1024 * 1024
 
 
@@ -243,7 +244,7 @@
     tile = FAR_DILATION * SUB
     chunks = block // tile
     refs = (o_ref, m_ref, l_ref)
-    step = 64
+    step = 128
     size = mid.shape[1]
     for pair, kv in enumerate((kv0, kv1)):
         for index in range(chunks):
@@ -289,7 +290,7 @@
     back = 1 if before else 0
     query_tile = 0 if before else chunks
     key_tile = (2 * chunks - 1 if before else chunks - 1) * tile
-    step = 64
+    step = 128
     size = mid.shape[1]
     for pair in range(len(kvs)):
         kv = kvs[pair]
@@ -546,6 +547,7 @@
     assert REACH == 4 * block and half == FAR_DILATION * SUB and width == 512
     ahead = [(n, (n + 2) % count) for n in range(count)]
     back = [(n + 2, n) for n in range(count - 2)]
+    onward = [(n, n + 2) for n in range(count - 2)]
     beside = [(n, n ^ 1) for n in range(count)]
     swap = [(0, 1), (1, 0)]
     crossed = [(2 * n + c, 2 * (n ^ 1) + 1 - c) for n in range(count) for c in range(2)]
@@ -560,9 +562,9 @@
     kv_t1, kv_m1 = project(tokens, x_other, [w_key, w_value], [256])
     kv_p1 = lax.ppermute(kv_t1, "sp", beside)
     kv_a1 = lax.ppermute(kv_m1, "sp", ahead)
-    kv_b0 = lax.ppermute(kv_p0, "sp", ahead)
+    kv_b0 = lax.ppermute(kv_p0, "sp", onward)
     q_b = lax.ppermute(q_p, "sp", back)
-    kv_b1 = lax.ppermute(kv_p1, "sp", ahead)
+    kv_b1 = lax.ppermute(kv_p1, "sp", onward)
     w_other = lax.ppermute(w_out, "tp", swap)
     bias = biases(block, heads)
     mine = block_attention(bias, q_m, kv_m0, kv_m1)

time: 77.7 us -> 70.2 us (0.903)
  waiting for transfers between devices: 29.8 us -> 18.5 us
  starting transfers between devices: 20.6 us -> 26 us
  Pallas kernels: 26.3 us -> 24.6 us
    ppermute x2, waiting for transfers between devices: 6.52 us -> 0.01 us  [the longest x1 0.01 us: layer(): kv_b1 = lax.ppermute(kv_p1, 'sp', onward)]
    ppermute x2, starting transfers between devices: 3.43 us -> 7.18 us  [the longest x1 3.72 us: layer(): kv_b0 = lax.ppermute(kv_p0, 'sp', onward)]
    ppermute x1, waiting for transfers between devices: 2.4 us -> 0.01 us  [layer(): q_a = lax.ppermute(q_m, 'sp', back)]
    ppermute x2, starting transfers between devices: 1.16 us -> 3.14 us  [layer(): same = lax.ppermute(same, 'sp', beside)]
    ppermute x1, waiting for transfers between devices: 1.75 us -> 0.01 us  [layer(): far_p = lax.ppermute(far0, 'sp', ahead)]
    pallas_call x13, Pallas kernels: 26.3 us -> 24.6 us  [call(): pl.pallas_call(kernel, out_shape=[jax.ShapeDtypeStruct(shape, kind) for s...]
    ppermute x2, starting transfers between devices: 3.21 us -> 2.11 us  [layer(): cross = lax.ppermute(cross, ('sp', 'tp'), crossed)]
    ppermute x1, starting transfers between devices: 0.54 us -> 1.58 us  [layer(): far_m = lax.ppermute(far1, 'sp', ahead)]
  transfers between devices with their start and end apart: 19 -> 19, of which waited for: 10 -> 7; matrix products, arithmetic and copies ran while one was open for 0% -> 0% of each run, Pallas kernels for 31% -> 32%
where the time goes in v4:
time: 70.2 us; the launch traced here: 69.9 us
  starting transfers between devices  26 us (37%)
  Pallas kernels  24.6 us (35%)
  waiting for transfers between devices  18.5 us (26%)
  between operations  0.82 us (1%)
    pallas_call x13, Pallas kernels, call(): pl.pallas_call(kernel, out_shape=[jax.ShapeDtypeStruct(shape, kind) for s...  24.6 us
    ppermute x1, waiting for transfers between devices, layer(): far_m = lax.ppermute(far1, 'sp', ahead)  5.02 us
    ppermute x1, waiting for transfers between devices, layer(): q_b = lax.ppermute(q_p, 'sp', back)  3.94 us
    ppermute x1, waiting for transfers between devices, layer(): kv_p1 = lax.ppermute(kv_t1, 'sp', beside)  3.78 us
    ppermute x1, starting transfers between devices, layer(): kv_b0 = lax.ppermute(kv_p0, 'sp', onward)  3.72 us
    ppermute x1, starting transfers between devices, layer(): kv_b1 = lax.ppermute(kv_p1, 'sp', onward)  3.47 us
    ppermute x2, starting transfers between devices, layer(): same = lax.ppermute(same, 'sp', beside)  3.14 us
    ppermute x1, starting transfers between devices, layer(): q_p = lax.ppermute(q_t, 'sp', beside)  2.94 us
  transfers between devices with their start and end apart: 19, of which 7 were waited for; matrix products, arithmetic and copies ran while one was open for 0% of the time, Pallas kernels for 32%

profile of v4, /device:TPU:0, one launch (start us, length us, event | category | flops | bytes accessed | tf_op | source)
XLA Modules:
  0.0 69.9 jit_solution(5303807912442074219)
XLA Ops:
  0.6 0.6 collective-permute-start
  1.2 0.1 collective-permute-start.18
  1.3 0.5 shard_map.68
  1.8 0.0 copy-start.1
  1.8 0.0 copy-start.2
  1.8 1.9 %collective-permute-done.refs_1_ = bf16[256,2048]{1,0:T(8,128)(2,1)S(1)} collective-permute-done((bf16[256,2048]{1,0:T(8,128)(2,1)}, bf16[256,2048]{1,0:T(8,128)(2,1)S(1)}, u32[]{:S(2)}, u32[]{:S(2)}) %collective-permute-start) | collective-permute-done | bytes 1048608 | tf_op jit(solution)/shard_map/ppermute | solution.py:555
  3.7 1.7 %shard_map.69 = (bf16[512,256]{1,0:T(8,128)(2,1)S(1)}, bf16[512,256]{1,0:T(8,128)(2,1)S(1)}) custom-call(bf16[256,2048]{1,0:T(8,128)(2,1)S(1)} %copy-done, bf16[256,2048]{1,0:T(8,128)(2,1)S(1)} %collective-permute-done.refs_1_, bf16[2048,512]{1,0:T(8,128)(2,1)S(1)} %copy-done.4), custom_call_target="tpu_custom_call" | custom-call | flops 1073741824 | bytes 1000000 | tf_op jit(solution)/shard_map/pallas_call | solution.py:49
  5.4 2.9 %collective-permute-start.1 = (bf16[512,256]{1,0:T(8,128)(2,1)S(1)}, bf16[512,256]{1,0:T(8,128)(2,1)S(1)}, u32[]{:S(2)}, u32[]{:S(2)}) collective-permute-start(bf16[512,256]{1,0:T(8,128)(2,1)S(1)} %get-tuple-element.38), channel_id=1, source_target_pairs={{0,2},{2,0},{4,6},{6,4},{8,10},{10,8},{12,14},{14,12},{1,3},{3,1},... | collective-permute-start | bytes 786440 | tf_op jit(solution)/shard_map/ppermute | solution.py:560
  8.3 1.7 %shard_map.70 = (bf16[512,256]{1,0:T(8,128)(2,1)S(1)}, bf16[512,256]{1,0:T(8,128)(2,1)S(1)}) custom-call(bf16[256,2048]{1,0:T(8,128)(2,1)S(1)} %copy-done, bf16[256,2048]{1,0:T(8,128)(2,1)S(1)} %collective-permute-done.refs_1_, bf16[2048,512]{1,0:T(8,128)(2,1)S(1)} %copy-done.1, bf16[2048,512]{1,0:T(8,128)(2,1)S(1)} %copy-done.2), custom_call_target="tpu_custom_call" | custom-call | flops 1073741824 | bytes 1000000 | tf_op jit(solution)/shard_map/pallas_call | solution.py:49
  10.0 0.1 collective-permute-start.2
  10.1 1.7 %shard_map.71 = (bf16[512,256]{1,0:T(8,128)(2,1)S(1)}, bf16[512,256]{1,0:T(8,128)(2,1)S(1)}) custom-call(bf16[256,2048]{1,0:T(8,128)(2,1)S(1)} %copy-done, bf16[256,2048]{1,0:T(8,128)(2,1)S(1)} %collective-permute-done.refs_1_, bf16[2048,512]{1,0:T(8,128)(2,1)S(1)} %copy-done.1, bf16[2048,512]{1,0:T(8,128)(2,1)S(1)} %copy-done.2), custom_call_target="tpu_custom_call" | custom-call | flops 1073741824 | bytes 1000000 | tf_op jit(solution)/shard_map/pallas_call | solution.py:49
  11.7 2.1 %collective-permute-start.3 = (bf16[512,256]{1,0:T(8,128)(2,1)S(1)}, bf16[512,256]{1,0:T(8,128)(2,1)S(1)}, u32[]{:S(2)}, u32[]{:S(2)}) collective-permute-start(bf16[512,256]{1,0:T(8,128)(2,1)S(1)} %get-tuple-element.42), channel_id=1, source_target_pairs={{0,2},{2,0},{4,6},{6,4},{8,10},{10,8},{12,14},{14,12},{1,3},{3,1},... | collective-permute-start | bytes 786440 | tf_op jit(solution)/shard_map/ppermute | solution.py:563
  13.8 1.6 %collective-permute-start.4 = (bf16[512,256]{1,0:T(8,128)(2,1)S(1)}, bf16[512,256]{1,0:T(8,128)(2,1)S(1)}, u32[]{:S(2)}, u32[]{:S(2)}) collective-permute-start(bf16[512,256]{1,0:T(8,128)(2,1)S(1)} %get-tuple-element.39.kv0.rest_0_), channel_id=1, source_target_pairs={{0,4},{2,6},{4,8},{6,10},{8,12},{10,14},{12,0},{14,2},{1,5},{3,7},... | collective-permute-start | bytes 786440 | tf_op jit(solution)/shard_map/ppermute | solution.py:558
  15.4 2.9 %shard_map.72 = (f32[512,256]{1,0:T(8,128)S(1)}, f32[512,256]{1,0:T(8,128)S(1)}, f32[512,256]{1,0:T(8,128)S(1)}) custom-call(f32[4,256,512]{2,1,0:T(8,128)S(1)} %get-tuple-element.34.near, f32[4,128,256]{2,1,0:T(8,128)S(1)} %get-tuple-element.35.mid, bf16[512,256]{1,0:T(8,128)(2,1)S(1)} %get-tuple-element.37.q.q_mine, ...), custom_call_target="tpu_custom_call" | custom-call | flops 4000000000 | bytes 1000000 | tf_op jit(solution)/shard_map/pallas_call | solution.py:49
  18.3 1.6 %collective-permute-start.6 = (bf16[512,256]{1,0:T(8,128)(2,1)S(1)}, bf16[512,256]{1,0:T(8,128)(2,1)S(1)}, u32[]{:S(2)}, u32[]{:S(2)}) collective-permute-start(bf16[512,256]{1,0:T(8,128)(2,1)S(1)} %get-tuple-element.40.kv1.rest_1_), channel_id=1, source_target_pairs={{0,4},{2,6},{4,8},{6,10},{8,12},{10,14},{12,0},{14,2},{1,5},{3,7},... | collective-permute-start | bytes 786440 | tf_op jit(solution)/shard_map/ppermute | solution.py:564
  19.9 1.2 %collective-permute-done.2.kv0.rest_2_ = bf16[512,256]{1,0:T(8,128)(2,1)S(1)} collective-permute-done((bf16[512,256]{1,0:T(8,128)(2,1)S(1)}, bf16[512,256]{1,0:T(8,128)(2,1)S(1)}, u32[]{:S(2)}, u32[]{:S(2)}) %collective-permute-start.2) | collective-permute-done | bytes 262176 | tf_op jit(solution)/shard_map/ppermute | solution.py:557
  21.1 1.3 %collective-permute-start.8 = (bf16[512,256]{1,0:T(8,128)(2,1)S(1)}, bf16[512,256]{1,0:T(8,128)(2,1)S(1)}, u32[]{:S(2)}, u32[]{:S(2)}) collective-permute-start(bf16[512,256]{1,0:T(8,128)(2,1)S(1)} %get-tuple-element.37.q.q_mine), channel_id=1, source_target_pairs={{4,0},{6,2},{8,4},{10,6},{12,8},{14,10},{5,1},{7,3},{9,5},{11,7},{... | collective-permute-start | bytes 786440 | tf_op jit(solution)/shard_map/ppermute | solution.py:561
  22.4 3.8 %collective-permute-done.3.kv1.rest_3_ = bf16[512,256]{1,0:T(8,128)(2,1)S(1)} collective-permute-done((bf16[512,256]{1,0:T(8,128)(2,1)S(1)}, bf16[512,256]{1,0:T(8,128)(2,1)S(1)}, u32[]{:S(2)}, u32[]{:S(2)}) %collective-permute-start.3) | collective-permute-done | bytes 262176 | tf_op jit(solution)/shard_map/ppermute | solution.py:563
  26.2 3.7 %collective-permute-start.5 = (bf16[512,256]{1,0:T(8,128)(2,1)S(1)}, bf16[512,256]{1,0:T(8,128)(2,1)S(1)}, u32[]{:S(2)}, u32[]{:S(2)}) collective-permute-start(bf16[512,256]{1,0:T(8,128)(2,1)S(1)} %collective-permute-done.2.kv0.rest_2_), channel_id=1, source_target_pairs={{0,4},{2,6},{4,8},{6,10},{8,12},{10,14},{1,5},{3,7},{5,9},{7,11},{... | collective-permute-start | bytes 786440 | tf_op jit(solution)/shard_map/ppermute | solution.py:565
  29.9 2.9 %shard_map.73 = (f32[512,256]{1,0:T(8,128)S(1)}, f32[512,256]{1,0:T(8,128)S(1)}, f32[512,256]{1,0:T(8,128)S(1)}) custom-call(f32[4,256,512]{2,1,0:T(8,128)S(1)} %get-tuple-element.34.near, f32[4,128,256]{2,1,0:T(8,128)S(1)} %get-tuple-element.35.mid, bf16[512,256]{1,0:T(8,128)(2,1)S(1)} %collective-permute-done.1.q.q_part, ...), custom_call_target="tpu_custom_call" | custom-call | flops 4000000000 | bytes 1000000 | tf_op jit(solution)/shard_map/pallas_call | solution.py:49
  32.8 0.0 collective-permute-done.6.kv_a1.kv_a
  32.8 3.5 %collective-permute-start.7 = (bf16[512,256]{1,0:T(8,128)(2,1)S(1)}, bf16[512,256]{1,0:T(8,128)(2,1)S(1)}, u32[]{:S(2)}, u32[]{:S(2)}) collective-permute-start(bf16[512,256]{1,0:T(8,128)(2,1)S(1)} %collective-permute-done.3.kv1.rest_3_), channel_id=1, source_target_pairs={{0,4},{2,6},{4,8},{6,10},{8,12},{10,14},{1,5},{3,7},{5,9},{7,11},{... | collective-permute-start | bytes 786440 | tf_op jit(solution)/shard_map/ppermute | solution.py:567
  36.3 1.5 %collective-permute-start.9 = (bf16[512,256]{1,0:T(8,128)(2,1)S(1)}, bf16[512,256]{1,0:T(8,128)(2,1)S(1)}, u32[]{:S(2)}, u32[]{:S(2)}) collective-permute-start(bf16[512,256]{1,0:T(8,128)(2,1)S(1)} %collective-permute-done.1.q.q_part), channel_id=1, source_target_pairs={{4,0},{6,2},{8,4},{10,6},{12,8},{14,10},{5,1},{7,3},{9,5},{11,7},{... | collective-permute-start | bytes 786440 | tf_op jit(solution)/shard_map/ppermute | solution.py:566
  37.7 3.4 %shard_map.74 = (f32[1024,256]{1,0:T(8,128)S(1)}, f32[1024,256]{1,0:T(8,128)S(1)}, f32[1024,256]{1,0:T(8,128)S(1)}, bf16[1024,256]{1,0:T(8,128)(2,1)S(1)}) custom-call(f32[4,256,512]{2,1,0:T(8,128)S(1)} %get-tuple-element.34.near, f32[4,128,256]{2,1,0:T(8,128)S(1)} %get-tuple-element.35.mid, f32[3,4,64,64]{3,2,1,0:T(8,128)S(1)} %get-tuple-element.36.far, ...), custom_call_target="tpu_custom_call" | custom-call | flops 4000000000 | bytes 1000000 | tf_op jit(solution)/shard_map/pallas_call | solution.py:49
  41.1 0.0 collective-permute-done.7.kv_b1.kv_b
  41.1 3.9 %collective-permute-done.9.q_b = bf16[512,256]{1,0:T(8,128)(2,1)S(1)} collective-permute-done((bf16[512,256]{1,0:T(8,128)(2,1)S(1)}, bf16[512,256]{1,0:T(8,128)(2,1)S(1)}, u32[]{:S(2)}, u32[]{:S(2)}) %collective-permute-start.9) | collective-permute-done | bytes 262176 | tf_op jit(solution)/shard_map/ppermute | solution.py:566
  45.1 1.2 %shard_map.78 = bf16[1088,128]{1,0:T(8,128)(2,1)S(1)} custom-call(f32[3,4,64,64]{3,2,1,0:T(8,128)S(1)} %get-tuple-element.36.far, bf16[512,256]{1,0:T(8,128)(2,1)S(1)} %collective-permute-done.8.q_a, bf16[512,256]{1,0:T(8,128)(2,1)S(1)} %collective-permute-done.9.q_b, bf16[512,256]{1,0:T(8,128)(2,1)S(1)} %collective-permute-done.6.kv_a1.kv_a, ...), custom_call_target="tpu_custom_call" | custom-call | flops 1000000000 | bytes 1000000 | tf_op jit(solution)/shard_map/pallas_call | solution.py:49
  46.3 1.6 %collective-permute-start.14 = (bf16[1088,128]{1,0:T(8,128)(2,1)S(1)}, bf16[1088,128]{1,0:T(8,128)(2,1)S(1)}, u32[]{:S(2)}, u32[]{:S(2)}) collective-permute-start(bf16[1088,128]{1,0:T(8,128)(2,1)S(1)} %shard_map.78), channel_id=1, source_target_pairs={{0,4},{2,6},{4,8},{6,10},{8,12},{10,14},{12,0},{14,2},{1,5},{3,7},... | collective-permute-start | bytes 835592 | tf_op jit(solution)/shard_map/ppermute | solution.py:576
  47.9 1.2 %shard_map.76 = bf16[1088,128]{1,0:T(8,128)(2,1)S(1)} custom-call(f32[3,4,64,64]{3,2,1,0:T(8,128)S(1)} %get-tuple-element.36.far, bf16[512,256]{1,0:T(8,128)(2,1)S(1)} %collective-permute-done.8.q_a, bf16[512,256]{1,0:T(8,128)(2,1)S(1)} %collective-permute-done.9.q_b, bf16[512,256]{1,0:T(8,128)(2,1)S(1)} %collective-permute-done.4.kv_a0.kv_a, ...), custom_call_target="tpu_custom_call" | custom-call | flops 1000000000 | bytes 1000000 | tf_op jit(solution)/shard_map/pallas_call | solution.py:49
  49.1 0.3 collective-permute-start.10
  49.4 3.1 %shard_map.75 = (f32[1024,256]{1,0:T(8,128)S(1)}, f32[1024,256]{1,0:T(8,128)S(1)}, f32[1024,256]{1,0:T(8,128)S(1)}) custom-call(f32[4,256,512]{2,1,0:T(8,128)S(1)} %get-tuple-element.34.near, f32[4,128,256]{2,1,0:T(8,128)S(1)} %get-tuple-element.35.mid, f32[3,4,64,64]{3,2,1,0:T(8,128)S(1)} %get-tuple-element.36.far, ...), custom_call_target="tpu_custom_call" | custom-call | flops 4000000000 | bytes 1000000 | tf_op jit(solution)/shard_map/pallas_call | solution.py:49
  52.5 5.0 %collective-permute-done.14.far_in = bf16[1088,128]{1,0:T(8,128)(2,1)S(1)} collective-permute-done((bf16[1088,128]{1,0:T(8,128)(2,1)S(1)}, bf16[1088,128]{1,0:T(8,128)(2,1)S(1)}, u32[]{:S(2)}, u32[]{:S(2)}) %collective-permute-start.14) | collective-permute-done | bytes 278560 | tf_op jit(solution)/shard_map/ppermute | solution.py:576
  57.5 1.1 %shard_map.79 = (bf16[256,128]{1,0:T(8,128)(2,1)S(1)}, bf16[256,128]{1,0:T(8,128)(2,1)S(1)}, bf16[320,128]{1,0:T(8,128)(2,1)S(1)}, bf16[256,128]{1,0:T(8,128)(2,1)S(1)}, bf16[16,512]{1,0:T(8,128)(2,1)S(1)}) custom-call(f32[1024,256]{1,0:T(8,128)S(1)} %get-tuple-element.53.o_in, f32[1024,256]{1,0:T(8,128)S(1)} %get-tuple-element.54.m_in, ...), custom_call_target="tpu_custom_call" | custom-call | flops 1000000000 | bytes 1000000 | tf_op jit(solution)/shard_map/pallas_call | solution.py:49
  58.6 1.6 %collective-permute-start.15 = (bf16[320,128]{1,0:T(8,128)(2,1)S(1)}, bf16[320,128]{1,0:T(8,128)(2,1)S(1)}, u32[]{:S(2)}, u32[]{:S(2)}) collective-permute-start(bf16[320,128]{1,0:T(8,128)(2,1)S(1)} %get-tuple-element.62), channel_id=1, source_target_pairs={{0,2},{2,0},{4,6},{6,4},{8,10},{10,8},{12,14},{14,12},{1,3},{3,1},... | collective-permute-start | bytes 245768 | tf_op jit(solution)/shard_map/ppermute | solution.py:581
  60.2 0.6 collective-permute-start.17
  60.8 0.0 collective-permute-done.10.far_in
  60.8 1.1 %shard_map.77 = (bf16[256,128]{1,0:T(8,128)(2,1)S(1)}, bf16[256,128]{1,0:T(8,128)(2,1)S(1)}, bf16[320,128]{1,0:T(8,128)(2,1)S(1)}, bf16[256,128]{1,0:T(8,128)(2,1)S(1)}, bf16[16,512]{1,0:T(8,128)(2,1)S(1)}) custom-call(f32[1024,256]{1,0:T(8,128)S(1)} %get-tuple-element.53.o_in, f32[1024,256]{1,0:T(8,128)S(1)} %get-tuple-element.54.m_in, ...), custom_call_target="tpu_custom_call" | custom-call | flops 1000000000 | bytes 1000000 | tf_op jit(solution)/shard_map/pallas_call | solution.py:49
  61.9 1.6 %collective-permute-start.11 = (bf16[320,128]{1,0:T(8,128)(2,1)S(1)}, bf16[320,128]{1,0:T(8,128)(2,1)S(1)}, u32[]{:S(2)}, u32[]{:S(2)}) collective-permute-start(bf16[320,128]{1,0:T(8,128)(2,1)S(1)} %get-tuple-element.57), channel_id=1, source_target_pairs={{0,2},{2,0},{4,6},{6,4},{8,10},{10,8},{12,14},{14,12},{1,3},{3,1},... | collective-permute-start | bytes 245768 | tf_op jit(solution)/shard_map/ppermute | solution.py:581
  63.4 0.0 collective-permute-done.16.refs_7_
  63.4 0.0 collective-permute-start.12
  63.4 0.4 collective-permute-done.17.refs_8_
  63.9 1.5 %collective-permute-start.13 = (bf16[256,128]{1,0:T(8,128)(2,1)S(1)}, bf16[256,128]{1,0:T(8,128)(2,1)S(1)}, u32[]{:S(2)}, u32[]{:S(2)}) collective-permute-start(bf16[256,128]{1,0:T(8,128)(2,1)S(1)} %get-tuple-element.59), channel_id=1, source_target_pairs={{0,3},{1,2},{2,1},{3,0},{4,7},{5,6},{6,5},{7,4},{8,11},{9,10},{10,... | collective-permute-start | bytes 196616 | tf_op jit(solution)/shard_map/ppermute | solution.py:582
  65.4 0.0 collective-permute-done.12.refs_2_
  65.4 2.2 %collective-permute-done.13.refs_3_ = bf16[256,128]{1,0:T(8,128)(2,1)S(1)} collective-permute-done((bf16[256,128]{1,0:T(8,128)(2,1)S(1)}, bf16[256,128]{1,0:T(8,128)(2,1)S(1)}, u32[]{:S(2)}, u32[]{:S(2)}) %collective-permute-start.13) | collective-permute-done | bytes 65568 | tf_op jit(solution)/shard_map/ppermute | solution.py:582
  67.6 0.0 collective-permute-done.15.refs_6_
  67.6 0.0 collective-permute-done.11.refs_1_
  67.6 0.0 collective-permute-done.18.refs_11_
  67.6 2.3 %shard_map.80 = (bf16[256,2048]{1,0:T(8,128)(2,1)}, f32[8,512]{1,0:T(8,128)}) custom-call(bf16[256,128]{1,0:T(8,128)(2,1)S(1)} %get-tuple-element.56.refs_0_, bf16[320,128]{1,0:T(8,128)(2,1)S(1)} %collective-permute-done.11.refs_1_, bf16[256,128]{1,0:T(8,128)(2,1)S(1)} %collective-permute-done.12.refs_2_, ...), custom_call_target="tpu_custom_call" | custom-call | flops 1073741824 | bytes 1000000 | tf_op jit(solution)/shard_map/pallas_call | solution.py:49
  (13 shorter events, 0.0 us)
Async XLA Ops:
  0.6 3.1 %copy-start = (bf16[256,2048]{1,0:T(8,128)(2,1)S(1)}, bf16[256,2048]{1,0:T(8,128)(2,1)}, u32[]{:S(2)}) copy-start(bf16[256,2048]{1,0:T(8,128)(2,1)} %refs_0_.5) | copy-start | bytes 3145732
  0.6 3.1 %copy-start.4 = (bf16[2048,512]{1,0:T(8,128)(2,1)S(1)}, bf16[2048,512]{1,0:T(8,128)(2,1)}, u32[]{:S(2)}) copy-start(bf16[2048,512]{1,0:T(8,128)(2,1)} %refs_2_.3) | copy-start | bytes 6291460
  0.6 3.1 %collective-permute-start = (bf16[256,2048]{1,0:T(8,128)(2,1)}, bf16[256,2048]{1,0:T(8,128)(2,1)S(1)}, u32[]{:S(2)}, u32[]{:S(2)}) collective-permute-start(bf16[256,2048]{1,0:T(8,128)(2,1)} %refs_0_.5), channel_id=1, source_target_pairs={{0,1},{1,0},{2,3},{3,2},{4,5},{5,4},{6,7},{7,6},{8,9},{9,8},{10,11... | collective-permute-start | bytes 3145736 | tf_op jit(solution)/shard_map/ppermute | solution.py:555
  1.2 66.4 %collective-permute-start.18 = (bf16[512,2048]{1,0:T(8,128)(2,1)}, bf16[512,2048]{1,0:T(8,128)(2,1)S(1)}, u32[]{:S(2)}, u32[]{:S(2)}) collective-permute-start(bf16[512,2048]{1,0:T(8,128)(2,1)} %refs_10_.1), channel_id=1, source_target_pairs={{0,1},{1,0},{2,3},{3,2},{4,5},{5,4},{6,7},{7,6},{8,9},{9,8},{10,11... | collective-permute-start | bytes 6291464 | tf_op jit(solution)/shard_map/ppermute | solution.py:568
  1.8 6.5 %copy-start.1 = (bf16[2048,512]{1,0:T(8,128)(2,1)S(1)}, bf16[2048,512]{1,0:T(8,128)(2,1)}, u32[]{:S(2)}) copy-start(bf16[2048,512]{1,0:T(8,128)(2,1)} %refs_2_.5) | copy-start | bytes 6291460
  1.8 6.5 %copy-start.2 = (bf16[2048,512]{1,0:T(8,128)(2,1)S(1)}, bf16[2048,512]{1,0:T(8,128)(2,1)}, u32[]{:S(2)}) copy-start(bf16[2048,512]{1,0:T(8,128)(2,1)} %refs_3_.3) | copy-start | bytes 6291460
  5.4 12.9 %collective-permute-start.1 = (bf16[512,256]{1,0:T(8,128)(2,1)S(1)}, bf16[512,256]{1,0:T(8,128)(2,1)S(1)}, u32[]{:S(2)}, u32[]{:S(2)}) collective-permute-start(bf16[512,256]{1,0:T(8,128)(2,1)S(1)} %get-tuple-element.38), channel_id=1, source_target_pairs={{0,2},{2,0},{4,6},{6,4},{8,10},{10,8},{12,14},{14,12},{1,3},{3,1},... | collective-permute-start | bytes 786440 | tf_op jit(solution)/shard_map/ppermute | solution.py:560
  10.0 11.1 %collective-permute-start.2 = (bf16[512,256]{1,0:T(8,128)(2,1)S(1)}, bf16[512,256]{1,0:T(8,128)(2,1)S(1)}, u32[]{:S(2)}, u32[]{:S(2)}) collective-permute-start(bf16[512,256]{1,0:T(8,128)(2,1)S(1)} %get-tuple-element.41), channel_id=1, source_target_pairs={{0,2},{2,0},{4,6},{6,4},{8,10},{10,8},{12,14},{14,12},{1,3},{3,1},... | collective-permute-start | bytes 786440 | tf_op jit(solution)/shard_map/ppermute | solution.py:557
  11.7 14.4 %collective-permute-start.3 = (bf16[512,256]{1,0:T(8,128)(2,1)S(1)}, bf16[512,256]{1,0:T(8,128)(2,1)S(1)}, u32[]{:S(2)}, u32[]{:S(2)}) collective-permute-start(bf16[512,256]{1,0:T(8,128)(2,1)S(1)} %get-tuple-element.42), channel_id=1, source_target_pairs={{0,2},{2,0},{4,6},{6,4},{8,10},{10,8},{12,14},{14,12},{1,3},{3,1},... | collective-permute-start | bytes 786440 | tf_op jit(solution)/shard_map/ppermute | solution.py:563
  13.8 34.1 %collective-permute-start.4 = (bf16[512,256]{1,0:T(8,128)(2,1)S(1)}, bf16[512,256]{1,0:T(8,128)(2,1)S(1)}, u32[]{:S(2)}, u32[]{:S(2)}) collective-permute-start(bf16[512,256]{1,0:T(8,128)(2,1)S(1)} %get-tuple-element.39.kv0.rest_0_), channel_id=1, source_target_pairs={{0,4},{2,6},{4,8},{6,10},{8,12},{10,14},{12,0},{14,2},{1,5},{3,7},... | collective-permute-start | bytes 786440 | tf_op jit(solution)/shard_map/ppermute | solution.py:558
  18.3 14.5 %collective-permute-start.6 = (bf16[512,256]{1,0:T(8,128)(2,1)S(1)}, bf16[512,256]{1,0:T(8,128)(2,1)S(1)}, u32[]{:S(2)}, u32[]{:S(2)}) collective-permute-start(bf16[512,256]{1,0:T(8,128)(2,1)S(1)} %get-tuple-element.40.kv1.rest_1_), channel_id=1, source_target_pairs={{0,4},{2,6},{4,8},{6,10},{8,12},{10,14},{12,0},{14,2},{1,5},{3,7},... | collective-permute-start | bytes 786440 | tf_op jit(solution)/shard_map/ppermute | solution.py:564
  21.1 15.2 %collective-permute-start.8 = (bf16[512,256]{1,0:T(8,128)(2,1)S(1)}, bf16[512,256]{1,0:T(8,128)(2,1)S(1)}, u32[]{:S(2)}, u32[]{:S(2)}) collective-permute-start(bf16[512,256]{1,0:T(8,128)(2,1)S(1)} %get-tuple-element.37.q.q_mine), channel_id=1, source_target_pairs={{4,0},{6,2},{8,4},{10,6},{12,8},{14,10},{5,1},{7,3},{9,5},{11,7},{... | collective-permute-start | bytes 786440 | tf_op jit(solution)/shard_map/ppermute | solution.py:561
  26.2 21.7 %collective-permute-start.5 = (bf16[512,256]{1,0:T(8,128)(2,1)S(1)}, bf16[512,256]{1,0:T(8,128)(2,1)S(1)}, u32[]{:S(2)}, u32[]{:S(2)}) collective-permute-start(bf16[512,256]{1,0:T(8,128)(2,1)S(1)} %collective-permute-done.2.kv0.rest_2_), channel_id=1, source_target_pairs={{0,4},{2,6},{4,8},{6,10},{8,12},{10,14},{1,5},{3,7},{5,9},{7,11},{... | collective-permute-start | bytes 786440 | tf_op jit(solution)/shard_map/ppermute | solution.py:565
  32.8 8.4 %collective-permute-start.7 = (bf16[512,256]{1,0:T(8,128)(2,1)S(1)}, bf16[512,256]{1,0:T(8,128)(2,1)S(1)}, u32[]{:S(2)}, u32[]{:S(2)}) collective-permute-start(bf16[512,256]{1,0:T(8,128)(2,1)S(1)} %collective-permute-done.3.kv1.rest_3_), channel_id=1, source_target_pairs={{0,4},{2,6},{4,8},{6,10},{8,12},{10,14},{1,5},{3,7},{5,9},{7,11},{... | collective-permute-start | bytes 786440 | tf_op jit(solution)/shard_map/ppermute | solution.py:567
  36.3 8.8 %collective-permute-start.9 = (bf16[512,256]{1,0:T(8,128)(2,1)S(1)}, bf16[512,256]{1,0:T(8,128)(2,1)S(1)}, u32[]{:S(2)}, u32[]{:S(2)}) collective-permute-start(bf16[512,256]{1,0:T(8,128)(2,1)S(1)} %collective-permute-done.1.q.q_part), channel_id=1, source_target_pairs={{4,0},{6,2},{8,4},{10,6},{12,8},{14,10},{5,1},{7,3},{9,5},{11,7},{... | collective-permute-start | bytes 786440 | tf_op jit(solution)/shard_map/ppermute | solution.py:566
  46.3 11.2 %collective-permute-start.14 = (bf16[1088,128]{1,0:T(8,128)(2,1)S(1)}, bf16[1088,128]{1,0:T(8,128)(2,1)S(1)}, u32[]{:S(2)}, u32[]{:S(2)}) collective-permute-start(bf16[1088,128]{1,0:T(8,128)(2,1)S(1)} %shard_map.78), channel_id=1, source_target_pairs={{0,4},{2,6},{4,8},{6,10},{8,12},{10,14},{12,0},{14,2},{1,5},{3,7},... | collective-permute-start | bytes 835592 | tf_op jit(solution)/shard_map/ppermute | solution.py:576
  49.1 11.7 %collective-permute-start.10 = (bf16[1088,128]{1,0:T(8,128)(2,1)S(1)}, bf16[1088,128]{1,0:T(8,128)(2,1)S(1)}, u32[]{:S(2)}, u32[]{:S(2)}) collective-permute-start(bf16[1088,128]{1,0:T(8,128)(2,1)S(1)} %shard_map.76), channel_id=1, source_target_pairs={{0,4},{2,6},{4,8},{6,10},{8,12},{10,14},{12,0},{14,2},{1,5},{3,7},... | collective-permute-start | bytes 835592 | tf_op jit(solution)/shard_map/ppermute | solution.py:573
  58.6 9.0 %copy-start.3 = (bf16[512,2048]{1,0:T(8,128)(2,1)S(1)}, bf16[512,2048]{1,0:T(8,128)(2,1)}, u32[]{:S(2)}) copy-start(bf16[512,2048]{1,0:T(8,128)(2,1)} %refs_10_.1) | copy-start | bytes 6291460
  58.6 9.0 %collective-permute-start.15 = (bf16[320,128]{1,0:T(8,128)(2,1)S(1)}, bf16[320,128]{1,0:T(8,128)(2,1)S(1)}, u32[]{:S(2)}, u32[]{:S(2)}) collective-permute-start(bf16[320,128]{1,0:T(8,128)(2,1)S(1)} %get-tuple-element.62), channel_id=1, source_target_pairs={{0,2},{2,0},{4,6},{6,4},{8,10},{10,8},{12,14},{14,12},{1,3},{3,1},... | collective-permute-start | bytes 245768 | tf_op jit(solution)/shard_map/ppermute | solution.py:581
  60.2 3.3 %collective-permute-start.16 = (bf16[256,128]{1,0:T(8,128)(2,1)S(1)}, bf16[256,128]{1,0:T(8,128)(2,1)S(1)}, u32[]{:S(2)}, u32[]{:S(2)}) collective-permute-start(bf16[256,128]{1,0:T(8,128)(2,1)S(1)} %get-tuple-element.63), channel_id=1, source_target_pairs={{0,1},{1,0},{2,3},{3,2},{4,5},{5,4},{6,7},{7,6},{8,9},{9,8},{10,11... | collective-permute-start | bytes 196616 | tf_op jit(solution)/shard_map/ppermute | solution.py:583
  60.2 3.7 %collective-permute-start.17 = (bf16[256,128]{1,0:T(8,128)(2,1)S(1)}, bf16[256,128]{1,0:T(8,128)(2,1)S(1)}, u32[]{:S(2)}, u32[]{:S(2)}) collective-permute-start(bf16[256,128]{1,0:T(8,128)(2,1)S(1)} %get-tuple-element.64), channel_id=1, source_target_pairs={{0,3},{1,2},{2,1},{3,0},{4,7},{5,6},{6,5},{7,4},{8,11},{9,10},{10,... | collective-permute-start | bytes 196616 | tf_op jit(solution)/shard_map/ppermute | solution.py:582
  61.9 5.7 %collective-permute-start.11 = (bf16[320,128]{1,0:T(8,128)(2,1)S(1)}, bf16[320,128]{1,0:T(8,128)(2,1)S(1)}, u32[]{:S(2)}, u32[]{:S(2)}) collective-permute-start(bf16[320,128]{1,0:T(8,128)(2,1)S(1)} %get-tuple-element.57), channel_id=1, source_target_pairs={{0,2},{2,0},{4,6},{6,4},{8,10},{10,8},{12,14},{14,12},{1,3},{3,1},... | collective-permute-start | bytes 245768 | tf_op jit(solution)/shard_map/ppermute | solution.py:581
  63.4 1.9 %collective-permute-start.12 = (bf16[256,128]{1,0:T(8,128)(2,1)S(1)}, bf16[256,128]{1,0:T(8,128)(2,1)S(1)}, u32[]{:S(2)}, u32[]{:S(2)}) collective-permute-start(bf16[256,128]{1,0:T(8,128)(2,1)S(1)} %get-tuple-element.58), channel_id=1, source_target_pairs={{0,1},{1,0},{2,3},{3,2},{4,5},{5,4},{6,7},{7,6},{8,9},{9,8},{10,11... | collective-permute-start | bytes 196616 | tf_op jit(solution)/shard_map/ppermute | solution.py:583
  63.9 3.7 %collective-permute-start.13 = (bf16[256,128]{1,0:T(8,128)(2,1)S(1)}, bf16[256,128]{1,0:T(8,128)(2,1)S(1)}, u32[]{:S(2)}, u32[]{:S(2)}) collective-permute-start(bf16[256,128]{1,0:T(8,128)(2,1)S(1)} %get-tuple-element.59), channel_id=1, source_target_pairs={{0,3},{1,2},{2,1},{3,0},{4,7},{5,6},{6,5},{7,4},{8,11},{9,10},{10,... | collective-permute-start | bytes 196616 | tf_op jit(solution)/shard_map/ppermute | solution.py:582

commit v5 on v4

--- a/solution.py
+++ b/solution.py
@@ -218,9 +218,8 @@
     )
 
 
-def stacked(ref, pair, rows, columns, extra=None):
-    both = jnp.concatenate([ref[2 * pair, rows, columns], ref[2 * pair + 1, rows, columns]], axis=0)
-    return both if extra is None else both + extra
+def stacked(ref, pair, rows, columns):
+    return jnp.concatenate([ref[2 * pair, rows, columns], ref[2 * pair + 1, rows, columns]], axis=0)
 
 
 def closed_gate():
@@ -283,7 +282,7 @@
     )
 
 
-def windows(refs, q, kvs, near, mid, far, before, closed):
+def windows(refs, q, kvs, near, mid, far, before):
     block = q.shape[0] // 2
     tile = FAR_DILATION * SUB
     chunks = block // tile
@@ -300,7 +299,7 @@
                 rows_of(q, starts, pair_lanes(pair)),
                 rows_of(kv, starts, KEYS),
                 rows_of(kv, starts, VALUES),
-                jnp.concatenate([far[back, 2 * pair], far[back, 2 * pair + 1]], axis=0) + closed,
+                jnp.concatenate([far[back, 2 * pair], far[back, 2 * pair + 1]], axis=0),
             )
             fold_in(refs, starts, pair_lanes(pair), result)
         for inner in range(tile // step):
@@ -309,7 +308,7 @@
                 q[start : start + step, pair_lanes(pair)],
                 kv[key_tile : key_tile + tile, KEYS],
                 kv[key_tile : key_tile + tile, VALUES],
-                stacked(near, pair, slice(inner * step, (inner + 1) * step), slice(0, tile), closed),
+                stacked(near, pair, slice(inner * step, (inner + 1) * step), slice(0, tile)),
             )
             where = (slice(start, start + step), pair_lanes(pair))
             old = tuple(ref[where] for ref in refs)
@@ -322,7 +321,7 @@
                 rows_of(q, starts, pair_lanes(pair)),
                 rows_of(kv, key_starts, KEYS),
                 rows_of(kv, key_starts, VALUES),
-                stacked(mid, pair, slice(0, size), slice(0, size), closed),
+                stacked(mid, pair, slice(0, size), slice(0, size)),
             )
             fold_in(refs, starts, pair_lanes(pair), result)
 
@@ -335,7 +334,7 @@
         place_pair(kv.at[n], kv_mine[n], kv_part[n])
     for ref, first, second in zip(refs, mine, part):
         place_pair(ref, first, second)
-    windows(refs, q_ref, [kv.at[0], kv.at[1]], near, mid, far, False, 0.0)
+    windows(refs, q_ref, [kv.at[0], kv.at[1]], near, mid, far, False)
 
 
 def pair_attention(bias, q_mine, q_part, kv_mine, kv_part, mine, part, after=()):
@@ -353,10 +352,13 @@
 
 def before_kernel(near, mid, far, q, kv_a0, kv_b0, kv_a1, kv_b1, o_in, m_in, l_in, *rest):
     o_ref, m_ref, l_ref, past = rest[-4:]
-    place_pair(past.at[0], kv_a0, kv_b0)
-    place_pair(past.at[1], kv_a1, kv_b1)
     o_ref[...], m_ref[...], l_ref[...] = o_in[...], m_in[...], l_in[...]
-    windows((o_ref, m_ref, l_ref), q, [past.at[0], past.at[1]], near, mid, far, True, closed_gate())
+
+    @pl.when(places()[1] > 0)
+    def _():
+        place_pair(past.at[0], kv_a0, kv_b0)
+        place_pair(past.at[1], kv_a1, kv_b1)
+        windows((o_ref, m_ref, l_ref), q, [past.at[0], past.at[1]], near, mid, far, True)
 
 
 def before_attention(bias, q, past, state, after=()):
@@ -413,22 +415,31 @@
     block = q_a.shape[0]
     tile = FAR_DILATION * SUB
     chunks = block // tile
-    place_pair(q, q_a.at[:, pair_lanes(pair)], q_b.at[:, pair_lanes(pair)])
-    place_pair(kv, kv_a, kv_b)
-    closed = closed_gate()
-    bias = jnp.concatenate([far[2, 2 * pair], far[2, 2 * pair + 1]], axis=0) + closed
-    for residue in range(FAR_DILATION):
-        starts = far_starts(residue, 2 * chunks)
-        o, m, l = attend(rows_of(q, starts, KEYS), rows_of(kv, starts, KEYS), rows_of(kv, starts, VALUES), bias)
-        some = l > 0.0
-        safe = jnp.where(some, l, 1.0)
-        o = o / safe
-        s = jnp.where(some, m + jnp.log2(safe), FLOOR)
-        for n, start in enumerate(starts):
-            where = pl.ds(start, SUB)
-            out_ref[where] = o[n * SUB : (n + 1) * SUB].astype(BF16)
-            sums[where] = s[n * SUB : (n + 1) * SUB]
-    store_packed(out_ref, 2 * block, pack_sums([sums[:block], sums[block:]]))
+    _, z, _ = places()
+    useful = (z > 0) & (z + 1 < lax.axis_size("sp") // 2)
+
+    @pl.when(useful)
+    def _():
+        place_pair(q, q_a.at[:, pair_lanes(pair)], q_b.at[:, pair_lanes(pair)])
+        place_pair(kv, kv_a, kv_b)
+        bias = jnp.concatenate([far[2, 2 * pair], far[2, 2 * pair + 1]], axis=0)
+        for residue in range(FAR_DILATION):
+            starts = far_starts(residue, 2 * chunks)
+            o, m, l = attend(rows_of(q, starts, KEYS), rows_of(kv, starts, KEYS), rows_of(kv, starts, VALUES), bias)
+            some = l > 0.0
+            safe = jnp.where(some, l, 1.0)
+            o = o / safe
+            s = jnp.where(some, m + jnp.log2(safe), FLOOR)
+            for n, start in enumerate(starts):
+                where = pl.ds(start, SUB)
+                out_ref[where] = o[n * SUB : (n + 1) * SUB].astype(BF16)
+                sums[where] = s[n * SUB : (n + 1) * SUB]
+        store_packed(out_ref, 2 * block, pack_sums([sums[:block], sums[block:]]))
+
+    @pl.when(jnp.logical_not(useful))
+    def _():
+        out_ref[: 2 * block] = jnp.zeros((2 * block, 128), BF16)
+        store_packed(out_ref, 2 * block, pack_sums([jnp.full((block, 128), FLOOR, F32)] * 2))
 
 
 def remote_attention(pair, far, q_a, q_b, kv_a, kv_b, after=()):
@@ -553,7 +564,7 @@
     crossed = [(2 * n + c, 2 * (n ^ 1) + 1 - c) for n in range(count) for c in range(2)]
 
     x_other = lax.ppermute(tokens, "tp", swap)
-    kv_t0, kv_m0 = project(tokens, x_other, [w_key, w_value], [0])
+    kv_t0, kv_m0 = project(tokens, x_other, [w_key[:, :256], w_value[:, :256]], [0])
     kv_p0 = lax.ppermute(kv_t0, "sp", beside)
     kv_a0 = lax.ppermute(kv_m0, "sp", ahead)
     q_t, q_m = project(tokens, x_other, [w_query], [0, 256])
@@ -573,7 +584,7 @@
     far_p = lax.ppermute(far0, "sp", ahead)
     *state, q = pair_attention(bias, q_m, q_p, (kv_m0, kv_m1), (kv_p0, kv_p1), mine, part)
     far1 = remote_attention(1, bias[2], q_a, q_b, kv_a1, kv_b1)
-    far_m = lax.ppermute(far1, "sp", ahead)
+    far_m = lax.ppermute(far1, "sp", onward)
     state = before_attention(bias, q, (kv_a0, kv_b0, kv_a1, kv_b1), state)
     pieces = []
     for pair, far in enumerate((far_p, far_m)):

time: 70.2 us -> 69.5 us (0.990)
  Pallas kernels: 24.6 us -> 19.7 us
  starting transfers between devices: 26 us -> 30 us
  waiting for transfers between devices: 18.5 us -> 16.9 us
  local copies, waits for them, and re-layouts: 0.02 us -> 1.58 us
    pallas_call x13, Pallas kernels: 24.6 us -> 19.7 us  [call(): pl.pallas_call(kernel, out_shape=[jax.ShapeDtypeStruct(shape, kind) for s...]
    ppermute x1, starting transfers between devices: 0.09 us -> 3.04 us  [layer(): kv_p0 = lax.ppermute(kv_t0, 'sp', beside)]
    ppermute x1, starting transfers between devices: 1.58 us -> 4.5 us  [layer(): far_m = lax.ppermute(far1, 'sp', onward)]
    ppermute x1, starting transfers between devices: 2.94 us -> 0.09 us  [layer(): q_p = lax.ppermute(q_t, 'sp', beside)]
    ppermute x1, waiting for transfers between devices: 1.86 us -> 0.48 us  [layer(): x_other = lax.ppermute(tokens, 'tp', swap)]
    slice x0 -> x2, local copies, waits for them, and re-layouts: none -> 1.36 us  [the longest x1 1.29 us: layer(): w_key[:, :256]]
    ppermute x1, waiting for transfers between devices: 0.01 us -> 1.2 us  [layer(): q_p = lax.ppermute(q_t, 'sp', beside)]
    ppermute x1, waiting for transfers between devices: 1.2 us -> 0.01 us  [layer(): kv_p0 = lax.ppermute(kv_t0, 'sp', beside)]
  transfers between devices with their start and end apart: 19 -> 19, of which waited for: 7 -> 7; matrix products, arithmetic and copies ran while one was open for 0% -> 2% of each run, Pallas kernels for 32% -> 25%
where the time goes in v5:
time: 69.5 us; the launch traced here: 69 us
  starting transfers between devices  30 us (43%)
  Pallas kernels  19.7 us (28%)
  waiting for transfers between devices  16.9 us (24%)
  local copies, waits for them, and re-layouts  1.58 us (2%)
  between operations  0.85 us (1%)
    pallas_call x13, Pallas kernels, call(): pl.pallas_call(kernel, out_shape=[jax.ShapeDtypeStruct(shape, kind) for s...  19.7 us
    ppermute x1, waiting for transfers between devices, layer(): far_m = lax.ppermute(far1, 'sp', onward)  5.04 us
    ppermute x1, starting transfers between devices, layer(): far_m = lax.ppermute(far1, 'sp', onward)  4.5 us
    ppermute x1, waiting for transfers between devices, layer(): q_b = lax.ppermute(q_p, 'sp', back)  3.84 us
    ppermute x1, starting transfers between devices, layer(): kv_b0 = lax.ppermute(kv_p0, 'sp', onward)  3.71 us
    ppermute x1, waiting for transfers between devices, layer(): kv_p1 = lax.ppermute(kv_t1, 'sp', beside)  3.68 us
    ppermute x1, starting transfers between devices, layer(): kv_b1 = lax.ppermute(kv_p1, 'sp', onward)  3.48 us
    ppermute x2, starting transfers between devices, layer(): same = lax.ppermute(same, 'sp', beside)  3.04 us
  transfers between devices with their start and end apart: 19, of which 7 were waited for; matrix products, arithmetic and copies ran while one was open for 2% of the time, Pallas kernels for 25%

profile of v5, /device:TPU:0, one launch (start us, length us, event | category | flops | bytes accessed | tf_op | source)
XLA Modules:
  0.0 69.0 jit_solution(1209466629282341687)
XLA Ops:
  0.6 0.6 collective-permute-start
  1.2 0.1 collective-permute-start.18
  1.3 1.3 %slice.6.refs_2_ = bf16[2048,256]{1,0:T(8,128)(2,1)S(1)} slice(bf16[2048,512]{1,0:T(8,128)(2,1)} %refs_2_.3), slice={[0:2048], [0:256]} | slice | bytes 2097152 | tf_op jit(solution)/shard_map/slice | solution.py:567
  2.6 0.1 slice.7.refs_3_
  2.7 0.0 copy-start
  2.7 0.5 shard_map.68
  3.2 0.0 copy-start.4
  3.2 0.5 collective-permute-done.refs_1_
  3.7 0.2 copy-done
  3.9 1.7 %shard_map.70 = (bf16[512,256]{1,0:T(8,128)(2,1)S(1)}, bf16[512,256]{1,0:T(8,128)(2,1)S(1)}) custom-call(bf16[256,2048]{1,0:T(8,128)(2,1)S(1)} %copy-done, bf16[256,2048]{1,0:T(8,128)(2,1)S(1)} %collective-permute-done.refs_1_, bf16[2048,256]{1,0:T(8,128)(2,1)S(1)} %slice.6.refs_2_, bf16[2048,256]{1,0:T(8,128)(2,1)S(1)} %slice.7.refs_3_), custom_call_target="tpu_custom_call" | custom-call | flops 1073741824 | bytes 1000000 | tf_op jit(solution)/shard_map/pallas_call | solution.py:49
  5.6 0.0 copy-start.1
  5.6 3.0 %collective-permute-start.2 = (bf16[512,256]{1,0:T(8,128)(2,1)S(1)}, bf16[512,256]{1,0:T(8,128)(2,1)S(1)}, u32[]{:S(2)}, u32[]{:S(2)}) collective-permute-start(bf16[512,256]{1,0:T(8,128)(2,1)S(1)} %get-tuple-element.41), channel_id=1, source_target_pairs={{0,2},{2,0},{4,6},{6,4},{8,10},{10,8},{12,14},{14,12},{1,3},{3,1},... | collective-permute-start | bytes 786440 | tf_op jit(solution)/shard_map/ppermute | solution.py:568
  8.6 1.7 %shard_map.69 = (bf16[512,256]{1,0:T(8,128)(2,1)S(1)}, bf16[512,256]{1,0:T(8,128)(2,1)S(1)}) custom-call(bf16[256,2048]{1,0:T(8,128)(2,1)S(1)} %copy-done, bf16[256,2048]{1,0:T(8,128)(2,1)S(1)} %collective-permute-done.refs_1_, bf16[2048,512]{1,0:T(8,128)(2,1)S(1)} %copy-done.4), custom_call_target="tpu_custom_call" | custom-call | flops 1073741824 | bytes 1000000 | tf_op jit(solution)/shard_map/pallas_call | solution.py:49
  10.3 0.1 collective-permute-start.1
  10.4 1.7 %shard_map.71 = (bf16[512,256]{1,0:T(8,128)(2,1)S(1)}, bf16[512,256]{1,0:T(8,128)(2,1)S(1)}) custom-call(bf16[256,2048]{1,0:T(8,128)(2,1)S(1)} %copy-done, bf16[256,2048]{1,0:T(8,128)(2,1)S(1)} %collective-permute-done.refs_1_, bf16[2048,512]{1,0:T(8,128)(2,1)S(1)} %copy-done.1, bf16[2048,512]{1,0:T(8,128)(2,1)S(1)} %copy-done.2), custom_call_target="tpu_custom_call" | custom-call | flops 1073741824 | bytes 1000000 | tf_op jit(solution)/shard_map/pallas_call | solution.py:49
  12.0 2.1 %collective-permute-start.3 = (bf16[512,256]{1,0:T(8,128)(2,1)S(1)}, bf16[512,256]{1,0:T(8,128)(2,1)S(1)}, u32[]{:S(2)}, u32[]{:S(2)}) collective-permute-start(bf16[512,256]{1,0:T(8,128)(2,1)S(1)} %get-tuple-element.42), channel_id=1, source_target_pairs={{0,2},{2,0},{4,6},{6,4},{8,10},{10,8},{12,14},{14,12},{1,3},{3,1},... | collective-permute-start | bytes 786440 | tf_op jit(solution)/shard_map/ppermute | solution.py:574
  14.1 1.6 %collective-permute-start.4 = (bf16[512,256]{1,0:T(8,128)(2,1)S(1)}, bf16[512,256]{1,0:T(8,128)(2,1)S(1)}, u32[]{:S(2)}, u32[]{:S(2)}) collective-permute-start(bf16[512,256]{1,0:T(8,128)(2,1)S(1)} %get-tuple-element.39.kv0.rest_0_), channel_id=1, source_target_pairs={{0,4},{2,6},{4,8},{6,10},{8,12},{10,14},{12,0},{14,2},{1,5},{3,7},... | collective-permute-start | bytes 786440 | tf_op jit(solution)/shard_map/ppermute | solution.py:569
  15.7 2.9 %shard_map.72 = (f32[512,256]{1,0:T(8,128)S(1)}, f32[512,256]{1,0:T(8,128)S(1)}, f32[512,256]{1,0:T(8,128)S(1)}) custom-call(f32[4,256,512]{2,1,0:T(8,128)S(1)} %get-tuple-element.34.near, f32[4,128,256]{2,1,0:T(8,128)S(1)} %get-tuple-element.35.mid, bf16[512,256]{1,0:T(8,128)(2,1)S(1)} %get-tuple-element.37.q.q_mine, ...), custom_call_target="tpu_custom_call" | custom-call | flops 4000000000 | bytes 1000000 | tf_op jit(solution)/shard_map/pallas_call | solution.py:49
  18.5 0.0 collective-permute-done.2.kv0.rest_2_
  18.6 1.6 %collective-permute-start.6 = (bf16[512,256]{1,0:T(8,128)(2,1)S(1)}, bf16[512,256]{1,0:T(8,128)(2,1)S(1)}, u32[]{:S(2)}, u32[]{:S(2)}) collective-permute-start(bf16[512,256]{1,0:T(8,128)(2,1)S(1)} %get-tuple-element.40.kv1.rest_1_), channel_id=1, source_target_pairs={{0,4},{2,6},{4,8},{6,10},{8,12},{10,14},{12,0},{14,2},{1,5},{3,7},... | collective-permute-start | bytes 786440 | tf_op jit(solution)/shard_map/ppermute | solution.py:575
  20.2 1.2 %collective-permute-done.1.q.q_part = bf16[512,256]{1,0:T(8,128)(2,1)S(1)} collective-permute-done((bf16[512,256]{1,0:T(8,128)(2,1)S(1)}, bf16[512,256]{1,0:T(8,128)(2,1)S(1)}, u32[]{:S(2)}, u32[]{:S(2)}) %collective-permute-start.1) | collective-permute-done | bytes 262176 | tf_op jit(solution)/shard_map/ppermute | solution.py:571
  21.4 1.3 %collective-permute-start.8 = (bf16[512,256]{1,0:T(8,128)(2,1)S(1)}, bf16[512,256]{1,0:T(8,128)(2,1)S(1)}, u32[]{:S(2)}, u32[]{:S(2)}) collective-permute-start(bf16[512,256]{1,0:T(8,128)(2,1)S(1)} %get-tuple-element.37.q.q_mine), channel_id=1, source_target_pairs={{4,0},{6,2},{8,4},{10,6},{12,8},{14,10},{5,1},{7,3},{9,5},{11,7},{... | collective-permute-start | bytes 786440 | tf_op jit(solution)/shard_map/ppermute | solution.py:572
  22.7 3.7 %collective-permute-done.3.kv1.rest_3_ = bf16[512,256]{1,0:T(8,128)(2,1)S(1)} collective-permute-done((bf16[512,256]{1,0:T(8,128)(2,1)S(1)}, bf16[512,256]{1,0:T(8,128)(2,1)S(1)}, u32[]{:S(2)}, u32[]{:S(2)}) %collective-permute-start.3) | collective-permute-done | bytes 262176 | tf_op jit(solution)/shard_map/ppermute | solution.py:574
  26.4 3.7 %collective-permute-start.5 = (bf16[512,256]{1,0:T(8,128)(2,1)S(1)}, bf16[512,256]{1,0:T(8,128)(2,1)S(1)}, u32[]{:S(2)}, u32[]{:S(2)}) collective-permute-start(bf16[512,256]{1,0:T(8,128)(2,1)S(1)} %collective-permute-done.2.kv0.rest_2_), channel_id=1, source_target_pairs={{0,4},{2,6},{4,8},{6,10},{8,12},{10,14},{1,5},{3,7},{5,9},{7,11},{... | collective-permute-start | bytes 786440 | tf_op jit(solution)/shard_map/ppermute | solution.py:576
  30.1 2.9 %shard_map.73 = (f32[512,256]{1,0:T(8,128)S(1)}, f32[512,256]{1,0:T(8,128)S(1)}, f32[512,256]{1,0:T(8,128)S(1)}) custom-call(f32[4,256,512]{2,1,0:T(8,128)S(1)} %get-tuple-element.34.near, f32[4,128,256]{2,1,0:T(8,128)S(1)} %get-tuple-element.35.mid, bf16[512,256]{1,0:T(8,128)(2,1)S(1)} %collective-permute-done.1.q.q_part, ...), custom_call_target="tpu_custom_call" | custom-call | flops 4000000000 | bytes 1000000 | tf_op jit(solution)/shard_map/pallas_call | solution.py:49
  33.0 3.5 %collective-permute-start.7 = (bf16[512,256]{1,0:T(8,128)(2,1)S(1)}, bf16[512,256]{1,0:T(8,128)(2,1)S(1)}, u32[]{:S(2)}, u32[]{:S(2)}) collective-permute-start(bf16[512,256]{1,0:T(8,128)(2,1)S(1)} %collective-permute-done.3.kv1.rest_3_), channel_id=1, source_target_pairs={{0,4},{2,6},{4,8},{6,10},{8,12},{10,14},{1,5},{3,7},{5,9},{7,11},{... | collective-permute-start | bytes 786440 | tf_op jit(solution)/shard_map/ppermute | solution.py:578
  36.4 0.0 collective-permute-done.8.q_a
  36.5 1.5 %collective-permute-start.9 = (bf16[512,256]{1,0:T(8,128)(2,1)S(1)}, bf16[512,256]{1,0:T(8,128)(2,1)S(1)}, u32[]{:S(2)}, u32[]{:S(2)}) collective-permute-start(bf16[512,256]{1,0:T(8,128)(2,1)S(1)} %collective-permute-done.1.q.q_part), channel_id=1, source_target_pairs={{4,0},{6,2},{8,4},{10,6},{12,8},{14,10},{5,1},{7,3},{9,5},{11,7},{... | collective-permute-start | bytes 786440 | tf_op jit(solution)/shard_map/ppermute | solution.py:577
  37.9 3.4 %shard_map.74 = (f32[1024,256]{1,0:T(8,128)S(1)}, f32[1024,256]{1,0:T(8,128)S(1)}, f32[1024,256]{1,0:T(8,128)S(1)}, bf16[1024,256]{1,0:T(8,128)(2,1)S(1)}) custom-call(f32[4,256,512]{2,1,0:T(8,128)S(1)} %get-tuple-element.34.near, f32[4,128,256]{2,1,0:T(8,128)S(1)} %get-tuple-element.35.mid, f32[3,4,64,64]{3,2,1,0:T(8,128)S(1)} %get-tuple-element.36.far, ...), custom_call_target="tpu_custom_call" | custom-call | flops 4000000000 | bytes 1000000 | tf_op jit(solution)/shard_map/pallas_call | solution.py:49
  41.4 3.8 %collective-permute-done.9.q_b = bf16[512,256]{1,0:T(8,128)(2,1)S(1)} collective-permute-done((bf16[512,256]{1,0:T(8,128)(2,1)S(1)}, bf16[512,256]{1,0:T(8,128)(2,1)S(1)}, u32[]{:S(2)}, u32[]{:S(2)}) %collective-permute-start.9) | collective-permute-done | bytes 262176 | tf_op jit(solution)/shard_map/ppermute | solution.py:577
  45.2 0.2 shard_map.78
  45.4 4.5 %collective-permute-start.14 = (bf16[1088,128]{1,0:T(8,128)(2,1)S(1)}, bf16[1088,128]{1,0:T(8,128)(2,1)S(1)}, u32[]{:S(2)}, u32[]{:S(2)}) collective-permute-start(bf16[1088,128]{1,0:T(8,128)(2,1)S(1)} %shard_map.78), channel_id=1, source_target_pairs={{0,4},{2,6},{4,8},{6,10},{8,12},{10,14},{1,5},{3,7},{5,9},{7,11},{... | collective-permute-start | bytes 835592 | tf_op jit(solution)/shard_map/ppermute | solution.py:587
  49.9 0.0 collective-permute-done.4.kv_a0.kv_a
  49.9 0.2 shard_map.76
  50.1 1.3 %collective-permute-start.10 = (bf16[1088,128]{1,0:T(8,128)(2,1)S(1)}, bf16[1088,128]{1,0:T(8,128)(2,1)S(1)}, u32[]{:S(2)}, u32[]{:S(2)}) collective-permute-start(bf16[1088,128]{1,0:T(8,128)(2,1)S(1)} %shard_map.76), channel_id=1, source_target_pairs={{0,4},{2,6},{4,8},{6,10},{8,12},{10,14},{12,0},{14,2},{1,5},{3,7},... | collective-permute-start | bytes 835592 | tf_op jit(solution)/shard_map/ppermute | solution.py:584
  51.5 0.2 shard_map.75
  51.7 5.0 %collective-permute-done.14.far_in = bf16[1088,128]{1,0:T(8,128)(2,1)S(1)} collective-permute-done((bf16[1088,128]{1,0:T(8,128)(2,1)S(1)}, bf16[1088,128]{1,0:T(8,128)(2,1)S(1)}, u32[]{:S(2)}, u32[]{:S(2)}) %collective-permute-start.14) | collective-permute-done | bytes 278560 | tf_op jit(solution)/shard_map/ppermute | solution.py:587
  56.7 1.1 %shard_map.79 = (bf16[256,128]{1,0:T(8,128)(2,1)S(1)}, bf16[256,128]{1,0:T(8,128)(2,1)S(1)}, bf16[320,128]{1,0:T(8,128)(2,1)S(1)}, bf16[256,128]{1,0:T(8,128)(2,1)S(1)}, bf16[16,512]{1,0:T(8,128)(2,1)S(1)}) custom-call(f32[1024,256]{1,0:T(8,128)S(1)} %get-tuple-element.53.o_in, f32[1024,256]{1,0:T(8,128)S(1)} %get-tuple-element.54.m_in, ...), custom_call_target="tpu_custom_call" | custom-call | flops 1000000000 | bytes 1000000 | tf_op jit(solution)/shard_map/pallas_call | solution.py:49
  57.8 1.5 %collective-permute-start.15 = (bf16[320,128]{1,0:T(8,128)(2,1)S(1)}, bf16[320,128]{1,0:T(8,128)(2,1)S(1)}, u32[]{:S(2)}, u32[]{:S(2)}) collective-permute-start(bf16[320,128]{1,0:T(8,128)(2,1)S(1)} %get-tuple-element.62), channel_id=1, source_target_pairs={{0,2},{2,0},{4,6},{6,4},{8,10},{10,8},{12,14},{14,12},{1,3},{3,1},... | collective-permute-start | bytes 245768 | tf_op jit(solution)/shard_map/ppermute | solution.py:592
  59.3 0.0 collective-permute-start.16
  59.3 0.7 collective-permute-start.17
  60.0 0.0 collective-permute-done.10.far_in
  60.0 1.1 %shard_map.77 = (bf16[256,128]{1,0:T(8,128)(2,1)S(1)}, bf16[256,128]{1,0:T(8,128)(2,1)S(1)}, bf16[320,128]{1,0:T(8,128)(2,1)S(1)}, bf16[256,128]{1,0:T(8,128)(2,1)S(1)}, bf16[16,512]{1,0:T(8,128)(2,1)S(1)}) custom-call(f32[1024,256]{1,0:T(8,128)S(1)} %get-tuple-element.53.o_in, f32[1024,256]{1,0:T(8,128)S(1)} %get-tuple-element.54.m_in, ...), custom_call_target="tpu_custom_call" | custom-call | flops 1000000000 | bytes 1000000 | tf_op jit(solution)/shard_map/pallas_call | solution.py:49
  61.0 1.5 %collective-permute-start.11 = (bf16[320,128]{1,0:T(8,128)(2,1)S(1)}, bf16[320,128]{1,0:T(8,128)(2,1)S(1)}, u32[]{:S(2)}, u32[]{:S(2)}) collective-permute-start(bf16[320,128]{1,0:T(8,128)(2,1)S(1)} %get-tuple-element.57), channel_id=1, source_target_pairs={{0,2},{2,0},{4,6},{6,4},{8,10},{10,8},{12,14},{14,12},{1,3},{3,1},... | collective-permute-start | bytes 245768 | tf_op jit(solution)/shard_map/ppermute | solution.py:592
  62.6 0.4 collective-permute-done.17.refs_8_
  63.0 1.5 %collective-permute-start.13 = (bf16[256,128]{1,0:T(8,128)(2,1)S(1)}, bf16[256,128]{1,0:T(8,128)(2,1)S(1)}, u32[]{:S(2)}, u32[]{:S(2)}) collective-permute-start(bf16[256,128]{1,0:T(8,128)(2,1)S(1)} %get-tuple-element.59), channel_id=1, source_target_pairs={{0,3},{1,2},{2,1},{3,0},{4,7},{5,6},{6,5},{7,4},{8,11},{9,10},{10,... | collective-permute-start | bytes 196616 | tf_op jit(solution)/shard_map/ppermute | solution.py:593
  64.6 2.1 %collective-permute-done.13.refs_3_ = bf16[256,128]{1,0:T(8,128)(2,1)S(1)} collective-permute-done((bf16[256,128]{1,0:T(8,128)(2,1)S(1)}, bf16[256,128]{1,0:T(8,128)(2,1)S(1)}, u32[]{:S(2)}, u32[]{:S(2)}) %collective-permute-start.13) | collective-permute-done | bytes 65568 | tf_op jit(solution)/shard_map/ppermute | solution.py:593
  66.7 2.3 %shard_map.80 = (bf16[256,2048]{1,0:T(8,128)(2,1)}, f32[8,512]{1,0:T(8,128)}) custom-call(bf16[256,128]{1,0:T(8,128)(2,1)S(1)} %get-tuple-element.56.refs_0_, bf16[320,128]{1,0:T(8,128)(2,1)S(1)} %collective-permute-done.11.refs_1_, bf16[256,128]{1,0:T(8,128)(2,1)S(1)} %collective-permute-done.12.refs_2_, ...), custom_call_target="tpu_custom_call" | custom-call | flops 1073741824 | bytes 1000000 | tf_op jit(solution)/shard_map/pallas_call | solution.py:49
  (15 shorter events, 0.0 us)
Async XLA Ops:
  0.6 1.9 %copy-start.2 = (bf16[2048,512]{1,0:T(8,128)(2,1)S(1)}, bf16[2048,512]{1,0:T(8,128)(2,1)}, u32[]{:S(2)}) copy-start(bf16[2048,512]{1,0:T(8,128)(2,1)} %refs_3_.1) | copy-start | bytes 6291460
  0.6 3.1 %collective-permute-start = (bf16[256,2048]{1,0:T(8,128)(2,1)}, bf16[256,2048]{1,0:T(8,128)(2,1)S(1)}, u32[]{:S(2)}, u32[]{:S(2)}) collective-permute-start(bf16[256,2048]{1,0:T(8,128)(2,1)} %refs_0_.5), channel_id=1, source_target_pairs={{0,1},{1,0},{2,3},{3,2},{4,5},{5,4},{6,7},{7,6},{8,9},{9,8},{10,11... | collective-permute-start | bytes 3145736 | tf_op jit(solution)/shard_map/ppermute | solution.py:566
  1.2 65.5 %collective-permute-start.18 = (bf16[512,2048]{1,0:T(8,128)(2,1)}, bf16[512,2048]{1,0:T(8,128)(2,1)S(1)}, u32[]{:S(2)}, u32[]{:S(2)}) collective-permute-start(bf16[512,2048]{1,0:T(8,128)(2,1)} %refs_10_.1), channel_id=1, source_target_pairs={{0,1},{1,0},{2,3},{3,2},{4,5},{5,4},{6,7},{7,6},{8,9},{9,8},{10,11... | collective-permute-start | bytes 6291464 | tf_op jit(solution)/shard_map/ppermute | solution.py:579
  2.7 1.2 %copy-start = (bf16[256,2048]{1,0:T(8,128)(2,1)S(1)}, bf16[256,2048]{1,0:T(8,128)(2,1)}, u32[]{:S(2)}) copy-start(bf16[256,2048]{1,0:T(8,128)(2,1)} %refs_0_.5) | copy-start | bytes 3145732
  3.2 5.4 %copy-start.4 = (bf16[2048,512]{1,0:T(8,128)(2,1)S(1)}, bf16[2048,512]{1,0:T(8,128)(2,1)}, u32[]{:S(2)}) copy-start(bf16[2048,512]{1,0:T(8,128)(2,1)} %refs_2_.2) | copy-start | bytes 6291460
  5.6 4.8 %copy-start.1 = (bf16[2048,512]{1,0:T(8,128)(2,1)S(1)}, bf16[2048,512]{1,0:T(8,128)(2,1)}, u32[]{:S(2)}) copy-start(bf16[2048,512]{1,0:T(8,128)(2,1)} %refs_2_.3) | copy-start | bytes 6291460
  5.6 13.0 %collective-permute-start.2 = (bf16[512,256]{1,0:T(8,128)(2,1)S(1)}, bf16[512,256]{1,0:T(8,128)(2,1)S(1)}, u32[]{:S(2)}, u32[]{:S(2)}) collective-permute-start(bf16[512,256]{1,0:T(8,128)(2,1)S(1)} %get-tuple-element.41), channel_id=1, source_target_pairs={{0,2},{2,0},{4,6},{6,4},{8,10},{10,8},{12,14},{14,12},{1,3},{3,1},... | collective-permute-start | bytes 786440 | tf_op jit(solution)/shard_map/ppermute | solution.py:568
  10.3 11.1 %collective-permute-start.1 = (bf16[512,256]{1,0:T(8,128)(2,1)S(1)}, bf16[512,256]{1,0:T(8,128)(2,1)S(1)}, u32[]{:S(2)}, u32[]{:S(2)}) collective-permute-start(bf16[512,256]{1,0:T(8,128)(2,1)S(1)} %get-tuple-element.38), channel_id=1, source_target_pairs={{0,2},{2,0},{4,6},{6,4},{8,10},{10,8},{12,14},{14,12},{1,3},{3,1},... | collective-permute-start | bytes 786440 | tf_op jit(solution)/shard_map/ppermute | solution.py:571
  12.0 14.3 %collective-permute-start.3 = (bf16[512,256]{1,0:T(8,128)(2,1)S(1)}, bf16[512,256]{1,0:T(8,128)(2,1)S(1)}, u32[]{:S(2)}, u32[]{:S(2)}) collective-permute-start(bf16[512,256]{1,0:T(8,128)(2,1)S(1)} %get-tuple-element.42), channel_id=1, source_target_pairs={{0,2},{2,0},{4,6},{6,4},{8,10},{10,8},{12,14},{14,12},{1,3},{3,1},... | collective-permute-start | bytes 786440 | tf_op jit(solution)/shard_map/ppermute | solution.py:574
  14.1 35.8 %collective-permute-start.4 = (bf16[512,256]{1,0:T(8,128)(2,1)S(1)}, bf16[512,256]{1,0:T(8,128)(2,1)S(1)}, u32[]{:S(2)}, u32[]{:S(2)}) collective-permute-start(bf16[512,256]{1,0:T(8,128)(2,1)S(1)} %get-tuple-element.39.kv0.rest_0_), channel_id=1, source_target_pairs={{0,4},{2,6},{4,8},{6,10},{8,12},{10,14},{12,0},{14,2},{1,5},{3,7},... | collective-permute-start | bytes 786440 | tf_op jit(solution)/shard_map/ppermute | solution.py:569
  18.6 14.4 %collective-permute-start.6 = (bf16[512,256]{1,0:T(8,128)(2,1)S(1)}, bf16[512,256]{1,0:T(8,128)(2,1)S(1)}, u32[]{:S(2)}, u32[]{:S(2)}) collective-permute-start(bf16[512,256]{1,0:T(8,128)(2,1)S(1)} %get-tuple-element.40.kv1.rest_1_), channel_id=1, source_target_pairs={{0,4},{2,6},{4,8},{6,10},{8,12},{10,14},{12,0},{14,2},{1,5},{3,7},... | collective-permute-start | bytes 786440 | tf_op jit(solution)/shard_map/ppermute | solution.py:575
  21.4 15.1 %collective-permute-start.8 = (bf16[512,256]{1,0:T(8,128)(2,1)S(1)}, bf16[512,256]{1,0:T(8,128)(2,1)S(1)}, u32[]{:S(2)}, u32[]{:S(2)}) collective-permute-start(bf16[512,256]{1,0:T(8,128)(2,1)S(1)} %get-tuple-element.37.q.q_mine), channel_id=1, source_target_pairs={{4,0},{6,2},{8,4},{10,6},{12,8},{14,10},{5,1},{7,3},{9,5},{11,7},{... | collective-permute-start | bytes 786440 | tf_op jit(solution)/shard_map/ppermute | solution.py:572
  26.4 23.6 %collective-permute-start.5 = (bf16[512,256]{1,0:T(8,128)(2,1)S(1)}, bf16[512,256]{1,0:T(8,128)(2,1)S(1)}, u32[]{:S(2)}, u32[]{:S(2)}) collective-permute-start(bf16[512,256]{1,0:T(8,128)(2,1)S(1)} %collective-permute-done.2.kv0.rest_2_), channel_id=1, source_target_pairs={{0,4},{2,6},{4,8},{6,10},{8,12},{10,14},{1,5},{3,7},{5,9},{7,11},{... | collective-permute-start | bytes 786440 | tf_op jit(solution)/shard_map/ppermute | solution.py:576
  33.0 8.4 %collective-permute-start.7 = (bf16[512,256]{1,0:T(8,128)(2,1)S(1)}, bf16[512,256]{1,0:T(8,128)(2,1)S(1)}, u32[]{:S(2)}, u32[]{:S(2)}) collective-permute-start(bf16[512,256]{1,0:T(8,128)(2,1)S(1)} %collective-permute-done.3.kv1.rest_3_), channel_id=1, source_target_pairs={{0,4},{2,6},{4,8},{6,10},{8,12},{10,14},{1,5},{3,7},{5,9},{7,11},{... | collective-permute-start | bytes 786440 | tf_op jit(solution)/shard_map/ppermute | solution.py:578
  36.5 8.7 %collective-permute-start.9 = (bf16[512,256]{1,0:T(8,128)(2,1)S(1)}, bf16[512,256]{1,0:T(8,128)(2,1)S(1)}, u32[]{:S(2)}, u32[]{:S(2)}) collective-permute-start(bf16[512,256]{1,0:T(8,128)(2,1)S(1)} %collective-permute-done.1.q.q_part), channel_id=1, source_target_pairs={{4,0},{6,2},{8,4},{10,6},{12,8},{14,10},{5,1},{7,3},{9,5},{11,7},{... | collective-permute-start | bytes 786440 | tf_op jit(solution)/shard_map/ppermute | solution.py:577
  45.4 11.3 %collective-permute-start.14 = (bf16[1088,128]{1,0:T(8,128)(2,1)S(1)}, bf16[1088,128]{1,0:T(8,128)(2,1)S(1)}, u32[]{:S(2)}, u32[]{:S(2)}) collective-permute-start(bf16[1088,128]{1,0:T(8,128)(2,1)S(1)} %shard_map.78), channel_id=1, source_target_pairs={{0,4},{2,6},{4,8},{6,10},{8,12},{10,14},{1,5},{3,7},{5,9},{7,11},{... | collective-permute-start | bytes 835592 | tf_op jit(solution)/shard_map/ppermute | solution.py:587
  50.1 9.8 %collective-permute-start.10 = (bf16[1088,128]{1,0:T(8,128)(2,1)S(1)}, bf16[1088,128]{1,0:T(8,128)(2,1)S(1)}, u32[]{:S(2)}, u32[]{:S(2)}) collective-permute-start(bf16[1088,128]{1,0:T(8,128)(2,1)S(1)} %shard_map.76), channel_id=1, source_target_pairs={{0,4},{2,6},{4,8},{6,10},{8,12},{10,14},{12,0},{14,2},{1,5},{3,7},... | collective-permute-start | bytes 835592 | tf_op jit(solution)/shard_map/ppermute | solution.py:584
  57.8 8.9 %copy-start.3 = (bf16[512,2048]{1,0:T(8,128)(2,1)S(1)}, bf16[512,2048]{1,0:T(8,128)(2,1)}, u32[]{:S(2)}) copy-start(bf16[512,2048]{1,0:T(8,128)(2,1)} %refs_10_.1) | copy-start | bytes 6291460
  57.8 8.9 %collective-permute-start.15 = (bf16[320,128]{1,0:T(8,128)(2,1)S(1)}, bf16[320,128]{1,0:T(8,128)(2,1)S(1)}, u32[]{:S(2)}, u32[]{:S(2)}) collective-permute-start(bf16[320,128]{1,0:T(8,128)(2,1)S(1)} %get-tuple-element.62), channel_id=1, source_target_pairs={{0,2},{2,0},{4,6},{6,4},{8,10},{10,8},{12,14},{14,12},{1,3},{3,1},... | collective-permute-start | bytes 245768 | tf_op jit(solution)/shard_map/ppermute | solution.py:592
  59.3 3.3 %collective-permute-start.16 = (bf16[256,128]{1,0:T(8,128)(2,1)S(1)}, bf16[256,128]{1,0:T(8,128)(2,1)S(1)}, u32[]{:S(2)}, u32[]{:S(2)}) collective-permute-start(bf16[256,128]{1,0:T(8,128)(2,1)S(1)} %get-tuple-element.63), channel_id=1, source_target_pairs={{0,1},{1,0},{2,3},{3,2},{4,5},{5,4},{6,7},{7,6},{8,9},{9,8},{10,11... | collective-permute-start | bytes 196616 | tf_op jit(solution)/shard_map/ppermute | solution.py:594
  59.3 3.7 %collective-permute-start.17 = (bf16[256,128]{1,0:T(8,128)(2,1)S(1)}, bf16[256,128]{1,0:T(8,128)(2,1)S(1)}, u32[]{:S(2)}, u32[]{:S(2)}) collective-permute-start(bf16[256,128]{1,0:T(8,128)(2,1)S(1)} %get-tuple-element.64), channel_id=1, source_target_pairs={{0,3},{1,2},{2,1},{3,0},{4,7},{5,6},{6,5},{7,4},{8,11},{9,10},{10,... | collective-permute-start | bytes 196616 | tf_op jit(solution)/shard_map/ppermute | solution.py:593
  61.0 5.7 %collective-permute-start.11 = (bf16[320,128]{1,0:T(8,128)(2,1)S(1)}, bf16[320,128]{1,0:T(8,128)(2,1)S(1)}, u32[]{:S(2)}, u32[]{:S(2)}) collective-permute-start(bf16[320,128]{1,0:T(8,128)(2,1)S(1)} %get-tuple-element.57), channel_id=1, source_target_pairs={{0,2},{2,0},{4,6},{6,4},{8,10},{10,8},{12,14},{14,12},{1,3},{3,1},... | collective-permute-start | bytes 245768 | tf_op jit(solution)/shard_map/ppermute | solution.py:592
  62.6 2.0 %collective-permute-start.12 = (bf16[256,128]{1,0:T(8,128)(2,1)S(1)}, bf16[256,128]{1,0:T(8,128)(2,1)S(1)}, u32[]{:S(2)}, u32[]{:S(2)}) collective-permute-start(bf16[256,128]{1,0:T(8,128)(2,1)S(1)} %get-tuple-element.58), channel_id=1, source_target_pairs={{0,1},{1,0},{2,3},{3,2},{4,5},{5,4},{6,7},{7,6},{8,9},{9,8},{10,11... | collective-permute-start | bytes 196616 | tf_op jit(solution)/shard_map/ppermute | solution.py:594
  63.0 3.7 %collective-permute-start.13 = (bf16[256,128]{1,0:T(8,128)(2,1)S(1)}, bf16[256,128]{1,0:T(8,128)(2,1)S(1)}, u32[]{:S(2)}, u32[]{:S(2)}) collective-permute-start(bf16[256,128]{1,0:T(8,128)(2,1)S(1)} %get-tuple-element.59), channel_id=1, source_target_pairs={{0,3},{1,2},{2,1},{3,0},{4,7},{5,6},{6,5},{7,4},{8,11},{9,10},{10,... | collective-permute-start | bytes 196616 | tf_op jit(solution)/shard_map/ppermute | solution.py:593

commit v6 on v5

--- a/solution.py
+++ b/solution.py
@@ -119,17 +119,41 @@
     return o1 * a + o2 * b, top, l1 * a + l2 * b
 
 
-def near_distance(keys_before, keys_own):
-    tile = FAR_DILATION * SUB
-    token = lambda n: FAR_DILATION * (n % SUB) + n // SUB
-    shape = (tile, (tile if keys_before else 0) + (tile if keys_own else 0))
-    row = token(lax.broadcasted_iota(jnp.int32, shape, 0))
+HALF = FAR_DILATION * SUB // 2
+
+
+def half_token(row, half):
+    size = SUB // 2
+    return FAR_DILATION * (size * half + row % size) + row // size
+
+
+def near_distance(half):
+    shape = (HALF, 2 * HALF)
+    row = half_token(lax.broadcasted_iota(jnp.int32, shape, 0), half)
     col = lax.broadcasted_iota(jnp.int32, shape, 1)
-    if keys_before:
-        key = jnp.where(col < tile, token(col) - tile, token(col - tile))
+    if half == 0:
+        key = jnp.where(col < HALF, half_token(col, 1) - 2 * HALF, half_token(col - HALF, 0))
     else:
-        key = token(col)
+        key = jnp.where(col < HALF, half_token(col, 0), half_token(col - HALF, 1))
     return row - key
+
+
+def halves(ref, start, lanes):
+    rows = ref[pl.ds(start, 2 * HALF), lanes].astype(F32)
+    size = SUB // 2
+    return [
+        jnp.concatenate([rows[n * SUB + h * size : n * SUB + (h + 1) * size] for n in range(FAR_DILATION)], axis=0).astype(BF16)
+        for h in range(2)
+    ]
+
+
+def half_rows(start, half):
+    size = SUB // 2
+    return [slice(start + n * SUB + half * size, start + n * SUB + (half + 1) * size) for n in range(FAR_DILATION)]
+
+
+def near_bias(near, pair, half, columns):
+    return jnp.concatenate([near[2 * pair, half, :, columns], near[2 * pair + 1, half, :, columns]], axis=0)
 
 
 def middle_distance(keys_before, keys_own, chunks):
@@ -188,7 +212,7 @@
     y, _, tp = places()
     tile = FAR_DILATION * SUB
     chunks = mid.shape[1] // (tile // MIDDLE_DILATION)
-    near_steps = near_distance(True, True)
+    near_steps = [near_distance(half) for half in range(2)]
     mid_steps = middle_distance(True, True, chunks)
     row = lax.broadcasted_iota(jnp.int32, far.shape[2:], 0)
     col = lax.broadcasted_iota(jnp.int32, far.shape[2:], 1)
@@ -198,19 +222,19 @@
     ) * LOG2E
     for head in range(heads):
         slope = far_slope(head, (1, 1))
-        near[head] = bias_of(near_steps, slope, 1)
+        for half in range(2):
+            near[head, half] = bias_of(near_steps[half], slope, 1)
         mid[head] = bias_of(mid_steps, slope, MIDDLE_DILATION)
         for back in range(3):
             far[back, head] = bias_of(row - col + back * far.shape[3], slope, FAR_DILATION)
 
 
 def biases(block, heads):
-    tile = FAR_DILATION * SUB
     size = block // MIDDLE_DILATION
     reach = 2 * block // FAR_DILATION
     return call(
         bias_kernel,
-        [((heads, tile, 2 * tile), F32), ((heads, size, 2 * size), F32), ((3, heads, reach, reach), F32)],
+        [((heads, 2, HALF, 2 * HALF), F32), ((heads, size, 2 * size), F32), ((3, heads, reach, reach), F32)],
         [],
         limit=8,
         flops=10**9,
@@ -243,23 +267,31 @@
     tile = FAR_DILATION * SUB
     chunks = block // tile
     refs = (o_ref, m_ref, l_ref)
-    step = 128
     size = mid.shape[1]
     for pair, kv in enumerate((kv0, kv1)):
+        earlier = None
         for index in range(chunks):
-            first = max(index - 1, 0) * tile
-            width = tile if index == 0 else 2 * tile
-            columns = slice(2 * tile - width, 2 * tile)
-            for inner in range(tile // step):
-                start = index * tile + inner * step
+            start = index * tile
+            queries = halves(q, start, pair_lanes(pair))
+            keys, values = halves(kv, start, KEYS), halves(kv, start, VALUES)
+            for half in range(2):
+                if half == 1:
+                    seen_keys, seen_values, columns = keys, values, slice(0, tile)
+                elif earlier is None:
+                    seen_keys, seen_values, columns = keys[:1], values[:1], slice(HALF, tile)
+                else:
+                    seen_keys, seen_values = [earlier[0], keys[0]], [earlier[1], values[0]]
+                    columns = slice(0, tile)
                 result = attend(
-                    q[start : start + step, pair_lanes(pair)],
-                    kv[first : first + width, KEYS],
-                    kv[first : first + width, VALUES],
-                    stacked(near, pair, slice(inner * step, (inner + 1) * step), columns),
+                    queries[half],
+                    jnp.concatenate(seen_keys, axis=0),
+                    jnp.concatenate(seen_values, axis=0),
+                    near_bias(near, pair, half, columns),
                 )
-                for ref, value in zip(refs, result):
-                    ref[start : start + step, pair_lanes(pair)] = value
+                for n, rows in enumerate(half_rows(start, half)):
+                    for ref, value in zip(refs, result):
+                        ref[rows, pair_lanes(pair)] = value[n * SUB // 2 : (n + 1) * SUB // 2]
+            earlier = (keys[1], values[1])
         for residue in range(MIDDLE_DILATION):
             starts = middle_starts(0, residue, chunks)
             result = attend(
@@ -289,7 +321,6 @@
     back = 1 if before else 0
     query_tile = 0 if before else chunks
     key_tile = (2 * chunks - 1 if before else chunks - 1) * tile
-    step = 128
     size = mid.shape[1]
     for pair in range(len(kvs)):
         kv = kvs[pair]
@@ -302,17 +333,16 @@
                 jnp.concatenate([far[back, 2 * pair], far[back, 2 * pair + 1]], axis=0),
             )
             fold_in(refs, starts, pair_lanes(pair), result)
-        for inner in range(tile // step):
-            start = query_tile * tile + inner * step
-            result = attend(
-                q[start : start + step, pair_lanes(pair)],
-                kv[key_tile : key_tile + tile, KEYS],
-                kv[key_tile : key_tile + tile, VALUES],
-                stacked(near, pair, slice(inner * step, (inner + 1) * step), slice(0, tile)),
-            )
-            where = (slice(start, start + step), pair_lanes(pair))
-            old = tuple(ref[where] for ref in refs)
-            for ref, value in zip(refs, merge(old, result)):
+        result = attend(
+            halves(q, query_tile * tile, pair_lanes(pair))[0],
+            halves(kv, key_tile, KEYS)[1],
+            halves(kv, key_tile, VALUES)[1],
+            near_bias(near, pair, 0, slice(0, HALF)),
+        )
+        for n, rows in enumerate(half_rows(query_tile * tile, 0)):
+            where = (rows, pair_lanes(pair))
+            piece = tuple(item[n * SUB // 2 : (n + 1) * SUB // 2] for item in result)
+            for ref, value in zip(refs, merge(tuple(ref[where] for ref in refs), piece)):
                 ref[where] = value
         for residue in range(MIDDLE_DILATION):
             starts = middle_starts(0 if before else 1, residue, chunks)

time: 69.5 us -> 68.3 us (0.983)
  Pallas kernels: 19.7 us -> 16.8 us
  waiting for transfers between devices: 16.9 us -> 19.5 us
  starting transfers between devices: 30 us -> 29.1 us
    pallas_call x13, Pallas kernels: 19.7 us -> 16.8 us  [call(): pl.pallas_call(kernel, out_shape=[jax.ShapeDtypeStruct(shape, kind) for s...]
    ppermute x1, waiting for transfers between devices: 1.2 us -> 2.39 us  [layer(): q_p = lax.ppermute(q_t, 'sp', beside)]
    ppermute x1, waiting for transfers between devices: 0.01 us -> 0.95 us  [layer(): kv_b1 = lax.ppermute(kv_p1, 'sp', onward)]
    ppermute x1, starting transfers between devices: 4.5 us -> 3.79 us  [layer(): far_m = lax.ppermute(far1, 'sp', onward)]
  transfers between devices with their start and end apart: 19 -> 19, of which waited for: 7 -> 8; matrix products, arithmetic and copies ran while one was open for 2% -> 2% of each run, Pallas kernels for 25% -> 21%
where the time goes in v6:
time: 68.3 us; the launch traced here: 67.8 us
  starting transfers between devices  29.1 us (43%)
  waiting for transfers between devices  19.5 us (29%)
  Pallas kernels  16.8 us (25%)
  local copies, waits for them, and re-layouts  1.58 us (2%)
  between operations  0.85 us (1%)
    pallas_call x13, Pallas kernels, call(): pl.pallas_call(kernel, out_shape=[jax.ShapeDtypeStruct(shape, kind) for s...  16.8 us
    ppermute x1, waiting for transfers between devices, layer(): far_m = lax.ppermute(far1, 'sp', onward)  5.03 us
    ppermute x1, waiting for transfers between devices, layer(): q_b = lax.ppermute(q_p, 'sp', back)  4.15 us
    ppermute x1, starting transfers between devices, layer(): far_m = lax.ppermute(far1, 'sp', onward)  3.79 us
    ppermute x1, starting transfers between devices, layer(): kv_b0 = lax.ppermute(kv_p0, 'sp', onward)  3.71 us
    ppermute x1, waiting for transfers between devices, layer(): kv_p1 = lax.ppermute(kv_t1, 'sp', beside)  3.68 us
    ppermute x1, starting transfers between devices, layer(): kv_b1 = lax.ppermute(kv_p1, 'sp', onward)  3.49 us
    ppermute x2, starting transfers between devices, layer(): same = lax.ppermute(same, 'sp', beside)  3.11 us
  transfers between devices with their start and end apart: 19, of which 8 were waited for; matrix products, arithmetic and copies ran while one was open for 2% of the time, Pallas kernels for 21%

profile of v6, /device:TPU:0, one launch (start us, length us, event | category | flops | bytes accessed | tf_op | source)
XLA Modules:
  0.0 67.8 jit_solution(16468984670308637557)
XLA Ops:
  0.6 0.6 collective-permute-start
  1.2 0.1 collective-permute-start.18
  1.3 1.3 %slice.6.refs_2_ = bf16[2048,256]{1,0:T(8,128)(2,1)S(1)} slice(bf16[2048,512]{1,0:T(8,128)(2,1)} %refs_2_.3), slice={[0:2048], [0:256]} | slice | bytes 2097152 | tf_op jit(solution)/shard_map/slice | solution.py:597
  2.6 0.1 slice.7.refs_3_
  2.7 0.0 copy-start
  2.7 0.4 shard_map.68
  3.0 0.0 copy-start.4
  3.1 0.6 collective-permute-done.refs_1_
  3.7 0.2 copy-done
  3.9 1.7 %shard_map.70 = (bf16[512,256]{1,0:T(8,128)(2,1)S(1)}, bf16[512,256]{1,0:T(8,128)(2,1)S(1)}) custom-call(bf16[256,2048]{1,0:T(8,128)(2,1)S(1)} %copy-done, bf16[256,2048]{1,0:T(8,128)(2,1)S(1)} %collective-permute-done.refs_1_, bf16[2048,256]{1,0:T(8,128)(2,1)S(1)} %slice.6.refs_2_, bf16[2048,256]{1,0:T(8,128)(2,1)S(1)} %slice.7.refs_3_), custom_call_target="tpu_custom_call" | custom-call | flops 1073741824 | bytes 1000000 | tf_op jit(solution)/shard_map/pallas_call | solution.py:49
  5.6 0.0 copy-start.1
  5.6 3.0 %collective-permute-start.2 = (bf16[512,256]{1,0:T(8,128)(2,1)S(1)}, bf16[512,256]{1,0:T(8,128)(2,1)S(1)}, u32[]{:S(2)}, u32[]{:S(2)}) collective-permute-start(bf16[512,256]{1,0:T(8,128)(2,1)S(1)} %get-tuple-element.41), channel_id=1, source_target_pairs={{0,2},{2,0},{4,6},{6,4},{8,10},{10,8},{12,14},{14,12},{1,3},{3,1},... | collective-permute-start | bytes 786440 | tf_op jit(solution)/shard_map/ppermute | solution.py:598
  8.6 1.7 %shard_map.69 = (bf16[512,256]{1,0:T(8,128)(2,1)S(1)}, bf16[512,256]{1,0:T(8,128)(2,1)S(1)}) custom-call(bf16[256,2048]{1,0:T(8,128)(2,1)S(1)} %copy-done, bf16[256,2048]{1,0:T(8,128)(2,1)S(1)} %collective-permute-done.refs_1_, bf16[2048,512]{1,0:T(8,128)(2,1)S(1)} %copy-done.4), custom_call_target="tpu_custom_call" | custom-call | flops 1073741824 | bytes 1000000 | tf_op jit(solution)/shard_map/pallas_call | solution.py:49
  10.3 0.1 collective-permute-start.1
  10.4 1.7 %shard_map.71 = (bf16[512,256]{1,0:T(8,128)(2,1)S(1)}, bf16[512,256]{1,0:T(8,128)(2,1)S(1)}) custom-call(bf16[256,2048]{1,0:T(8,128)(2,1)S(1)} %copy-done, bf16[256,2048]{1,0:T(8,128)(2,1)S(1)} %collective-permute-done.refs_1_, bf16[2048,512]{1,0:T(8,128)(2,1)S(1)} %copy-done.1, bf16[2048,512]{1,0:T(8,128)(2,1)S(1)} %copy-done.2), custom_call_target="tpu_custom_call" | custom-call | flops 1073741824 | bytes 1000000 | tf_op jit(solution)/shard_map/pallas_call | solution.py:49
  12.0 2.1 %collective-permute-start.3 = (bf16[512,256]{1,0:T(8,128)(2,1)S(1)}, bf16[512,256]{1,0:T(8,128)(2,1)S(1)}, u32[]{:S(2)}, u32[]{:S(2)}) collective-permute-start(bf16[512,256]{1,0:T(8,128)(2,1)S(1)} %get-tuple-element.42), channel_id=1, source_target_pairs={{0,2},{2,0},{4,6},{6,4},{8,10},{10,8},{12,14},{14,12},{1,3},{3,1},... | collective-permute-start | bytes 786440 | tf_op jit(solution)/shard_map/ppermute | solution.py:604
  14.1 1.6 %collective-permute-start.4 = (bf16[512,256]{1,0:T(8,128)(2,1)S(1)}, bf16[512,256]{1,0:T(8,128)(2,1)S(1)}, u32[]{:S(2)}, u32[]{:S(2)}) collective-permute-start(bf16[512,256]{1,0:T(8,128)(2,1)S(1)} %get-tuple-element.39.kv0.rest_0_), channel_id=1, source_target_pairs={{0,4},{2,6},{4,8},{6,10},{8,12},{10,14},{12,0},{14,2},{1,5},{3,7},... | collective-permute-start | bytes 786440 | tf_op jit(solution)/shard_map/ppermute | solution.py:599
  15.7 1.7 %shard_map.72 = (f32[512,256]{1,0:T(8,128)S(1)}, f32[512,256]{1,0:T(8,128)S(1)}, f32[512,256]{1,0:T(8,128)S(1)}) custom-call(f32[4,2,128,256]{3,2,1,0:T(8,128)S(1)} %get-tuple-element.34.near, f32[4,128,256]{2,1,0:T(8,128)S(1)} %get-tuple-element.35.mid, bf16[512,256]{1,0:T(8,128)(2,1)S(1)} %get-tuple-element.37.q.q_mine, ...), custom_call_target="tpu_custom_call" | custom-call | flops 4000000000 | bytes 1000000 | tf_op jit(solution)/shard_map/pallas_call | solution.py:49
  17.4 1.6 %collective-permute-start.6 = (bf16[512,256]{1,0:T(8,128)(2,1)S(1)}, bf16[512,256]{1,0:T(8,128)(2,1)S(1)}, u32[]{:S(2)}, u32[]{:S(2)}) collective-permute-start(bf16[512,256]{1,0:T(8,128)(2,1)S(1)} %get-tuple-element.40.kv1.rest_1_), channel_id=1, source_target_pairs={{0,4},{2,6},{4,8},{6,10},{8,12},{10,14},{12,0},{14,2},{1,5},{3,7},... | collective-permute-start | bytes 786440 | tf_op jit(solution)/shard_map/ppermute | solution.py:605
  19.0 2.4 %collective-permute-done.1.q.q_part = bf16[512,256]{1,0:T(8,128)(2,1)S(1)} collective-permute-done((bf16[512,256]{1,0:T(8,128)(2,1)S(1)}, bf16[512,256]{1,0:T(8,128)(2,1)S(1)}, u32[]{:S(2)}, u32[]{:S(2)}) %collective-permute-start.1) | collective-permute-done | bytes 262176 | tf_op jit(solution)/shard_map/ppermute | solution.py:601
  21.4 1.3 %collective-permute-start.8 = (bf16[512,256]{1,0:T(8,128)(2,1)S(1)}, bf16[512,256]{1,0:T(8,128)(2,1)S(1)}, u32[]{:S(2)}, u32[]{:S(2)}) collective-permute-start(bf16[512,256]{1,0:T(8,128)(2,1)S(1)} %get-tuple-element.37.q.q_mine), channel_id=1, source_target_pairs={{4,0},{6,2},{8,4},{10,6},{12,8},{14,10},{5,1},{7,3},{9,5},{11,7},{... | collective-permute-start | bytes 786440 | tf_op jit(solution)/shard_map/ppermute | solution.py:602
  22.7 3.7 %collective-permute-done.3.kv1.rest_3_ = bf16[512,256]{1,0:T(8,128)(2,1)S(1)} collective-permute-done((bf16[512,256]{1,0:T(8,128)(2,1)S(1)}, bf16[512,256]{1,0:T(8,128)(2,1)S(1)}, u32[]{:S(2)}, u32[]{:S(2)}) %collective-permute-start.3) | collective-permute-done | bytes 262176 | tf_op jit(solution)/shard_map/ppermute | solution.py:604
  26.4 3.7 %collective-permute-start.5 = (bf16[512,256]{1,0:T(8,128)(2,1)S(1)}, bf16[512,256]{1,0:T(8,128)(2,1)S(1)}, u32[]{:S(2)}, u32[]{:S(2)}) collective-permute-start(bf16[512,256]{1,0:T(8,128)(2,1)S(1)} %collective-permute-done.2.kv0.rest_2_), channel_id=1, source_target_pairs={{0,4},{2,6},{4,8},{6,10},{8,12},{10,14},{1,5},{3,7},{5,9},{7,11},{... | collective-permute-start | bytes 786440 | tf_op jit(solution)/shard_map/ppermute | solution.py:606
  30.1 1.7 %shard_map.73 = (f32[512,256]{1,0:T(8,128)S(1)}, f32[512,256]{1,0:T(8,128)S(1)}, f32[512,256]{1,0:T(8,128)S(1)}) custom-call(f32[4,2,128,256]{3,2,1,0:T(8,128)S(1)} %get-tuple-element.34.near, f32[4,128,256]{2,1,0:T(8,128)S(1)} %get-tuple-element.35.mid, bf16[512,256]{1,0:T(8,128)(2,1)S(1)} %collective-permute-done.1.q.q_part, ...), custom_call_target="tpu_custom_call" | custom-call | flops 4000000000 | bytes 1000000 | tf_op jit(solution)/shard_map/pallas_call | solution.py:49
  31.8 3.5 %collective-permute-start.7 = (bf16[512,256]{1,0:T(8,128)(2,1)S(1)}, bf16[512,256]{1,0:T(8,128)(2,1)S(1)}, u32[]{:S(2)}, u32[]{:S(2)}) collective-permute-start(bf16[512,256]{1,0:T(8,128)(2,1)S(1)} %collective-permute-done.3.kv1.rest_3_), channel_id=1, source_target_pairs={{0,4},{2,6},{4,8},{6,10},{8,12},{10,14},{1,5},{3,7},{5,9},{7,11},{... | collective-permute-start | bytes 786440 | tf_op jit(solution)/shard_map/ppermute | solution.py:608
  35.3 0.0 collective-permute-done.8.q_a
  35.3 1.3 %collective-permute-start.9 = (bf16[512,256]{1,0:T(8,128)(2,1)S(1)}, bf16[512,256]{1,0:T(8,128)(2,1)S(1)}, u32[]{:S(2)}, u32[]{:S(2)}) collective-permute-start(bf16[512,256]{1,0:T(8,128)(2,1)S(1)} %collective-permute-done.1.q.q_part), channel_id=1, source_target_pairs={{4,0},{6,2},{8,4},{10,6},{12,8},{14,10},{5,1},{7,3},{9,5},{11,7},{... | collective-permute-start | bytes 786440 | tf_op jit(solution)/shard_map/ppermute | solution.py:607
  36.6 3.0 %shard_map.74 = (f32[1024,256]{1,0:T(8,128)S(1)}, f32[1024,256]{1,0:T(8,128)S(1)}, f32[1024,256]{1,0:T(8,128)S(1)}, bf16[1024,256]{1,0:T(8,128)(2,1)S(1)}) custom-call(f32[4,2,128,256]{3,2,1,0:T(8,128)S(1)} %get-tuple-element.34.near, f32[4,128,256]{2,1,0:T(8,128)S(1)} %get-tuple-element.35.mid, f32[3,4,64,64]{3,2,1,0:T(8,128)S(1)} %get-tuple-element.36.far, ...), custom_call_target="tpu_custom_call" | custom-call | flops 4000000000 | bytes 1000000 | tf_op jit(solution)/shard_map/pallas_call | solution.py:49
  39.6 1.0 %collective-permute-done.7.kv_b1.kv_b = bf16[512,256]{1,0:T(8,128)(2,1)S(1)} collective-permute-done((bf16[512,256]{1,0:T(8,128)(2,1)S(1)}, bf16[512,256]{1,0:T(8,128)(2,1)S(1)}, u32[]{:S(2)}, u32[]{:S(2)}) %collective-permute-start.7) | collective-permute-done | bytes 262176 | tf_op jit(solution)/shard_map/ppermute | solution.py:608
  40.6 4.1 %collective-permute-done.9.q_b = bf16[512,256]{1,0:T(8,128)(2,1)S(1)} collective-permute-done((bf16[512,256]{1,0:T(8,128)(2,1)S(1)}, bf16[512,256]{1,0:T(8,128)(2,1)S(1)}, u32[]{:S(2)}, u32[]{:S(2)}) %collective-permute-start.9) | collective-permute-done | bytes 262176 | tf_op jit(solution)/shard_map/ppermute | solution.py:607
  44.7 0.2 shard_map.78
  44.9 3.8 %collective-permute-start.14 = (bf16[1088,128]{1,0:T(8,128)(2,1)S(1)}, bf16[1088,128]{1,0:T(8,128)(2,1)S(1)}, u32[]{:S(2)}, u32[]{:S(2)}) collective-permute-start(bf16[1088,128]{1,0:T(8,128)(2,1)S(1)} %shard_map.78), channel_id=1, source_target_pairs={{0,4},{2,6},{4,8},{6,10},{8,12},{10,14},{1,5},{3,7},{5,9},{7,11},{... | collective-permute-start | bytes 835592 | tf_op jit(solution)/shard_map/ppermute | solution.py:617
  48.7 0.0 collective-permute-done.4.kv_a0.kv_a
  48.7 0.2 shard_map.76
  49.0 1.3 %collective-permute-start.10 = (bf16[1088,128]{1,0:T(8,128)(2,1)S(1)}, bf16[1088,128]{1,0:T(8,128)(2,1)S(1)}, u32[]{:S(2)}, u32[]{:S(2)}) collective-permute-start(bf16[1088,128]{1,0:T(8,128)(2,1)S(1)} %shard_map.76), channel_id=1, source_target_pairs={{0,4},{2,6},{4,8},{6,10},{8,12},{10,14},{12,0},{14,2},{1,5},{3,7},... | collective-permute-start | bytes 835592 | tf_op jit(solution)/shard_map/ppermute | solution.py:614
  50.3 0.2 shard_map.75
  50.5 5.0 %collective-permute-done.14.far_in = bf16[1088,128]{1,0:T(8,128)(2,1)S(1)} collective-permute-done((bf16[1088,128]{1,0:T(8,128)(2,1)S(1)}, bf16[1088,128]{1,0:T(8,128)(2,1)S(1)}, u32[]{:S(2)}, u32[]{:S(2)}) %collective-permute-start.14) | collective-permute-done | bytes 278560 | tf_op jit(solution)/shard_map/ppermute | solution.py:617
  55.5 1.1 %shard_map.79 = (bf16[256,128]{1,0:T(8,128)(2,1)S(1)}, bf16[256,128]{1,0:T(8,128)(2,1)S(1)}, bf16[320,128]{1,0:T(8,128)(2,1)S(1)}, bf16[256,128]{1,0:T(8,128)(2,1)S(1)}, bf16[16,512]{1,0:T(8,128)(2,1)S(1)}) custom-call(f32[1024,256]{1,0:T(8,128)S(1)} %get-tuple-element.53.o_in, f32[1024,256]{1,0:T(8,128)S(1)} %get-tuple-element.54.m_in, ...), custom_call_target="tpu_custom_call" | custom-call | flops 1000000000 | bytes 1000000 | tf_op jit(solution)/shard_map/pallas_call | solution.py:49
  56.6 1.6 %collective-permute-start.15 = (bf16[320,128]{1,0:T(8,128)(2,1)S(1)}, bf16[320,128]{1,0:T(8,128)(2,1)S(1)}, u32[]{:S(2)}, u32[]{:S(2)}) collective-permute-start(bf16[320,128]{1,0:T(8,128)(2,1)S(1)} %get-tuple-element.62), channel_id=1, source_target_pairs={{0,2},{2,0},{4,6},{6,4},{8,10},{10,8},{12,14},{14,12},{1,3},{3,1},... | collective-permute-start | bytes 245768 | tf_op jit(solution)/shard_map/ppermute | solution.py:622
  58.1 0.6 collective-permute-start.17
  58.8 0.0 collective-permute-done.10.far_in
  58.8 1.1 %shard_map.77 = (bf16[256,128]{1,0:T(8,128)(2,1)S(1)}, bf16[256,128]{1,0:T(8,128)(2,1)S(1)}, bf16[320,128]{1,0:T(8,128)(2,1)S(1)}, bf16[256,128]{1,0:T(8,128)(2,1)S(1)}, bf16[16,512]{1,0:T(8,128)(2,1)S(1)}) custom-call(f32[1024,256]{1,0:T(8,128)S(1)} %get-tuple-element.53.o_in, f32[1024,256]{1,0:T(8,128)S(1)} %get-tuple-element.54.m_in, ...), custom_call_target="tpu_custom_call" | custom-call | flops 1000000000 | bytes 1000000 | tf_op jit(solution)/shard_map/pallas_call | solution.py:49
  59.8 1.6 %collective-permute-start.11 = (bf16[320,128]{1,0:T(8,128)(2,1)S(1)}, bf16[320,128]{1,0:T(8,128)(2,1)S(1)}, u32[]{:S(2)}, u32[]{:S(2)}) collective-permute-start(bf16[320,128]{1,0:T(8,128)(2,1)S(1)} %get-tuple-element.57), channel_id=1, source_target_pairs={{0,2},{2,0},{4,6},{6,4},{8,10},{10,8},{12,14},{14,12},{1,3},{3,1},... | collective-permute-start | bytes 245768 | tf_op jit(solution)/shard_map/ppermute | solution.py:622
  61.4 0.0 collective-permute-done.16.refs_7_
  61.4 0.4 collective-permute-done.17.refs_8_
  61.8 1.5 %collective-permute-start.13 = (bf16[256,128]{1,0:T(8,128)(2,1)S(1)}, bf16[256,128]{1,0:T(8,128)(2,1)S(1)}, u32[]{:S(2)}, u32[]{:S(2)}) collective-permute-start(bf16[256,128]{1,0:T(8,128)(2,1)S(1)} %get-tuple-element.59), channel_id=1, source_target_pairs={{0,3},{1,2},{2,1},{3,0},{4,7},{5,6},{6,5},{7,4},{8,11},{9,10},{10,... | collective-permute-start | bytes 196616 | tf_op jit(solution)/shard_map/ppermute | solution.py:623
  63.4 2.2 %collective-permute-done.13.refs_3_ = bf16[256,128]{1,0:T(8,128)(2,1)S(1)} collective-permute-done((bf16[256,128]{1,0:T(8,128)(2,1)S(1)}, bf16[256,128]{1,0:T(8,128)(2,1)S(1)}, u32[]{:S(2)}, u32[]{:S(2)}) %collective-permute-start.13) | collective-permute-done | bytes 65568 | tf_op jit(solution)/shard_map/ppermute | solution.py:623
  65.6 2.3 %shard_map.80 = (bf16[256,2048]{1,0:T(8,128)(2,1)}, f32[8,512]{1,0:T(8,128)}) custom-call(bf16[256,128]{1,0:T(8,128)(2,1)S(1)} %get-tuple-element.56.refs_0_, bf16[320,128]{1,0:T(8,128)(2,1)S(1)} %collective-permute-done.11.refs_1_, bf16[256,128]{1,0:T(8,128)(2,1)S(1)} %collective-permute-done.12.refs_2_, ...), custom_call_target="tpu_custom_call" | custom-call | flops 1073741824 | bytes 1000000 | tf_op jit(solution)/shard_map/pallas_call | solution.py:49
  (15 shorter events, 0.0 us)
Async XLA Ops:
  0.6 1.9 %copy-start.2 = (bf16[2048,512]{1,0:T(8,128)(2,1)S(1)}, bf16[2048,512]{1,0:T(8,128)(2,1)}, u32[]{:S(2)}) copy-start(bf16[2048,512]{1,0:T(8,128)(2,1)} %refs_3_.1) | copy-start | bytes 6291460
  0.6 3.1 %collective-permute-start = (bf16[256,2048]{1,0:T(8,128)(2,1)}, bf16[256,2048]{1,0:T(8,128)(2,1)S(1)}, u32[]{:S(2)}, u32[]{:S(2)}) collective-permute-start(bf16[256,2048]{1,0:T(8,128)(2,1)} %refs_0_.5), channel_id=1, source_target_pairs={{0,1},{1,0},{2,3},{3,2},{4,5},{5,4},{6,7},{7,6},{8,9},{9,8},{10,11... | collective-permute-start | bytes 3145736 | tf_op jit(solution)/shard_map/ppermute | solution.py:596
  1.2 64.3 %collective-permute-start.18 = (bf16[512,2048]{1,0:T(8,128)(2,1)}, bf16[512,2048]{1,0:T(8,128)(2,1)S(1)}, u32[]{:S(2)}, u32[]{:S(2)}) collective-permute-start(bf16[512,2048]{1,0:T(8,128)(2,1)} %refs_10_.1), channel_id=1, source_target_pairs={{0,1},{1,0},{2,3},{3,2},{4,5},{5,4},{6,7},{7,6},{8,9},{9,8},{10,11... | collective-permute-start | bytes 6291464 | tf_op jit(solution)/shard_map/ppermute | solution.py:609
  2.7 1.2 %copy-start = (bf16[256,2048]{1,0:T(8,128)(2,1)S(1)}, bf16[256,2048]{1,0:T(8,128)(2,1)}, u32[]{:S(2)}) copy-start(bf16[256,2048]{1,0:T(8,128)(2,1)} %refs_0_.5) | copy-start | bytes 3145732
  3.0 5.6 %copy-start.4 = (bf16[2048,512]{1,0:T(8,128)(2,1)S(1)}, bf16[2048,512]{1,0:T(8,128)(2,1)}, u32[]{:S(2)}) copy-start(bf16[2048,512]{1,0:T(8,128)(2,1)} %refs_2_.2) | copy-start | bytes 6291460
  5.6 4.8 %copy-start.1 = (bf16[2048,512]{1,0:T(8,128)(2,1)S(1)}, bf16[2048,512]{1,0:T(8,128)(2,1)}, u32[]{:S(2)}) copy-start(bf16[2048,512]{1,0:T(8,128)(2,1)} %refs_2_.3) | copy-start | bytes 6291460
  5.6 11.8 %collective-permute-start.2 = (bf16[512,256]{1,0:T(8,128)(2,1)S(1)}, bf16[512,256]{1,0:T(8,128)(2,1)S(1)}, u32[]{:S(2)}, u32[]{:S(2)}) collective-permute-start(bf16[512,256]{1,0:T(8,128)(2,1)S(1)} %get-tuple-element.41), channel_id=1, source_target_pairs={{0,2},{2,0},{4,6},{6,4},{8,10},{10,8},{12,14},{14,12},{1,3},{3,1},... | collective-permute-start | bytes 786440 | tf_op jit(solution)/shard_map/ppermute | solution.py:598
  10.3 11.1 %collective-permute-start.1 = (bf16[512,256]{1,0:T(8,128)(2,1)S(1)}, bf16[512,256]{1,0:T(8,128)(2,1)S(1)}, u32[]{:S(2)}, u32[]{:S(2)}) collective-permute-start(bf16[512,256]{1,0:T(8,128)(2,1)S(1)} %get-tuple-element.38), channel_id=1, source_target_pairs={{0,2},{2,0},{4,6},{6,4},{8,10},{10,8},{12,14},{14,12},{1,3},{3,1},... | collective-permute-start | bytes 786440 | tf_op jit(solution)/shard_map/ppermute | solution.py:601
  12.0 14.3 %collective-permute-start.3 = (bf16[512,256]{1,0:T(8,128)(2,1)S(1)}, bf16[512,256]{1,0:T(8,128)(2,1)S(1)}, u32[]{:S(2)}, u32[]{:S(2)}) collective-permute-start(bf16[512,256]{1,0:T(8,128)(2,1)S(1)} %get-tuple-element.42), channel_id=1, source_target_pairs={{0,2},{2,0},{4,6},{6,4},{8,10},{10,8},{12,14},{14,12},{1,3},{3,1},... | collective-permute-start | bytes 786440 | tf_op jit(solution)/shard_map/ppermute | solution.py:604
  14.1 34.6 %collective-permute-start.4 = (bf16[512,256]{1,0:T(8,128)(2,1)S(1)}, bf16[512,256]{1,0:T(8,128)(2,1)S(1)}, u32[]{:S(2)}, u32[]{:S(2)}) collective-permute-start(bf16[512,256]{1,0:T(8,128)(2,1)S(1)} %get-tuple-element.39.kv0.rest_0_), channel_id=1, source_target_pairs={{0,4},{2,6},{4,8},{6,10},{8,12},{10,14},{12,0},{14,2},{1,5},{3,7},... | collective-permute-start | bytes 786440 | tf_op jit(solution)/shard_map/ppermute | solution.py:599
  17.4 14.4 %collective-permute-start.6 = (bf16[512,256]{1,0:T(8,128)(2,1)S(1)}, bf16[512,256]{1,0:T(8,128)(2,1)S(1)}, u32[]{:S(2)}, u32[]{:S(2)}) collective-permute-start(bf16[512,256]{1,0:T(8,128)(2,1)S(1)} %get-tuple-element.40.kv1.rest_1_), channel_id=1, source_target_pairs={{0,4},{2,6},{4,8},{6,10},{8,12},{10,14},{12,0},{14,2},{1,5},{3,7},... | collective-permute-start | bytes 786440 | tf_op jit(solution)/shard_map/ppermute | solution.py:605
  21.4 13.9 %collective-permute-start.8 = (bf16[512,256]{1,0:T(8,128)(2,1)S(1)}, bf16[512,256]{1,0:T(8,128)(2,1)S(1)}, u32[]{:S(2)}, u32[]{:S(2)}) collective-permute-start(bf16[512,256]{1,0:T(8,128)(2,1)S(1)} %get-tuple-element.37.q.q_mine), channel_id=1, source_target_pairs={{4,0},{6,2},{8,4},{10,6},{12,8},{14,10},{5,1},{7,3},{9,5},{11,7},{... | collective-permute-start | bytes 786440 | tf_op jit(solution)/shard_map/ppermute | solution.py:602
  26.4 22.4 %collective-permute-start.5 = (bf16[512,256]{1,0:T(8,128)(2,1)S(1)}, bf16[512,256]{1,0:T(8,128)(2,1)S(1)}, u32[]{:S(2)}, u32[]{:S(2)}) collective-permute-start(bf16[512,256]{1,0:T(8,128)(2,1)S(1)} %collective-permute-done.2.kv0.rest_2_), channel_id=1, source_target_pairs={{0,4},{2,6},{4,8},{6,10},{8,12},{10,14},{1,5},{3,7},{5,9},{7,11},{... | collective-permute-start | bytes 786440 | tf_op jit(solution)/shard_map/ppermute | solution.py:606
  31.8 8.8 %collective-permute-start.7 = (bf16[512,256]{1,0:T(8,128)(2,1)S(1)}, bf16[512,256]{1,0:T(8,128)(2,1)S(1)}, u32[]{:S(2)}, u32[]{:S(2)}) collective-permute-start(bf16[512,256]{1,0:T(8,128)(2,1)S(1)} %collective-permute-done.3.kv1.rest_3_), channel_id=1, source_target_pairs={{0,4},{2,6},{4,8},{6,10},{8,12},{10,14},{1,5},{3,7},{5,9},{7,11},{... | collective-permute-start | bytes 786440 | tf_op jit(solution)/shard_map/ppermute | solution.py:608
  35.3 9.4 %collective-permute-start.9 = (bf16[512,256]{1,0:T(8,128)(2,1)S(1)}, bf16[512,256]{1,0:T(8,128)(2,1)S(1)}, u32[]{:S(2)}, u32[]{:S(2)}) collective-permute-start(bf16[512,256]{1,0:T(8,128)(2,1)S(1)} %collective-permute-done.1.q.q_part), channel_id=1, source_target_pairs={{4,0},{6,2},{8,4},{10,6},{12,8},{14,10},{5,1},{7,3},{9,5},{11,7},{... | collective-permute-start | bytes 786440 | tf_op jit(solution)/shard_map/ppermute | solution.py:607
  44.9 10.6 %collective-permute-start.14 = (bf16[1088,128]{1,0:T(8,128)(2,1)S(1)}, bf16[1088,128]{1,0:T(8,128)(2,1)S(1)}, u32[]{:S(2)}, u32[]{:S(2)}) collective-permute-start(bf16[1088,128]{1,0:T(8,128)(2,1)S(1)} %shard_map.78), channel_id=1, source_target_pairs={{0,4},{2,6},{4,8},{6,10},{8,12},{10,14},{1,5},{3,7},{5,9},{7,11},{... | collective-permute-start | bytes 835592 | tf_op jit(solution)/shard_map/ppermute | solution.py:617
  49.0 9.8 %collective-permute-start.10 = (bf16[1088,128]{1,0:T(8,128)(2,1)S(1)}, bf16[1088,128]{1,0:T(8,128)(2,1)S(1)}, u32[]{:S(2)}, u32[]{:S(2)}) collective-permute-start(bf16[1088,128]{1,0:T(8,128)(2,1)S(1)} %shard_map.76), channel_id=1, source_target_pairs={{0,4},{2,6},{4,8},{6,10},{8,12},{10,14},{12,0},{14,2},{1,5},{3,7},... | collective-permute-start | bytes 835592 | tf_op jit(solution)/shard_map/ppermute | solution.py:614
  56.6 9.0 %copy-start.3 = (bf16[512,2048]{1,0:T(8,128)(2,1)S(1)}, bf16[512,2048]{1,0:T(8,128)(2,1)}, u32[]{:S(2)}) copy-start(bf16[512,2048]{1,0:T(8,128)(2,1)} %refs_10_.1) | copy-start | bytes 6291460
  56.6 9.0 %collective-permute-start.15 = (bf16[320,128]{1,0:T(8,128)(2,1)S(1)}, bf16[320,128]{1,0:T(8,128)(2,1)S(1)}, u32[]{:S(2)}, u32[]{:S(2)}) collective-permute-start(bf16[320,128]{1,0:T(8,128)(2,1)S(1)} %get-tuple-element.62), channel_id=1, source_target_pairs={{0,2},{2,0},{4,6},{6,4},{8,10},{10,8},{12,14},{14,12},{1,3},{3,1},... | collective-permute-start | bytes 245768 | tf_op jit(solution)/shard_map/ppermute | solution.py:622
  58.1 3.3 %collective-permute-start.16 = (bf16[256,128]{1,0:T(8,128)(2,1)S(1)}, bf16[256,128]{1,0:T(8,128)(2,1)S(1)}, u32[]{:S(2)}, u32[]{:S(2)}) collective-permute-start(bf16[256,128]{1,0:T(8,128)(2,1)S(1)} %get-tuple-element.63), channel_id=1, source_target_pairs={{0,1},{1,0},{2,3},{3,2},{4,5},{5,4},{6,7},{7,6},{8,9},{9,8},{10,11... | collective-permute-start | bytes 196616 | tf_op jit(solution)/shard_map/ppermute | solution.py:624
  58.1 3.7 %collective-permute-start.17 = (bf16[256,128]{1,0:T(8,128)(2,1)S(1)}, bf16[256,128]{1,0:T(8,128)(2,1)S(1)}, u32[]{:S(2)}, u32[]{:S(2)}) collective-permute-start(bf16[256,128]{1,0:T(8,128)(2,1)S(1)} %get-tuple-element.64), channel_id=1, source_target_pairs={{0,3},{1,2},{2,1},{3,0},{4,7},{5,6},{6,5},{7,4},{8,11},{9,10},{10,... | collective-permute-start | bytes 196616 | tf_op jit(solution)/shard_map/ppermute | solution.py:623
  59.8 5.7 %collective-permute-start.11 = (bf16[320,128]{1,0:T(8,128)(2,1)S(1)}, bf16[320,128]{1,0:T(8,128)(2,1)S(1)}, u32[]{:S(2)}, u32[]{:S(2)}) collective-permute-start(bf16[320,128]{1,0:T(8,128)(2,1)S(1)} %get-tuple-element.57), channel_id=1, source_target_pairs={{0,2},{2,0},{4,6},{6,4},{8,10},{10,8},{12,14},{14,12},{1,3},{3,1},... | collective-permute-start | bytes 245768 | tf_op jit(solution)/shard_map/ppermute | solution.py:622
  61.4 2.0 %collective-permute-start.12 = (bf16[256,128]{1,0:T(8,128)(2,1)S(1)}, bf16[256,128]{1,0:T(8,128)(2,1)S(1)}, u32[]{:S(2)}, u32[]{:S(2)}) collective-permute-start(bf16[256,128]{1,0:T(8,128)(2,1)S(1)} %get-tuple-element.58), channel_id=1, source_target_pairs={{0,1},{1,0},{2,3},{3,2},{4,5},{5,4},{6,7},{7,6},{8,9},{9,8},{10,11... | collective-permute-start | bytes 196616 | tf_op jit(solution)/shard_map/ppermute | solution.py:624
  61.8 3.7 %collective-permute-start.13 = (bf16[256,128]{1,0:T(8,128)(2,1)S(1)}, bf16[256,128]{1,0:T(8,128)(2,1)S(1)}, u32[]{:S(2)}, u32[]{:S(2)}) collective-permute-start(bf16[256,128]{1,0:T(8,128)(2,1)S(1)} %get-tuple-element.59), channel_id=1, source_target_pairs={{0,3},{1,2},{2,1},{3,0},{4,7},{5,6},{6,5},{7,4},{8,11},{9,10},{10,... | collective-permute-start | bytes 196616 | tf_op jit(solution)/shard_map/ppermute | solution.py:623
